TPU v7x, 256 devices: a whole 4x4x8 slice. The times are simulated.
256 devices in a mesh: kv: 32 (over z, y), tp: 8 (over x, core).
Axes of the slice: x: 4, y: 4, z: 8, core: 2. Of those that a mesh axis runs over, the one named last changes fastest.
Arguments:
- residual_in: bfloat16 [256, 2048], P(None, ('kv', 'tp')), may hold values from -14 to 14
- delta_state: float32 [256, 32, 128, 128], P('kv', 'tp'), may hold values from -1 to 1
- norm_gain_first: float32 [2048], P('kv'), may hold values from 0.1 to 1.9
- gate_first: bfloat16 [2048, 5632], P('kv', 'tp'), may hold values from -0.125 to 0.125
- up_first: bfloat16 [2048, 5632], P('kv', 'tp'), may hold values from -0.125 to 0.125
- down_first: bfloat16 [5632, 2048], P('tp', 'kv'), may hold values from -0.15625 to 0.15625
- norm_gain_mixer: float32 [2048], P('kv'), may hold values from 0.1 to 1.9
- query_weight: bfloat16 [2048, 2048], P('kv', 'tp'), may hold values from -0.125 to 0.125
- key_weight: bfloat16 [2048, 2048], P('kv', 'tp'), may hold values from -0.125 to 0.125
- value_weight: bfloat16 [2048, 4096], P('kv', 'tp'), may hold values from -0.125 to 0.125
- output_gate_weight: bfloat16 [2048, 4096], P('kv', 'tp'), may hold values from -0.125 to 0.125
- beta_weight: bfloat16 [2048, 32], P('kv'), may hold values from -0.125 to 0.125
- decay_weight: bfloat16 [2048, 32], P('kv'), may hold values from -0.125 to 0.125
- decay_rate: float32 [32], P('tp'), may hold values from -2.3 to 1.1
- decay_bias: float32 [32], P('tp'), may hold values from -1 to 1
- head_gain: float32 [128], replicated, may hold values from 0.1 to 1.9
- out_weight: bfloat16 [4096, 2048], P('tp', 'kv'), may hold values from -0.125 to 0.125
- norm_gain_second: float32 [2048], P('kv'), may hold values from 0.1 to 1.9
- gate_second: bfloat16 [2048, 5632], P('kv', 'tp'), may hold values from -0.125 to 0.125
- up_second: bfloat16 [2048, 5632], P('kv', 'tp'), may hold values from -0.125 to 0.125
- down_second: bfloat16 [5632, 2048], P('tp', 'kv'), may hold values from -0.15625 to 0.15625
Outputs:
- residual_out: bfloat16 [256, 2048], P(None, ('kv', 'tp'))
- delta_state_out: float32 [256, 32, 128, 128], P('kv', 'tp')
All inputs are finite; a program needn't handle non-finite values.
Results may differ from a plain program's by a relative error of at most 0.03.
Values may be sent and summed in bfloat16 or wider, within the bound.
No kernel may reach another device: no remote copies, remote signals or barrier semaphores. Data moves between devices by JAX's collectives and lax.ppermute only.
A program may use at most 64 MiB of HBM per device.

v0:
```python
import jax
import jax.numpy as jnp
from jax import lax
from jax.experimental import pallas as pl
from jax.experimental.pallas import tpu as pltpu
from jax.sharding import Mesh
from jax.sharding import PartitionSpec as P


D = 2048
HEAD = 128
GATES = 128

epsilon = 1e-06

TP = ("x", "c")
ACROSS = ("z", "x", "c")

bf16 = jnp.bfloat16
f32 = jnp.float32


def exchange(blocks, axis):
    return lax.all_to_all(blocks, axis, split_axis=0, concat_axis=0, tiled=True)


def from_everyone(value, axis):
    return exchange(jnp.broadcast_to(value, (lax.axis_size(axis), *value.shape)), axis)


def everyone_sum(value, axis):
    return from_everyone(value, axis).astype(f32).sum(axis=0)


def ring_sum(value, axis):
    size = lax.axis_size(axis)
    total = value.astype(f32)
    for places in range(1, size):
        total = total + lax.ppermute(value, axis, [(i, (i + places) % size) for i in range(size)]).astype(f32)
    return total


def times_transposed(left, right_rows):
    return lax.dot_general(left, right_rows, (((1,), (1,)), ((), ())), preferred_element_type=f32)


def square_columns(as_float):
    squares = jnp.sum(as_float * as_float, axis=1, keepdims=True)
    high = squares.astype(bf16).astype(f32)
    lane = lax.broadcasted_iota(jnp.int32, (squares.shape[0], GATES), 1)
    return jnp.where(lane == 0, high, jnp.where(lane == 1, squares - high, 0.0))


def row_scale(first_two):
    return lax.rsqrt((first_two[:, :1] + first_two[:, 1:2]) / D + epsilon)


def around(block, axis):
    size = lax.axis_size(axis)
    ahead = [(i, (i + 1) % size) for i in range(size)]
    behind = [(i, (i - 1) % size) for i in range(size)]
    blocks = [block] + [None] * (size - 1)
    forward = backward = block
    for step in range(1, size // 2):
        forward = blocks[size - step] = lax.ppermute(forward, axis, ahead)
        backward = blocks[step] = lax.ppermute(backward, axis, behind)
    half = block.shape[1] // 2
    forward = lax.ppermute(forward[:, :half], axis, ahead)
    backward = lax.ppermute(backward[:, half:], axis, behind)
    blocks[size // 2] = jnp.concatenate([forward, backward], axis=1)
    return blocks


def hidden_units(residual, partial_value):
    both = jnp.concatenate([partial_value, square_columns(residual.astype(f32))], axis=1).astype(bf16)
    summed = ring_sum(both, "y")
    width = partial_value.shape[1]
    scale = row_scale(summed[:, width:])
    gate_act = summed[:, : width // 2] * scale
    up_act = summed[:, width // 2 : width] * scale
    return (jax.nn.silu(gate_act) * up_act).astype(bf16)


def unit_heads(activated):
    squares = jnp.sum(activated * activated, axis=-1, keepdims=True)
    return activated * lax.rsqrt(squares + epsilon)


def mixer_kernel(
    arrived_ref, rate_ref, bias_ref, gain_ref, state_ref, out_ref, new_ref, made, read_ref, went
):
    count, heads = state_ref.shape[:2]
    pairs = heads // 2
    store = [pltpu.make_async_copy(made.at[s], new_ref.at[s], went.at[s]) for s in range(count)]
    summed = arrived_ref[0].astype(f32)
    for i in range(1, arrived_ref.shape[0]):
        summed = summed + arrived_ref[i].astype(f32)
    width = summed.shape[1] - GATES
    tail = summed[:, width:]
    scale = row_scale(tail[:, 2 * heads : 2 * heads + 2])
    gates = tail * scale
    activated = jax.nn.silu(summed[:, :width] * scale)
    beta = jax.nn.sigmoid(gates[:, :heads])
    drive = gates[:, heads : 2 * heads] + bias_ref[...]
    softplus = jnp.maximum(drive, 0.0) + jnp.log1p(jnp.exp(-jnp.abs(drive)))
    decay = jnp.exp(-jnp.exp(rate_ref[...]) * softplus)
    head = lambda at: activated[:, at * HEAD : (at + 1) * HEAD]
    rows = [unit_heads(head(m)) * HEAD ** (-0.5) for m in range(pairs)]
    rows += [unit_heads(head(pairs + m)) for m in range(pairs)]
    rows.append(jnp.zeros((HEAD - 2 * pairs * count, HEAD), f32))
    turned = jnp.concatenate(rows, axis=0).T
    for s in range(count):
        for m in range(pairs):
            at = m * count + s
            query = jnp.broadcast_to(turned[:, at : at + 1], (HEAD, HEAD))
            at += pairs * count
            key = jnp.broadcast_to(turned[:, at : at + 1], (HEAD, HEAD))
            for h in (2 * m, 2 * m + 1):
                faded = state_ref[s, h] * decay[s : s + 1, h : h + 1]
                predicted = jnp.sum(faded * key, axis=0, keepdims=True)
                value = head(2 * pairs + h)[s : s + 1]
                correction = beta[s : s + 1, h : h + 1] * (value - predicted)
                updated = faded + key * correction
                made[s, h] = updated
                read_ref[s : s + 1, h * HEAD : (h + 1) * HEAD] = jnp.sum(
                    updated * query, axis=0, keepdims=True
                )
        store[s].start()
    for h in range(heads):
        columns = slice(h * HEAD, (h + 1) * HEAD)
        reading = read_ref[:, columns]
        mean = jnp.sum(reading * reading, axis=-1, keepdims=True) / HEAD
        normed = reading * lax.rsqrt(mean + epsilon) * gain_ref[...] * head(2 * pairs + heads + h)
        for i in range(out_ref.shape[0]):
            out_ref[i, :, columns] = normed.astype(bf16)
    for copy in store:
        copy.wait()


def mixer_values(residual, mixer_in, decay_rate, decay_bias, head_gain, old_state):
    row_count, heads_dev, head_size = old_state.shape[:3]
    projected = jnp.dot(residual, mixer_in, preferred_element_type=f32)
    width = mixer_in.shape[1] - GATES
    squares = square_columns(residual.astype(f32))
    tail = projected[:, width:] + jnp.roll(squares, 2 * heads_dev, axis=1)
    both = jnp.concatenate([projected[:, :width], tail], axis=1).astype(bf16)
    arrived = exchange(both.reshape(-1, row_count, both.shape[1]), "y")
    whole = pl.BlockSpec(memory_space=pltpu.VMEM)
    return pl.pallas_call(
        mixer_kernel,
        out_shape=(
            jax.ShapeDtypeStruct((arrived.shape[0], row_count, heads_dev * head_size), bf16),
            jax.ShapeDtypeStruct(old_state.shape, f32),
        ),
        in_specs=[whole] * 5,
        out_specs=(whole, pl.BlockSpec(memory_space=pl.ANY)),
        scratch_shapes=[
            pltpu.VMEM(old_state.shape, f32),
            pltpu.VMEM((row_count, heads_dev * head_size), f32),
            pltpu.SemaphoreType.DMA((row_count,)),
        ],
        compiler_params=pltpu.CompilerParams(vmem_limit_bytes=16 * 1024 * 1024),
        cost_estimate=pl.CostEstimate(flops=20_000_000, bytes_accessed=4_200_000, transcendentals=20_000),
    )(arrived, decay_rate[None, :], decay_bias[None, :], head_gain[None, :], old_state)


def body(
    residual_in,
    delta_state,
    norm_gain_first,
    gate_first,
    up_first,
    down_first,
    norm_gain_mixer,
    query_weight,
    key_weight,
    value_weight,
    output_gate_weight,
    beta_weight,
    decay_weight,
    decay_rate,
    decay_bias,
    head_gain,
    out_weight,
    norm_gain_second,
    gate_second,
    up_second,
    down_second,
):
    planes, tp_count = lax.axis_size("z"), lax.axis_size(TP)
    heads_dev = decay_rate.shape[0]

    def scaled_rows(gain, weights):
        return (jnp.concatenate(weights, axis=1).astype(f32) * gain[:, None]).astype(bf16)

    def gathered(weights):
        return lax.all_gather(jnp.concatenate(weights, axis=1), "z", axis=0, tiled=True)

    head_start = lax.axis_index(TP) * heads_dev
    gate_cols = [
        lax.dynamic_slice_in_dim(beta_weight, head_start, heads_dev, 1),
        lax.dynamic_slice_in_dim(decay_weight, head_start, heads_dev, 1),
        jnp.zeros((beta_weight.shape[0], GATES - 2 * heads_dev), bf16),
    ]
    first_in = scaled_rows(norm_gain_first, [gate_first, up_first])
    first_in, query_weight, gate_cols[0], gate_cols[1], down_first = lax.optimization_barrier(
        (first_in, query_weight, gate_cols[0], gate_cols[1], down_first)
    )
    mixer_in = scaled_rows(
        norm_gain_mixer, [query_weight, key_weight, value_weight, output_gate_weight, *gate_cols]
    )
    first_blocks = around(first_in, "z")
    first_blocks[1], first_blocks[-1], norm_gain_second, out_weight = lax.optimization_barrier(
        (first_blocks[1], first_blocks[-1], norm_gain_second, out_weight)
    )
    second_in = scaled_rows(norm_gain_second, [gate_second, up_second])
    width, mixer_width = first_in.shape[1], mixer_in.shape[1]
    middle = jnp.concatenate([mixer_in, down_first.T], axis=1)
    middle = gathered([middle])
    mixer_in, down_first = middle[:, :mixer_width], middle[:, mixer_width:]
    last = gathered([out_weight.T, second_in, down_second.T])
    values_width = out_weight.shape[0]
    out_rows, second_in, down_second = (
        last[:, :values_width],
        last[:, values_width : values_width + width],
        last[:, values_width + width :],
    )

    columns = residual_in.T
    own_cols, rows = columns.shape[0], columns.shape[1] // planes
    pieces = jnp.moveaxis(columns.reshape(own_cols, planes, rows), 1, 0)
    pieces = jnp.broadcast_to(pieces[:, None], (planes, tp_count, own_cols, rows))
    arrived = exchange(pieces.reshape(-1, own_cols, rows), ACROSS)
    arrived = arrived.reshape(planes, -1, rows)
    arrived, first_blocks[2], first_blocks[-2] = lax.optimization_barrier(
        (arrived, first_blocks[2], first_blocks[-2])
    )
    residual = arrived.reshape(-1, rows).T
    twice = jnp.concatenate([arrived, arrived], axis=0)
    ahead = lax.dynamic_slice_in_dim(twice, lax.axis_index("z"), planes, 0)
    products = [
        lax.dot_general(ahead[o], first_blocks[o], (((0,), (0,)), ((), ())), preferred_element_type=f32)
        for step in range(planes // 2 + 1)
        for o in sorted({step, (planes - step) % planes})
    ]
    partial_value = products[0]
    for product in products[1:]:
        partial_value = partial_value + product

    hidden = hidden_units(residual, partial_value)
    projected = times_transposed(hidden, down_first).astype(bf16)
    after_first = (residual.astype(f32) + 0.5 * everyone_sum(projected, TP)).astype(bf16)

    normed, new_state = mixer_values(
        after_first, mixer_in, decay_rate, decay_bias, head_gain, delta_state
    )
    normed = exchange(normed, "y").reshape(rows, -1)
    projected = times_transposed(normed, out_rows).astype(bf16)
    after_mixer = (after_first.astype(f32) + everyone_sum(projected, TP)).astype(bf16)

    hidden = hidden_units(after_mixer, jnp.dot(after_mixer, second_in, preferred_element_type=f32))
    projected = times_transposed(down_second, hidden).astype(bf16)
    pieces = jnp.concatenate([projected, after_mixer.T], axis=1)
    arrived = exchange(pieces.reshape(-1, own_cols, 2 * rows), ACROSS)
    arrived = arrived.reshape(planes, tp_count, own_cols, 2 * rows).astype(f32)
    final = arrived[:, 0, :, rows:] + 0.5 * arrived[..., :rows].sum(axis=1)
    residual_out = jnp.moveaxis(final, 1, 2).reshape(planes * rows, own_cols).astype(bf16)
    return (residual_out, new_state)


def solution(mesh):
    cut = Mesh(mesh.devices.reshape(8, 4, 4, 2), ("z", "y", "x", "c"))
    kv, tp = ("z", "y"), ("x", "c")
    wide, tall = P(kv, tp), P(tp, kv)
    placed = (
        P(None, kv + tp),
        P(kv, tp, None, None),
        P(kv),
        wide,
        wide,
        tall,
        P(kv),
        wide,
        wide,
        wide,
        wide,
        P(kv, None),
        P(kv, None),
        P(tp),
        P(tp),
        P(),
        tall,
        P(kv),
        wide,
        wide,
        tall,
    )

    return jax.shard_map(
        body,
        mesh=cut,
        in_specs=placed,
        out_specs=(P(None, kv + tp), P(kv, tp, None, None)),
        check_vma=False,
    )
```

profile of v0, /device:TPU:1, one launch (start us, length us, event | category | flops | bytes accessed | tf_op | source)
XLA Modules:
  0.0 162.5 jit_solution(10236831994402487837)
XLA Ops:
  7.3 0.8 constant_dynamic-slice_fusion
  8.0 1.0 multiply_convert_fusion.2
  9.1 0.1 copy.51
  9.2 0.1 copy.52
  9.3 1.0 concatenate.51
  10.3 0.8 multiply_convert_fusion
  11.1 1.6 %pad_maximum_fusion.1 = bf16[64,2368]{1,0:T(8,128)(2,1)} fusion(bf16[64,704]{1,0:T(8,128)(2,1)} %bitcast.102, bf16[64,1664]{1,0:T(8,128)(2,1)S(1)} %multiply_convert_fusion), kind=kLoop, calls=%fused_computation.24 | loop fusion | flops 606208 | bytes 606208 | tf_op jit(solution)/shard_map/concatenate | solution.py:218
  12.7 6.5 %collective-permute-start = (bf16[64,1408]{1,0:T(8,128)(2,1)S(1)}, bf16[64,1408]{1,0:T(8,128)(2,1)S(1)}, u32[]{:S(2)}, u32[]{:S(2)}) collective-permute-start(bf16[64,1408]{1,0:T(8,128)(2,1)S(1)} %multiply_convert_fusion.2), channel_id=1, source_target_pairs={{0,224},{32,0},{64,32},{96,64},{128,96},{160,128},{192,160},{224,1... | collective-permute-start | bytes 540680 | tf_op jit(solution)/shard_map/ppermute | solution.py:66
  19.2 0.8 reshape.68
  20.0 0.7 reshape.78
  20.8 8.6 %all-to-all-start = ((bf16[64,2,128]{2,1,0:T(2,128)(2,1)}), bf16[64,2,128]{2,1,0:T(2,128)(2,1)S(1)}, u32[]{:S(2)}, u32[]{:S(2)}) async-start(bf16[64,2,128]{2,1,0:T(2,128)(2,1)} %reshape.78), calls=%async_computation | async-start | bytes 65536 | tf_op jit(solution)/shard_map/all_to_all | solution.py:24
  29.4 9.7 %all-to-all-done = bf16[64,2,128]{2,1,0:T(2,128)(2,1)S(1)} async-done(((bf16[64,2,128]{2,1,0:T(2,128)(2,1)}), bf16[64,2,128]{2,1,0:T(2,128)(2,1)S(1)}, u32[]{:S(2)}, u32[]{:S(2)}) %all-to-all-start) | async-done | bytes 32800 | tf_op jit(solution)/shard_map/all_to_all | solution.py:24
  39.1 0.1 reshape.79
  39.3 0.2 collective-permute-start.2
  39.5 1.3 collective-permute-start.3
  40.8 0.1 multiply_convert_fusion.1
  41.0 0.8 pad_maximum_fusion
  41.8 6.9 %collective-permute-done.2 = bf16[64,1408]{1,0:T(8,128)(2,1)S(1)} collective-permute-done((bf16[64,1408]{1,0:T(8,128)(2,1)S(1)}, bf16[64,1408]{1,0:T(8,128)(2,1)S(1)}, u32[]{:S(2)}, u32[]{:S(2)}) %collective-permute-start.2) | collective-permute-done | bytes 180256 | tf_op jit(solution)/shard_map/ppermute | solution.py:66
  48.7 1.8 %collective-permute-done.3 = bf16[64,1408]{1,0:T(8,128)(2,1)S(1)} collective-permute-done((bf16[64,1408]{1,0:T(8,128)(2,1)S(1)}, bf16[64,1408]{1,0:T(8,128)(2,1)S(1)}, u32[]{:S(2)}, u32[]{:S(2)}) %collective-permute-start.3) | collective-permute-done | bytes 180256 | tf_op jit(solution)/shard_map/ppermute | solution.py:65
  50.5 0.1 fusion.14
  50.6 0.2 fusion.47
  50.8 0.2 fusion.46
  51.0 0.1 copy.55
  51.1 0.1 fusion.24
  51.2 0.2 convolution_add_fusion.3
  51.5 0.2 convolution_add_fusion.2
  51.7 0.5 collective-permute-start.5
  52.2 2.2 %collective-permute-start.4 = (bf16[64,1408]{1,0:T(8,128)(2,1)S(1)}, bf16[64,1408]{1,0:T(8,128)(2,1)S(1)}, u32[]{:S(2)}, u32[]{:S(2)}) collective-permute-start(bf16[64,1408]{1,0:T(8,128)(2,1)S(1)} %collective-permute-done.2), channel_id=1, source_target_pairs={{0,224},{32,0},{64,32},{96,64},{128,96},{160,128},{192,160},{224,1... | collective-permute-start | bytes 540680 | tf_op jit(solution)/shard_map/ppermute | solution.py:66
  54.4 0.2 fusion.2
  54.7 7.5 %collective-permute-done.5 = bf16[64,1408]{1,0:T(8,128)(2,1)S(1)} collective-permute-done((bf16[64,1408]{1,0:T(8,128)(2,1)S(1)}, bf16[64,1408]{1,0:T(8,128)(2,1)S(1)}, u32[]{:S(2)}, u32[]{:S(2)}) %collective-permute-start.5) | collective-permute-done | bytes 180256 | tf_op jit(solution)/shard_map/ppermute | solution.py:65
  62.2 0.1 collective-permute-start.6
  62.3 0.1 slice.135
  62.4 2.7 %collective-permute-start.7 = (bf16[64,704]{1,0:T(8,128)(2,1)S(1)}, bf16[64,704]{1,0:T(8,128)(2,1)S(1)}, u32[]{:S(2)}, u32[]{:S(2)}) collective-permute-start(bf16[64,704]{1,0:T(8,128)(2,1)S(1)} %slice.135), channel_id=1, source_target_pairs={{0,224},{32,0},{64,32},{96,64},{128,96},{160,128},{192,160},{224,1... | collective-permute-start | bytes 270344 | tf_op jit(solution)/shard_map/ppermute | solution.py:69
  65.2 0.2 fusion.45
  65.4 1.6 %collective-permute-done.6 = bf16[64,704]{1,0:T(8,128)(2,1)S(1)} collective-permute-done((bf16[64,704]{1,0:T(8,128)(2,1)S(1)}, bf16[64,704]{1,0:T(8,128)(2,1)S(1)}, u32[]{:S(2)}, u32[]{:S(2)}) %collective-permute-start.6) | collective-permute-done | bytes 90144 | tf_op jit(solution)/shard_map/ppermute | solution.py:68
  67.0 0.2 fusion.10
  67.2 0.2 fusion.3
  67.5 2.9 %collective-permute-start.10 = (bf16[32,1536]{1,0:T(8,128)(2,1)S(1)}, bf16[32,1536]{1,0:T(8,128)(2,1)S(1)}, u32[]{:S(2)}, u32[]{:S(2)}) collective-permute-start(bf16[32,1536]{1,0:T(8,128)(2,1)S(1)} %pad_maximum_fusion.3), channel_id=1, source_target_pairs={{0,24},{8,0},{16,8},{24,16},{1,25},{9,1},{17,9},{25,17},{2,26},{10... | collective-permute-start | bytes 294920 | tf_op jit(solution)/shard_map/ppermute | solution.py:39
  70.3 1.8 %collective-permute-start.9 = (bf16[32,1536]{1,0:T(8,128)(2,1)S(1)}, bf16[32,1536]{1,0:T(8,128)(2,1)S(1)}, u32[]{:S(2)}, u32[]{:S(2)}) collective-permute-start(bf16[32,1536]{1,0:T(8,128)(2,1)S(1)} %pad_maximum_fusion.3), channel_id=1, source_target_pairs={{0,16},{8,24},{16,0},{24,8},{1,17},{9,25},{17,1},{25,9},{2,18},{10... | collective-permute-start | bytes 294920 | tf_op jit(solution)/shard_map/ppermute | solution.py:39
  72.1 3.9 %collective-permute-done.8 = bf16[32,1536]{1,0:T(8,128)(2,1)S(1)} collective-permute-done((bf16[32,1536]{1,0:T(8,128)(2,1)S(1)}, bf16[32,1536]{1,0:T(8,128)(2,1)S(1)}, u32[]{:S(2)}, u32[]{:S(2)}) %collective-permute-start.8) | collective-permute-done | bytes 98336 | tf_op jit(solution)/shard_map/ppermute | solution.py:39
  76.1 0.2 fusion.44
  76.4 1.6 %convolution_convert_fusion.2 = bf16[32,512]{1,0:T(8,128)(2,1)S(1)} fusion(bf16[512,2368]{1,0:T(8,128)(2,1)} %all-gather.5.cloned.1.call-done, f32[32,1536]{1,0:T(8,128)S(1)} %convert_add_fusion.1, f32[32]{0:T(128)S(1)} %fusion.44), kind=kOutput, calls=%fused_computation.13 | convolution fusion | flops 23265280 | bytes 1015936 | tf_op jit(solution)/shard_map/dot_general | solution.py:44
  78.0 14.1 %all_to_all.30 = bf16[8,32,512]{2,1,0:T(8,128)(2,1)S(1)} all-to-all(bf16[8,32,512]{2,1,0:T(8,128)(2,1)S(1)} %broadcast_in_dim.77), channel_id=1, replica_groups=mesh['z'=8,'y'=4,'x'=4,'c'=2] {'x','c'}, dimensions={0} | all-to-all | bytes 524288 | tf_op jit(solution)/shard_map/all_to_all | solution.py:24
  92.2 0.1 fusion.20
  92.4 1.9 %fusion.4 = f32[32,1664]{1,0:T(8,128)S(1)} fusion(bf16[32,512]{1,0:T(8,128)(2,1)S(1)} %get-tuple-element.31, bf16[512,2368]{1,0:T(8,128)(2,1)} %all-gather.5.cloned.1.call-done), kind=kOutput, calls=%fused_computation.9 | convolution fusion | flops 54525952 | bytes 1949696 | tf_op jit(solution)/shard_map/dot_general | solution.py:142
  94.4 8.0 %all_to_all.31.arrived_ref = bf16[4,8,1664]{2,1,0:T(8,128)(2,1)S(1)} all-to-all(bf16[4,8,1664]{2,1,0:T(8,128)(2,1)S(1)} %pad_maximum_fusion.2), channel_id=1, replica_groups=mesh['z'=8,'y'=4,'x'=4,'c'=2] {'y'}, dimensions={0} | all-to-all | bytes 212992 | tf_op jit(solution)/shard_map/all_to_all | solution.py:24
  102.5 2.2 %shard_map.212 = (bf16[4,8,512]{2,1,0:T(8,128)(2,1)S(1)}, f32[8,4,128,128]{3,2,1,0:T(8,128)}) custom-call(bf16[4,8,1664]{2,1,0:T(8,128)(2,1)S(1)} %all_to_all.31.arrived_ref, f32[1,4]{1,0:T(1,128)S(1)} %bitcast.95, f32[1,4]{1,0:T(1,128)S(1)} %bitcast.96, f32[1,128]{1,0:T(1,128)S(1)} %bitcast.97, f32[8,4,128,128]{3,2,1,0:T(8,128)S(1)} %copy-done), custom_call_target="tpu_custom_call" | custom-call | flops 20000000 | bytes 4200000 | tf_op jit(solution)/shard_map/pallas_call | solution.py:149
  104.7 6.7 %all_to_all.32 = bf16[4,8,512]{2,1,0:T(8,128)(2,1)S(1)} all-to-all(bf16[4,8,512]{2,1,0:T(8,128)(2,1)S(1)} %get-tuple-element.28), channel_id=1, replica_groups=mesh['z'=8,'y'=4,'x'=4,'c'=2] {'y'}, dimensions={0} | all-to-all | bytes 65536 | tf_op jit(solution)/shard_map/all_to_all | solution.py:24
  111.4 1.3 convolution_convert_fusion.3
  112.7 12.4 %all_to_all.33 = bf16[8,32,512]{2,1,0:T(8,128)(2,1)S(1)} all-to-all(bf16[8,32,512]{2,1,0:T(8,128)(2,1)S(1)} %broadcast_in_dim.83), channel_id=1, replica_groups=mesh['z'=8,'y'=4,'x'=4,'c'=2] {'x','c'}, dimensions={0} | all-to-all | bytes 524288 | tf_op jit(solution)/shard_map/all_to_all | solution.py:24
  125.1 0.1 multiply_reduce_fusion
  125.4 1.7 %convolution_convert_fusion = bf16[32,1408]{1,0:T(8,128)(2,1)S(1)} fusion(bf16[512,2624]{1,0:T(8,128)(2,1)} %all-gather.3.cloned.1.call-done, f32[32,512]{1,0:T(8,128)S(1)} %convert_reduce_fusion, bf16[32,512]{1,0:T(8,128)(2,1)S(1)} %get-tuple-element.31), kind=kOutput, calls=%fused_computation.8 | convolution fusion | flops 46231552 | bytes 1630208 | tf_op jit(solution)/shard_map/dot_general | solution.py:261
  127.1 0.4 collective-permute-start.11
  127.5 1.8 %collective-permute-start.12 = (bf16[32,1536]{1,0:T(8,128)(2,1)S(1)}, bf16[32,1536]{1,0:T(8,128)(2,1)S(1)}, u32[]{:S(2)}, u32[]{:S(2)}) collective-permute-start(bf16[32,1536]{1,0:T(8,128)(2,1)S(1)} %pad_maximum_fusion.4), channel_id=1, source_target_pairs={{0,16},{8,24},{16,0},{24,8},{1,17},{9,25},{17,1},{25,9},{2,18},{10... | collective-permute-start | bytes 294920 | tf_op jit(solution)/shard_map/ppermute | solution.py:39
  129.2 0.8 collective-permute-start.13
  130.1 3.2 %collective-permute-done.11 = bf16[32,1536]{1,0:T(8,128)(2,1)S(1)} collective-permute-done((bf16[32,1536]{1,0:T(8,128)(2,1)S(1)}, bf16[32,1536]{1,0:T(8,128)(2,1)S(1)}, u32[]{:S(2)}, u32[]{:S(2)}) %collective-permute-start.11) | collective-permute-done | bytes 98336 | tf_op jit(solution)/shard_map/ppermute | solution.py:39
  133.3 0.9 collective-permute-done.13
  134.3 0.2 fusion.39
  134.4 1.5 convolution_convert_fusion.1
  136.0 0.1 copy.53
  136.1 0.2 reshape.80
  136.2 18.4 %all_to_all.34 = bf16[64,2,256]{2,1,0:T(2,128)(2,1)S(1)} all-to-all(bf16[64,2,256]{2,1,0:T(2,128)(2,1)S(1)} %reshape.80), channel_id=1, replica_groups=mesh['z'=8,'y'=4,'x'=4,'c'=2] {'z','x','c'}, dimensions={0} | all-to-all | bytes 131072 | tf_op jit(solution)/shard_map/all_to_all | solution.py:24
  154.7 0.1 reshape.81
  155.0 0.7 convert_element_type.226
  (64 shorter events, 1.1 us)
Async XLA Ops:
  7.2 33.8 %copy-start.7 = (bf16[512,64]{0,1:T(8,128)(2,1)S(1)}, bf16[512,64]{0,1:T(8,128)(2,1)}, u32[]{:S(2)}) copy-start(bf16[512,64]{0,1:T(8,128)(2,1)} %param.37) | copy-start | bytes 196612
  7.2 33.6 %copy-start.8 = (f32[64]{0:T(128)S(1)}, f32[64]{0:T(128)}, u32[]{:S(2)}) copy-start(f32[64]{0:T(128)} %param.38) | copy-start | bytes 772
  7.2 33.6 %copy-start.5 = (bf16[64,704]{1,0:T(8,128)(2,1)S(1)}, bf16[64,704]{1,0:T(8,128)(2,1)}, u32[]{:S(2)}) copy-start(bf16[64,704]{1,0:T(8,128)(2,1)} %param.39) | copy-start | bytes 270340
  7.2 33.6 %copy-start.4 = (bf16[64,704]{1,0:T(8,128)(2,1)S(1)}, bf16[64,704]{1,0:T(8,128)(2,1)}, u32[]{:S(2)}) copy-start(bf16[64,704]{1,0:T(8,128)(2,1)} %param.40) | copy-start | bytes 270340
  7.2 33.7 %copy-start.6 = (bf16[704,64]{0,1:T(8,128)(2,1)S(1)}, bf16[704,64]{0,1:T(8,128)(2,1)}, u32[]{:S(2)}) copy-start(bf16[704,64]{0,1:T(8,128)(2,1)} %param.41) | copy-start | bytes 270340
  7.2 69.1 %all-gather.5.cloned.1.call-start = ((), (), s32[]{:S(2)}) async-start(), calls=%async_computation.7 | async-start | bytes 2801664 | tf_op jit(solution)/shard_map/all_gather | solution.py:197
  12.7 26.5 %collective-permute-start = (bf16[64,1408]{1,0:T(8,128)(2,1)S(1)}, bf16[64,1408]{1,0:T(8,128)(2,1)S(1)}, u32[]{:S(2)}, u32[]{:S(2)}) collective-permute-start(bf16[64,1408]{1,0:T(8,128)(2,1)S(1)} %multiply_convert_fusion.2), channel_id=1, source_target_pairs={{0,224},{32,0},{64,32},{96,64},{128,96},{160,128},{192,160},{224,1... | collective-permute-start | bytes 540680 | tf_op jit(solution)/shard_map/ppermute | solution.py:66
  19.2 20.1 %collective-permute-start.1 = (bf16[64,1408]{1,0:T(8,128)(2,1)S(1)}, bf16[64,1408]{1,0:T(8,128)(2,1)S(1)}, u32[]{:S(2)}, u32[]{:S(2)}) collective-permute-start(bf16[64,1408]{1,0:T(8,128)(2,1)S(1)} %multiply_convert_fusion.2), channel_id=1, source_target_pairs={{0,32},{32,64},{64,96},{96,128},{128,160},{160,192},{192,224},{224... | collective-permute-start | bytes 540680 | tf_op jit(solution)/shard_map/ppermute | solution.py:65
  20.8 18.4 %all-to-all-start = ((bf16[64,2,128]{2,1,0:T(2,128)(2,1)}), bf16[64,2,128]{2,1,0:T(2,128)(2,1)S(1)}, u32[]{:S(2)}, u32[]{:S(2)}) async-start(bf16[64,2,128]{2,1,0:T(2,128)(2,1)} %reshape.78), calls=%async_computation | async-start | bytes 65536 | tf_op jit(solution)/shard_map/all_to_all | solution.py:24
  29.4 82.0 %all-gather.3.cloned.1.call-start = ((), (), s32[]{:S(2)}) async-start(), calls=%async_computation.6 | async-start | bytes 3096576 | tf_op jit(solution)/shard_map/all_gather | solution.py:197
  39.3 9.4 %collective-permute-start.2 = (bf16[64,1408]{1,0:T(8,128)(2,1)S(1)}, bf16[64,1408]{1,0:T(8,128)(2,1)S(1)}, u32[]{:S(2)}, u32[]{:S(2)}) collective-permute-start(bf16[64,1408]{1,0:T(8,128)(2,1)S(1)} %collective-permute-done), channel_id=1, source_target_pairs={{0,224},{32,0},{64,32},{96,64},{128,96},{160,128},{192,160},{224,1... | collective-permute-start | bytes 540680 | tf_op jit(solution)/shard_map/ppermute | solution.py:66
  39.5 11.0 %collective-permute-start.3 = (bf16[64,1408]{1,0:T(8,128)(2,1)S(1)}, bf16[64,1408]{1,0:T(8,128)(2,1)S(1)}, u32[]{:S(2)}, u32[]{:S(2)}) collective-permute-start(bf16[64,1408]{1,0:T(8,128)(2,1)S(1)} %collective-permute-done.1), channel_id=1, source_target_pairs={{0,32},{32,64},{64,96},{96,128},{128,160},{160,192},{192,224},{224... | collective-permute-start | bytes 540680 | tf_op jit(solution)/shard_map/ppermute | solution.py:65
  51.7 10.5 %collective-permute-start.5 = (bf16[64,1408]{1,0:T(8,128)(2,1)S(1)}, bf16[64,1408]{1,0:T(8,128)(2,1)S(1)}, u32[]{:S(2)}, u32[]{:S(2)}) collective-permute-start(bf16[64,1408]{1,0:T(8,128)(2,1)S(1)} %collective-permute-done.3), channel_id=1, source_target_pairs={{0,32},{32,64},{64,96},{96,128},{128,160},{160,192},{192,224},{224... | collective-permute-start | bytes 540680 | tf_op jit(solution)/shard_map/ppermute | solution.py:65
  52.2 10.1 %collective-permute-start.4 = (bf16[64,1408]{1,0:T(8,128)(2,1)S(1)}, bf16[64,1408]{1,0:T(8,128)(2,1)S(1)}, u32[]{:S(2)}, u32[]{:S(2)}) collective-permute-start(bf16[64,1408]{1,0:T(8,128)(2,1)S(1)} %collective-permute-done.2), channel_id=1, source_target_pairs={{0,224},{32,0},{64,32},{96,64},{128,96},{160,128},{192,160},{224,1... | collective-permute-start | bytes 540680 | tf_op jit(solution)/shard_map/ppermute | solution.py:66
  62.2 4.8 %collective-permute-start.6 = (bf16[64,704]{1,0:T(8,128)(2,1)S(1)}, bf16[64,704]{1,0:T(8,128)(2,1)S(1)}, u32[]{:S(2)}, u32[]{:S(2)}) collective-permute-start(bf16[64,704]{1,0:T(8,128)(2,1)S(1)} %slice.134), channel_id=1, source_target_pairs={{0,32},{32,64},{64,96},{96,128},{128,160},{160,192},{192,224},{224... | collective-permute-start | bytes 270344 | tf_op jit(solution)/shard_map/ppermute | solution.py:68
  62.4 4.6 %collective-permute-start.7 = (bf16[64,704]{1,0:T(8,128)(2,1)S(1)}, bf16[64,704]{1,0:T(8,128)(2,1)S(1)}, u32[]{:S(2)}, u32[]{:S(2)}) collective-permute-start(bf16[64,704]{1,0:T(8,128)(2,1)S(1)} %slice.135), channel_id=1, source_target_pairs={{0,224},{32,0},{64,32},{96,64},{128,96},{160,128},{192,160},{224,1... | collective-permute-start | bytes 270344 | tf_op jit(solution)/shard_map/ppermute | solution.py:69
  67.5 4.7 %collective-permute-start.10 = (bf16[32,1536]{1,0:T(8,128)(2,1)S(1)}, bf16[32,1536]{1,0:T(8,128)(2,1)S(1)}, u32[]{:S(2)}, u32[]{:S(2)}) collective-permute-start(bf16[32,1536]{1,0:T(8,128)(2,1)S(1)} %pad_maximum_fusion.3), channel_id=1, source_target_pairs={{0,24},{8,0},{16,8},{24,16},{1,25},{9,1},{17,9},{25,17},{2,26},{10... | collective-permute-start | bytes 294920 | tf_op jit(solution)/shard_map/ppermute | solution.py:39
  70.3 5.7 %collective-permute-start.8 = (bf16[32,1536]{1,0:T(8,128)(2,1)S(1)}, bf16[32,1536]{1,0:T(8,128)(2,1)S(1)}, u32[]{:S(2)}, u32[]{:S(2)}) collective-permute-start(bf16[32,1536]{1,0:T(8,128)(2,1)S(1)} %pad_maximum_fusion.3), channel_id=1, source_target_pairs={{0,8},{8,16},{16,24},{24,0},{1,9},{9,17},{17,25},{25,1},{2,10},{10... | collective-permute-start | bytes 294920 | tf_op jit(solution)/shard_map/ppermute | solution.py:39
  70.3 5.7 %collective-permute-start.9 = (bf16[32,1536]{1,0:T(8,128)(2,1)S(1)}, bf16[32,1536]{1,0:T(8,128)(2,1)S(1)}, u32[]{:S(2)}, u32[]{:S(2)}) collective-permute-start(bf16[32,1536]{1,0:T(8,128)(2,1)S(1)} %pad_maximum_fusion.3), channel_id=1, source_target_pairs={{0,16},{8,24},{16,0},{24,8},{1,17},{9,25},{17,1},{25,9},{2,18},{10... | collective-permute-start | bytes 294920 | tf_op jit(solution)/shard_map/ppermute | solution.py:39
  76.3 26.2 %copy-start = (f32[8,4,128,128]{3,2,1,0:T(8,128)S(1)}, f32[8,4,128,128]{3,2,1,0:T(8,128)}, u32[]{:S(2)}) copy-start(f32[8,4,128,128]{3,2,1,0:T(8,128)} %state_ref.1) | copy-start | bytes 6291460
  76.3 26.2 %copy-start.1 = (f32[4]{0:T(128)S(1)}, f32[4]{0:T(128)}, u32[]{:S(2)}) copy-start(f32[4]{0:T(128)} %param.34) | copy-start | bytes 52
  76.3 26.1 %copy-start.2 = (f32[4]{0:T(128)S(1)}, f32[4]{0:T(128)}, u32[]{:S(2)}) copy-start(f32[4]{0:T(128)} %param.35) | copy-start | bytes 52
  76.3 26.1 %copy-start.3 = (f32[128]{0:T(128)S(1)}, f32[128]{0:T(128)}, u32[]{:S(2)}) copy-start(f32[128]{0:T(128)} %param.36) | copy-start | bytes 1540
  127.1 6.2 %collective-permute-start.11 = (bf16[32,1536]{1,0:T(8,128)(2,1)S(1)}, bf16[32,1536]{1,0:T(8,128)(2,1)S(1)}, u32[]{:S(2)}, u32[]{:S(2)}) collective-permute-start(bf16[32,1536]{1,0:T(8,128)(2,1)S(1)} %pad_maximum_fusion.4), channel_id=1, source_target_pairs={{0,8},{8,16},{16,24},{24,0},{1,9},{9,17},{17,25},{25,1},{2,10},{10... | collective-permute-start | bytes 294920 | tf_op jit(solution)/shard_map/ppermute | solution.py:39
  127.5 5.8 %collective-permute-start.12 = (bf16[32,1536]{1,0:T(8,128)(2,1)S(1)}, bf16[32,1536]{1,0:T(8,128)(2,1)S(1)}, u32[]{:S(2)}, u32[]{:S(2)}) collective-permute-start(bf16[32,1536]{1,0:T(8,128)(2,1)S(1)} %pad_maximum_fusion.4), channel_id=1, source_target_pairs={{0,16},{8,24},{16,0},{24,8},{1,17},{9,25},{17,1},{25,9},{2,18},{10... | collective-permute-start | bytes 294920 | tf_op jit(solution)/shard_map/ppermute | solution.py:39
  129.2 5.0 %collective-permute-start.13 = (bf16[32,1536]{1,0:T(8,128)(2,1)S(1)}, bf16[32,1536]{1,0:T(8,128)(2,1)S(1)}, u32[]{:S(2)}, u32[]{:S(2)}) collective-permute-start(bf16[32,1536]{1,0:T(8,128)(2,1)S(1)} %pad_maximum_fusion.4), channel_id=1, source_target_pairs={{0,24},{8,0},{16,8},{24,16},{1,25},{9,1},{17,9},{25,17},{2,26},{10... | collective-permute-start | bytes 294920 | tf_op jit(solution)/shard_map/ppermute | solution.py:39
Sparse Core Ops, SparseCore 0:
  12.9 49.9 all-gather.4
  64.7 41.6 all-gather.2
where the time goes:
time: 163 us; the launch traced here: 162 us
  blocking collectives  59.6 us (37%)
  waiting for transfers between devices  35.7 us (22%)
  starting transfers between devices  29.9 us (18%)
  between operations  14.5 us (9%)
  matrix products  9.6 us (6%)
  other arithmetic  5.89 us (4%)
  local copies, waits for them, and re-layouts  5.16 us (3%)
  Pallas kernels  2.23 us (1%)
    all_to_all x5, blocking collectives, exchange(): return lax.all_to_all(blocks, axis, split_axis=0, concat_axis=0, tiled=True)  59.6 us
    all_to_all x1, waiting for transfers between devices, exchange(): return lax.all_to_all(blocks, axis, split_axis=0, concat_axis=0, tiled=True)  9.7 us
    ppermute x3, waiting for transfers between devices, around(): forward = blocks[size - step] = lax.ppermute(forward, axis, ahead)  9.31 us
    ppermute x3, starting transfers between devices, around(): backward = blocks[step] = lax.ppermute(backward, axis, behind)  8.93 us
    all_to_all x1, starting transfers between devices, exchange(): return lax.all_to_all(blocks, axis, split_axis=0, concat_axis=0, tiled=True)  8.6 us
    ppermute x6, waiting for transfers between devices, ring_sum(): lax.ppermute(value, axis, [(i, (i + places) % size) for i in range(size)])  8.05 us
    ppermute x6, starting transfers between devices, ring_sum(): lax.ppermute(value, axis, [(i, (i + places) % size) for i in range(size)])  7.61 us
    ppermute x3, waiting for transfers between devices, around(): backward = blocks[step] = lax.ppermute(backward, axis, behind)  6.93 us
  transfers between devices with their start and end apart: 17, of which 8 were waited for; matrix products, arithmetic and copies ran while one was open for 5% of the time, Pallas kernels for 1%

commit v1 on v0

--- a/solution.py
+++ b/solution.py
@@ -64,7 +64,7 @@
     for step in range(1, size // 2):
         forward = blocks[size - step] = lax.ppermute(forward, axis, ahead)
         backward = blocks[step] = lax.ppermute(backward, axis, behind)
-    half = block.shape[1] // 2
+    half = block.shape[1] // 256 * 128
     forward = lax.ppermute(forward[:, :half], axis, ahead)
     backward = lax.ppermute(backward[:, half:], axis, behind)
     blocks[size // 2] = jnp.concatenate([forward, backward], axis=1)
@@ -203,28 +203,22 @@
         jnp.zeros((beta_weight.shape[0], GATES - 2 * heads_dev), bf16),
     ]
     first_in = scaled_rows(norm_gain_first, [gate_first, up_first])
-    first_in, query_weight, gate_cols[0], gate_cols[1], down_first = lax.optimization_barrier(
-        (first_in, query_weight, gate_cols[0], gate_cols[1], down_first)
-    )
+    width = first_in.shape[1]
+    first_blocks = around(jnp.concatenate([first_in, down_first.T], axis=1), "z")
     mixer_in = scaled_rows(
         norm_gain_mixer, [query_weight, key_weight, value_weight, output_gate_weight, *gate_cols]
     )
-    first_blocks = around(first_in, "z")
-    first_blocks[1], first_blocks[-1], norm_gain_second, out_weight = lax.optimization_barrier(
-        (first_blocks[1], first_blocks[-1], norm_gain_second, out_weight)
-    )
     second_in = scaled_rows(norm_gain_second, [gate_second, up_second])
-    width, mixer_width = first_in.shape[1], mixer_in.shape[1]
-    middle = jnp.concatenate([mixer_in, down_first.T], axis=1)
+    mixer_width = mixer_in.shape[1]
+    middle = jnp.concatenate([mixer_in, out_weight.T], axis=1)
+    last = jnp.concatenate([second_in, down_second.T], axis=1)
+    first_blocks[2], first_blocks[-2], middle, last = lax.optimization_barrier(
+        (first_blocks[2], first_blocks[-2], middle, last)
+    )
     middle = gathered([middle])
-    mixer_in, down_first = middle[:, :mixer_width], middle[:, mixer_width:]
-    last = gathered([out_weight.T, second_in, down_second.T])
-    values_width = out_weight.shape[0]
-    out_rows, second_in, down_second = (
-        last[:, :values_width],
-        last[:, values_width : values_width + width],
-        last[:, values_width + width :],
-    )
+    last = gathered([last])
+    mixer_in, out_rows = middle[:, :mixer_width], middle[:, mixer_width:]
+    second_in, down_second = last[:, :width], last[:, width:]
 
     columns = residual_in.T
     own_cols, rows = columns.shape[0], columns.shape[1] // planes
@@ -232,14 +226,20 @@
     pieces = jnp.broadcast_to(pieces[:, None], (planes, tp_count, own_cols, rows))
     arrived = exchange(pieces.reshape(-1, own_cols, rows), ACROSS)
     arrived = arrived.reshape(planes, -1, rows)
-    arrived, first_blocks[2], first_blocks[-2] = lax.optimization_barrier(
-        (arrived, first_blocks[2], first_blocks[-2])
+    arrived, first_blocks[3], first_blocks[-3] = lax.optimization_barrier(
+        (arrived, first_blocks[3], first_blocks[-3])
     )
     residual = arrived.reshape(-1, rows).T
+    across = planes * own_cols * tp_count
+    block_size = own_cols * tp_count
+    to = lax.broadcasted_iota(jnp.int32, (across, across), 1)
+    at = lax.broadcasted_iota(jnp.int32, (across, across), 0)
+    turned = lax.rem(to + (planes - lax.axis_index("z")) * block_size, across)
+    order = (at == turned).astype(bf16)
     twice = jnp.concatenate([arrived, arrived], axis=0)
     ahead = lax.dynamic_slice_in_dim(twice, lax.axis_index("z"), planes, 0)
     products = [
-        lax.dot_general(ahead[o], first_blocks[o], (((0,), (0,)), ((), ())), preferred_element_type=f32)
+        lax.dot_general(ahead[o], first_blocks[o][:, :width], (((0,), (0,)), ((), ())), preferred_element_type=f32)
         for step in range(planes // 2 + 1)
         for o in sorted({step, (planes - step) % planes})
     ]
@@ -248,7 +248,9 @@
         partial_value = partial_value + product
 
     hidden = hidden_units(residual, partial_value)
+    down_first = jnp.concatenate([block[:, width:] for block in first_blocks], axis=0)
     projected = times_transposed(hidden, down_first).astype(bf16)
+    projected = jnp.dot(projected, order, preferred_element_type=f32).astype(bf16)
     after_first = (residual.astype(f32) + 0.5 * everyone_sum(projected, TP)).astype(bf16)
 
     normed, new_state = mixer_values(

time: 163 us -> 169 us (1.037)
  waiting for transfers between devices: 35.7 us -> 44.8 us
  blocking collectives: 59.6 us -> 57.7 us
    ppermute x3, waiting for transfers between devices: 6.93 us -> 16.7 us  [around(): backward = blocks[step] = lax.ppermute(backward, axis, behind)]
    ppermute x3, waiting for transfers between devices: 9.31 us -> 4.94 us  [around(): forward = blocks[size - step] = lax.ppermute(forward, axis, ahead)]
    ppermute x1, waiting for transfers between devices: 1.63 us -> 5.75 us  [around(): forward = lax.ppermute(forward[:, :half], axis, ahead)]
    ppermute x1, starting transfers between devices: 2.73 us -> 0.08 us  [around(): backward = lax.ppermute(backward[:, half:], axis, behind)]
    all_to_all x5, blocking collectives: 59.6 us -> 57.7 us  [exchange(): return lax.all_to_all(blocks, axis, split_axis=0, concat_axis=0, tiled=True)]
    dot_general x3 -> x2, matrix products: 4.4 us -> 2.76 us  [times_transposed(): lax.dot_general(left, right_rows, (((1,), (1,)), ((), ())), preferred_ele...]
  transfers between devices with their start and end apart: 17 -> 17, of which waited for: 8 -> 10; matrix products, arithmetic and copies ran while one was open for 5% -> 8% of each run, Pallas kernels for 1% -> 1%
where the time goes in v1:
time: 169 us
  blocking collectives  57.7 us (34%)
  waiting for transfers between devices  44.8 us (27%)
  starting transfers between devices  29.7 us (18%)
  between operations  14.5 us (9%)
  matrix products  8.46 us (5%)
  other arithmetic  6.85 us (4%)
  local copies, waits for them, and re-layouts  4.4 us (3%)
  Pallas kernels  2.23 us (1%)
    all_to_all x5, blocking collectives, exchange(): return lax.all_to_all(blocks, axis, split_axis=0, concat_axis=0, tiled=True)  57.7 us
    ppermute x3, waiting for transfers between devices, around(): backward = blocks[step] = lax.ppermute(backward, axis, behind)  16.7 us
    ppermute x3, starting transfers between devices, around(): backward = blocks[step] = lax.ppermute(backward, axis, behind)  10.2 us
    all_to_all x1, waiting for transfers between devices, exchange(): return lax.all_to_all(blocks, axis, split_axis=0, concat_axis=0, tiled=True)  9.29 us
    all_to_all x1, starting transfers between devices, exchange(): return lax.all_to_all(blocks, axis, split_axis=0, concat_axis=0, tiled=True)  8.75 us
    ppermute x6, waiting for transfers between devices, ring_sum(): lax.ppermute(value, axis, [(i, (i + places) % size) for i in range(size)])  8.15 us
    ppermute x6, starting transfers between devices, ring_sum(): lax.ppermute(value, axis, [(i, (i + places) % size) for i in range(size)])  7.81 us
    ppermute x1, waiting for transfers between devices, around(): forward = lax.ppermute(forward[:, :half], axis, ahead)  5.75 us
  transfers between devices with their start and end apart: 17, of which 10 were waited for; matrix products, arithmetic and copies ran while one was open for 8% of the time, Pallas kernels for 1%

profile of v1, /device:TPU:1, one launch (start us, length us, event | category | flops | bytes accessed | tf_op | source)
XLA Modules:
  0.0 168.6 jit_solution(12134180039084689457)
XLA Ops:
  7.3 1.1 multiply_convert_fusion.2
  8.4 0.9 pad_maximum_fusion
  9.3 6.5 %collective-permute-start = (bf16[64,2112]{1,0:T(8,128)(2,1)S(1)}, bf16[64,2112]{1,0:T(8,128)(2,1)S(1)}, u32[]{:S(2)}, u32[]{:S(2)}) collective-permute-start(bf16[64,2112]{1,0:T(8,128)(2,1)S(1)} %pad_maximum_fusion), channel_id=1, source_target_pairs={{0,224},{32,0},{64,32},{96,64},{128,96},{160,128},{192,160},{224,1... | collective-permute-start | bytes 811016 | tf_op jit(solution)/shard_map/ppermute | solution.py:66
  15.7 0.7 constant_dynamic-slice_fusion
  16.5 0.1 copy.41
  16.6 0.1 copy.42
  16.7 1.0 concatenate.53
  17.7 0.8 multiply_convert_fusion
  18.5 1.0 multiply_convert_fusion.1
  19.5 0.7 pad_maximum_fusion.1
  20.3 0.8 collective-permute-done
  21.1 3.4 %collective-permute-start.1 = (bf16[64,2112]{1,0:T(8,128)(2,1)S(1)}, bf16[64,2112]{1,0:T(8,128)(2,1)S(1)}, u32[]{:S(2)}, u32[]{:S(2)}) collective-permute-start(bf16[64,2112]{1,0:T(8,128)(2,1)S(1)} %collective-permute-done), channel_id=1, source_target_pairs={{0,224},{32,0},{64,32},{96,64},{128,96},{160,128},{192,160},{224,1... | collective-permute-start | bytes 811016 | tf_op jit(solution)/shard_map/ppermute | solution.py:66
  24.5 0.7 pad_maximum_fusion.2
  25.3 3.7 %collective-permute-done.1 = bf16[64,2112]{1,0:T(8,128)(2,1)S(1)} collective-permute-done((bf16[64,2112]{1,0:T(8,128)(2,1)S(1)}, bf16[64,2112]{1,0:T(8,128)(2,1)S(1)}, u32[]{:S(2)}, u32[]{:S(2)}) %collective-permute-start.1) | collective-permute-done | bytes 270368 | tf_op jit(solution)/shard_map/ppermute | solution.py:66
  29.0 3.1 %collective-permute-done.3 = bf16[64,2112]{1,0:T(8,128)(2,1)S(1)} collective-permute-done((bf16[64,2112]{1,0:T(8,128)(2,1)S(1)}, bf16[64,2112]{1,0:T(8,128)(2,1)S(1)}, u32[]{:S(2)}, u32[]{:S(2)}) %collective-permute-start.3) | collective-permute-done | bytes 270368 | tf_op jit(solution)/shard_map/ppermute | solution.py:65
  32.2 0.1 reshape.68
  32.3 0.7 reshape.78
  33.0 8.8 %all-to-all-start = ((bf16[64,2,128]{2,1,0:T(2,128)(2,1)}), bf16[64,2,128]{2,1,0:T(2,128)(2,1)S(1)}, u32[]{:S(2)}, u32[]{:S(2)}) async-start(bf16[64,2,128]{2,1,0:T(2,128)(2,1)} %reshape.78), calls=%async_computation | async-start | bytes 65536 | tf_op jit(solution)/shard_map/all_to_all | solution.py:24
  41.9 9.3 %all-to-all-done = bf16[64,2,128]{2,1,0:T(2,128)(2,1)S(1)} async-done(((bf16[64,2,128]{2,1,0:T(2,128)(2,1)}), bf16[64,2,128]{2,1,0:T(2,128)(2,1)S(1)}, u32[]{:S(2)}, u32[]{:S(2)}) %all-to-all-start) | async-done | bytes 32800 | tf_op jit(solution)/shard_map/all_to_all | solution.py:24
  51.2 0.1 reshape.79
  51.3 0.3 collective-permute-start.4
  51.6 1.3 collective-permute-start.5
  52.9 12.1 %collective-permute-done.4 = bf16[64,2112]{1,0:T(8,128)(2,1)S(1)} collective-permute-done((bf16[64,2112]{1,0:T(8,128)(2,1)S(1)}, bf16[64,2112]{1,0:T(8,128)(2,1)S(1)}, u32[]{:S(2)}, u32[]{:S(2)}) %collective-permute-start.4) | collective-permute-done | bytes 270368 | tf_op jit(solution)/shard_map/ppermute | solution.py:66
  65.0 1.8 %collective-permute-done.5 = bf16[64,2112]{1,0:T(8,128)(2,1)S(1)} collective-permute-done((bf16[64,2112]{1,0:T(8,128)(2,1)S(1)}, bf16[64,2112]{1,0:T(8,128)(2,1)S(1)}, u32[]{:S(2)}, u32[]{:S(2)}) %collective-permute-start.5) | collective-permute-done | bytes 270368 | tf_op jit(solution)/shard_map/ppermute | solution.py:65
  66.8 0.1 fusion.19
  66.9 0.1 copy.55
  67.0 0.1 fusion.29
  67.1 0.2 fusion.53
  67.3 0.2 convolution_add_fusion.6
  67.5 0.2 convolution_add_fusion.5
  67.8 0.2 convolution_add_fusion.4
  68.1 1.5 collective-permute-start.6
  69.6 0.2 convolution_add_fusion.3
  69.8 0.2 convolution_add_fusion.2
  70.0 0.2 convolution_add_fusion.1
  70.3 5.7 %collective-permute-done.6 = bf16[64,1024]{1,0:T(8,128)(2,1)S(1)} collective-permute-done((bf16[64,1024]{1,0:T(8,128)(2,1)S(1)}, bf16[64,1024]{1,0:T(8,128)(2,1)S(1)}, u32[]{:S(2)}, u32[]{:S(2)}) %collective-permute-start.6) | collective-permute-done | bytes 131104 | tf_op jit(solution)/shard_map/ppermute | solution.py:68
  76.1 0.2 fusion
  76.3 3.2 %collective-permute-start.10 = (bf16[32,1536]{1,0:T(8,128)(2,1)S(1)}, bf16[32,1536]{1,0:T(8,128)(2,1)S(1)}, u32[]{:S(2)}, u32[]{:S(2)}) collective-permute-start(bf16[32,1536]{1,0:T(8,128)(2,1)S(1)} %pad_maximum_fusion.6), channel_id=1, source_target_pairs={{0,24},{8,0},{16,8},{24,16},{1,25},{9,1},{17,9},{25,17},{2,26},{10... | collective-permute-start | bytes 294920 | tf_op jit(solution)/shard_map/ppermute | solution.py:39
  79.5 1.6 collective-permute-start.9
  81.2 4.0 %collective-permute-done.8 = bf16[32,1536]{1,0:T(8,128)(2,1)S(1)} collective-permute-done((bf16[32,1536]{1,0:T(8,128)(2,1)S(1)}, bf16[32,1536]{1,0:T(8,128)(2,1)S(1)}, u32[]{:S(2)}, u32[]{:S(2)}) %collective-permute-start.8) | collective-permute-done | bytes 98336 | tf_op jit(solution)/shard_map/ppermute | solution.py:39
  85.3 0.2 fusion.52
  85.5 0.5 convolution_convert_fusion.2
  86.1 13.0 %all_to_all.30 = bf16[8,32,512]{2,1,0:T(8,128)(2,1)S(1)} all-to-all(bf16[8,32,512]{2,1,0:T(8,128)(2,1)S(1)} %broadcast_in_dim.77), channel_id=1, replica_groups=mesh['z'=8,'y'=4,'x'=4,'c'=2] {'x','c'}, dimensions={0} | all-to-all | bytes 524288 | tf_op jit(solution)/shard_map/all_to_all | solution.py:24
  99.1 0.1 fusion.25
  99.4 1.9 %fusion.1 = f32[32,1664]{1,0:T(8,128)S(1)} fusion(bf16[32,512]{1,0:T(8,128)(2,1)S(1)} %get-tuple-element.21, bf16[512,2176]{1,0:T(8,128)(2,1)} %all-gather.5.cloned.1.call-done), kind=kOutput, calls=%fused_computation.9 | convolution fusion | flops 54525952 | bytes 1949696 | tf_op jit(solution)/shard_map/dot_general | solution.py:142
  101.4 8.0 %all_to_all.31.arrived_ref = bf16[4,8,1664]{2,1,0:T(8,128)(2,1)S(1)} all-to-all(bf16[4,8,1664]{2,1,0:T(8,128)(2,1)S(1)} %pad_maximum_fusion.5), channel_id=1, replica_groups=mesh['z'=8,'y'=4,'x'=4,'c'=2] {'y'}, dimensions={0} | all-to-all | bytes 212992 | tf_op jit(solution)/shard_map/all_to_all | solution.py:24
  109.5 2.2 %shard_map.212 = (bf16[4,8,512]{2,1,0:T(8,128)(2,1)S(1)}, f32[8,4,128,128]{3,2,1,0:T(8,128)}) custom-call(bf16[4,8,1664]{2,1,0:T(8,128)(2,1)S(1)} %all_to_all.31.arrived_ref, f32[1,4]{1,0:T(1,128)S(1)} %bitcast.91, f32[1,4]{1,0:T(1,128)S(1)} %bitcast.92, f32[1,128]{1,0:T(1,128)S(1)} %bitcast.93, f32[8,4,128,128]{3,2,1,0:T(8,128)S(1)} %copy-done), custom_call_target="tpu_custom_call" | custom-call | flops 20000000 | bytes 4200000 | tf_op jit(solution)/shard_map/pallas_call | solution.py:149
  111.7 6.7 %all_to_all.32 = bf16[4,8,512]{2,1,0:T(8,128)(2,1)S(1)} all-to-all(bf16[4,8,512]{2,1,0:T(8,128)(2,1)S(1)} %get-tuple-element.18), channel_id=1, replica_groups=mesh['z'=8,'y'=4,'x'=4,'c'=2] {'y'}, dimensions={0} | all-to-all | bytes 65536 | tf_op jit(solution)/shard_map/all_to_all | solution.py:24
  118.3 1.3 convolution_convert_fusion.4
  119.7 12.4 %all_to_all.33 = bf16[8,32,512]{2,1,0:T(8,128)(2,1)S(1)} all-to-all(bf16[8,32,512]{2,1,0:T(8,128)(2,1)S(1)} %broadcast_in_dim.83), channel_id=1, replica_groups=mesh['z'=8,'y'=4,'x'=4,'c'=2] {'x','c'}, dimensions={0} | all-to-all | bytes 524288 | tf_op jit(solution)/shard_map/all_to_all | solution.py:24
  132.2 0.1 multiply_reduce_fusion
  132.4 1.7 %convolution_convert_fusion = bf16[32,1408]{1,0:T(8,128)(2,1)S(1)} fusion(bf16[512,2112]{1,0:T(8,128)(2,1)} %all-gather.3.cloned.1.call-done, f32[32,512]{1,0:T(8,128)S(1)} %convert_reduce_fusion, bf16[32,512]{1,0:T(8,128)(2,1)S(1)} %get-tuple-element.21), kind=kOutput, calls=%fused_computation.8 | convolution fusion | flops 46231552 | bytes 1630208 | tf_op jit(solution)/shard_map/dot_general | solution.py:263
  134.1 0.4 collective-permute-start.11
  134.5 1.8 %collective-permute-start.12 = (bf16[32,1536]{1,0:T(8,128)(2,1)S(1)}, bf16[32,1536]{1,0:T(8,128)(2,1)S(1)}, u32[]{:S(2)}, u32[]{:S(2)}) collective-permute-start(bf16[32,1536]{1,0:T(8,128)(2,1)S(1)} %pad_maximum_fusion.7), channel_id=1, source_target_pairs={{0,16},{8,24},{16,0},{24,8},{1,17},{9,25},{17,1},{25,9},{2,18},{10... | collective-permute-start | bytes 294920 | tf_op jit(solution)/shard_map/ppermute | solution.py:39
  136.3 0.8 collective-permute-start.13
  137.1 3.2 %collective-permute-done.11 = bf16[32,1536]{1,0:T(8,128)(2,1)S(1)} collective-permute-done((bf16[32,1536]{1,0:T(8,128)(2,1)S(1)}, bf16[32,1536]{1,0:T(8,128)(2,1)S(1)}, u32[]{:S(2)}, u32[]{:S(2)}) %collective-permute-start.11) | collective-permute-done | bytes 98336 | tf_op jit(solution)/shard_map/ppermute | solution.py:39
  140.3 0.9 collective-permute-done.13
  141.3 0.2 fusion.47
  141.4 1.5 convolution_convert_fusion.1
  143.0 0.1 copy.53
  143.1 0.2 reshape.80
  143.2 17.5 %all_to_all.34 = bf16[64,2,256]{2,1,0:T(2,128)(2,1)S(1)} all-to-all(bf16[64,2,256]{2,1,0:T(2,128)(2,1)S(1)} %reshape.80), channel_id=1, replica_groups=mesh['z'=8,'y'=4,'x'=4,'c'=2] {'z','x','c'}, dimensions={0} | all-to-all | bytes 131072 | tf_op jit(solution)/shard_map/all_to_all | solution.py:24
  160.8 0.1 reshape.81
  161.1 0.7 convert_element_type.231
  (73 shorter events, 1.3 us)
Async XLA Ops:
  7.2 34.7 %copy-start.4 = (bf16[704,64]{0,1:T(8,128)(2,1)S(1)}, bf16[704,64]{0,1:T(8,128)(2,1)}, u32[]{:S(2)}) copy-start(bf16[704,64]{0,1:T(8,128)(2,1)} %param.26) | copy-start | bytes 270340
  7.2 12.3 %copy-start.6 = (bf16[512,64]{0,1:T(8,128)(2,1)S(1)}, bf16[512,64]{0,1:T(8,128)(2,1)}, u32[]{:S(2)}) copy-start(bf16[512,64]{0,1:T(8,128)(2,1)} %param.37) | copy-start | bytes 196612
  7.2 17.3 %copy-start.5 = (bf16[704,64]{0,1:T(8,128)(2,1)S(1)}, bf16[704,64]{0,1:T(8,128)(2,1)}, u32[]{:S(2)}) copy-start(bf16[704,64]{0,1:T(8,128)(2,1)} %param.41) | copy-start | bytes 270340
  7.2 24.9 %copy-start.7 = (bf16[256,8]{0,1:T(8,128)(2,1)S(1)}, bf16[256,8]{0,1:T(8,128)(2,1)}, u32[]{:S(2)}) copy-start(bf16[256,8]{0,1:T(8,128)(2,1)} %param.21) | copy-start | bytes 12292
  7.2 92.2 %all-gather.5.cloned.1.call-start = ((), (), s32[]{:S(2)}) async-start(), calls=%async_computation.7 | async-start | bytes 2506752 | tf_op jit(solution)/shard_map/all_gather | solution.py:197
  9.3 11.8 %collective-permute-start = (bf16[64,2112]{1,0:T(8,128)(2,1)S(1)}, bf16[64,2112]{1,0:T(8,128)(2,1)S(1)}, u32[]{:S(2)}, u32[]{:S(2)}) collective-permute-start(bf16[64,2112]{1,0:T(8,128)(2,1)S(1)} %pad_maximum_fusion), channel_id=1, source_target_pairs={{0,224},{32,0},{64,32},{96,64},{128,96},{160,128},{192,160},{224,1... | collective-permute-start | bytes 811016 | tf_op jit(solution)/shard_map/ppermute | solution.py:66
  15.7 8.8 %collective-permute-start.2 = (bf16[64,2112]{1,0:T(8,128)(2,1)S(1)}, bf16[64,2112]{1,0:T(8,128)(2,1)S(1)}, u32[]{:S(2)}, u32[]{:S(2)}) collective-permute-start(bf16[64,2112]{1,0:T(8,128)(2,1)S(1)} %pad_maximum_fusion), channel_id=1, source_target_pairs={{0,32},{32,64},{64,96},{96,128},{128,160},{160,192},{192,224},{224... | collective-permute-start | bytes 811016 | tf_op jit(solution)/shard_map/ppermute | solution.py:65
  21.1 7.9 %collective-permute-start.1 = (bf16[64,2112]{1,0:T(8,128)(2,1)S(1)}, bf16[64,2112]{1,0:T(8,128)(2,1)S(1)}, u32[]{:S(2)}, u32[]{:S(2)}) collective-permute-start(bf16[64,2112]{1,0:T(8,128)(2,1)S(1)} %collective-permute-done), channel_id=1, source_target_pairs={{0,224},{32,0},{64,32},{96,64},{128,96},{160,128},{192,160},{224,1... | collective-permute-start | bytes 811016 | tf_op jit(solution)/shard_map/ppermute | solution.py:66
  24.5 7.6 %collective-permute-start.3 = (bf16[64,2112]{1,0:T(8,128)(2,1)S(1)}, bf16[64,2112]{1,0:T(8,128)(2,1)S(1)}, u32[]{:S(2)}, u32[]{:S(2)}) collective-permute-start(bf16[64,2112]{1,0:T(8,128)(2,1)S(1)} %collective-permute-done.2), channel_id=1, source_target_pairs={{0,32},{32,64},{64,96},{96,128},{128,160},{160,192},{192,224},{224... | collective-permute-start | bytes 811016 | tf_op jit(solution)/shard_map/ppermute | solution.py:65
  33.0 18.2 %all-to-all-start = ((bf16[64,2,128]{2,1,0:T(2,128)(2,1)}), bf16[64,2,128]{2,1,0:T(2,128)(2,1)S(1)}, u32[]{:S(2)}, u32[]{:S(2)}) async-start(bf16[64,2,128]{2,1,0:T(2,128)(2,1)} %reshape.78), calls=%async_computation | async-start | bytes 65536 | tf_op jit(solution)/shard_map/all_to_all | solution.py:24
  41.8 90.6 %all-gather.3.cloned.1.call-start = ((), (), s32[]{:S(2)}) async-start(), calls=%async_computation.6 | async-start | bytes 2506752 | tf_op jit(solution)/shard_map/all_gather | solution.py:197
  51.3 13.7 %collective-permute-start.4 = (bf16[64,2112]{1,0:T(8,128)(2,1)S(1)}, bf16[64,2112]{1,0:T(8,128)(2,1)S(1)}, u32[]{:S(2)}, u32[]{:S(2)}) collective-permute-start(bf16[64,2112]{1,0:T(8,128)(2,1)S(1)} %collective-permute-done.1), channel_id=1, source_target_pairs={{0,224},{32,0},{64,32},{96,64},{128,96},{160,128},{192,160},{224,1... | collective-permute-start | bytes 811016 | tf_op jit(solution)/shard_map/ppermute | solution.py:66
  51.6 15.2 %collective-permute-start.5 = (bf16[64,2112]{1,0:T(8,128)(2,1)S(1)}, bf16[64,2112]{1,0:T(8,128)(2,1)S(1)}, u32[]{:S(2)}, u32[]{:S(2)}) collective-permute-start(bf16[64,2112]{1,0:T(8,128)(2,1)S(1)} %collective-permute-done.3), channel_id=1, source_target_pairs={{0,32},{32,64},{64,96},{96,128},{128,160},{160,192},{192,224},{224... | collective-permute-start | bytes 811016 | tf_op jit(solution)/shard_map/ppermute | solution.py:65
  68.0 8.1 %collective-permute-start.7 = (bf16[64,1088]{1,0:T(8,128)(2,1)S(1)}, bf16[64,1088]{1,0:T(8,128)(2,1)S(1)}, u32[]{:S(2)}, u32[]{:S(2)}) collective-permute-start(bf16[64,1088]{1,0:T(8,128)(2,1)S(1)} %slice.189), channel_id=1, source_target_pairs={{0,224},{32,0},{64,32},{96,64},{128,96},{160,128},{192,160},{224,1... | collective-permute-start | bytes 417800 | tf_op jit(solution)/shard_map/ppermute | solution.py:69
  68.1 8.0 %collective-permute-start.6 = (bf16[64,1024]{1,0:T(8,128)(2,1)S(1)}, bf16[64,1024]{1,0:T(8,128)(2,1)S(1)}, u32[]{:S(2)}, u32[]{:S(2)}) collective-permute-start(bf16[64,1024]{1,0:T(8,128)(2,1)S(1)} %slice.188), channel_id=1, source_target_pairs={{0,32},{32,64},{64,96},{96,128},{128,160},{160,192},{192,224},{224... | collective-permute-start | bytes 393224 | tf_op jit(solution)/shard_map/ppermute | solution.py:68
  76.3 4.9 %collective-permute-start.10 = (bf16[32,1536]{1,0:T(8,128)(2,1)S(1)}, bf16[32,1536]{1,0:T(8,128)(2,1)S(1)}, u32[]{:S(2)}, u32[]{:S(2)}) collective-permute-start(bf16[32,1536]{1,0:T(8,128)(2,1)S(1)} %pad_maximum_fusion.6), channel_id=1, source_target_pairs={{0,24},{8,0},{16,8},{24,16},{1,25},{9,1},{17,9},{25,17},{2,26},{10... | collective-permute-start | bytes 294920 | tf_op jit(solution)/shard_map/ppermute | solution.py:39
  79.5 5.7 %collective-permute-start.8 = (bf16[32,1536]{1,0:T(8,128)(2,1)S(1)}, bf16[32,1536]{1,0:T(8,128)(2,1)S(1)}, u32[]{:S(2)}, u32[]{:S(2)}) collective-permute-start(bf16[32,1536]{1,0:T(8,128)(2,1)S(1)} %pad_maximum_fusion.6), channel_id=1, source_target_pairs={{0,8},{8,16},{16,24},{24,0},{1,9},{9,17},{17,25},{25,1},{2,10},{10... | collective-permute-start | bytes 294920 | tf_op jit(solution)/shard_map/ppermute | solution.py:39
  79.5 5.7 %collective-permute-start.9 = (bf16[32,1536]{1,0:T(8,128)(2,1)S(1)}, bf16[32,1536]{1,0:T(8,128)(2,1)S(1)}, u32[]{:S(2)}, u32[]{:S(2)}) collective-permute-start(bf16[32,1536]{1,0:T(8,128)(2,1)S(1)} %pad_maximum_fusion.6), channel_id=1, source_target_pairs={{0,16},{8,24},{16,0},{24,8},{1,17},{9,25},{17,1},{25,9},{2,18},{10... | collective-permute-start | bytes 294920 | tf_op jit(solution)/shard_map/ppermute | solution.py:39
  86.0 23.4 %copy-start = (f32[8,4,128,128]{3,2,1,0:T(8,128)S(1)}, f32[8,4,128,128]{3,2,1,0:T(8,128)}, u32[]{:S(2)}) copy-start(f32[8,4,128,128]{3,2,1,0:T(8,128)} %state_ref.1) | copy-start | bytes 6291460
  86.0 23.4 %copy-start.1 = (f32[4]{0:T(128)S(1)}, f32[4]{0:T(128)}, u32[]{:S(2)}) copy-start(f32[4]{0:T(128)} %param.34) | copy-start | bytes 52
  86.0 23.4 %copy-start.2 = (f32[4]{0:T(128)S(1)}, f32[4]{0:T(128)}, u32[]{:S(2)}) copy-start(f32[4]{0:T(128)} %param.35) | copy-start | bytes 52
  86.1 23.4 %copy-start.3 = (f32[128]{0:T(128)S(1)}, f32[128]{0:T(128)}, u32[]{:S(2)}) copy-start(f32[128]{0:T(128)} %param.36) | copy-start | bytes 1540
  134.1 6.2 %collective-permute-start.11 = (bf16[32,1536]{1,0:T(8,128)(2,1)S(1)}, bf16[32,1536]{1,0:T(8,128)(2,1)S(1)}, u32[]{:S(2)}, u32[]{:S(2)}) collective-permute-start(bf16[32,1536]{1,0:T(8,128)(2,1)S(1)} %pad_maximum_fusion.7), channel_id=1, source_target_pairs={{0,8},{8,16},{16,24},{24,0},{1,9},{9,17},{17,25},{25,1},{2,10},{10... | collective-permute-start | bytes 294920 | tf_op jit(solution)/shard_map/ppermute | solution.py:39
  134.5 5.8 %collective-permute-start.12 = (bf16[32,1536]{1,0:T(8,128)(2,1)S(1)}, bf16[32,1536]{1,0:T(8,128)(2,1)S(1)}, u32[]{:S(2)}, u32[]{:S(2)}) collective-permute-start(bf16[32,1536]{1,0:T(8,128)(2,1)S(1)} %pad_maximum_fusion.7), channel_id=1, source_target_pairs={{0,16},{8,24},{16,0},{24,8},{1,17},{9,25},{17,1},{25,9},{2,18},{10... | collective-permute-start | bytes 294920 | tf_op jit(solution)/shard_map/ppermute | solution.py:39
  136.3 4.9 %collective-permute-start.13 = (bf16[32,1536]{1,0:T(8,128)(2,1)S(1)}, bf16[32,1536]{1,0:T(8,128)(2,1)S(1)}, u32[]{:S(2)}, u32[]{:S(2)}) collective-permute-start(bf16[32,1536]{1,0:T(8,128)(2,1)S(1)} %pad_maximum_fusion.7), channel_id=1, source_target_pairs={{0,24},{8,0},{16,8},{24,16},{1,25},{9,1},{17,9},{25,17},{2,26},{10... | collective-permute-start | bytes 294920 | tf_op jit(solution)/shard_map/ppermute | solution.py:39
Sparse Core Ops, SparseCore 0:
  32.3 44.5 all-gather.4
  78.6 38.0 all-gather.2

commit v2 on v1

--- a/solution.py
+++ b/solution.py
@@ -1,5 +1,6 @@
 import jax
 import jax.numpy as jnp
+import numpy as np
 from jax import lax
 from jax.experimental import pallas as pl
 from jax.experimental.pallas import tpu as pltpu
@@ -45,10 +46,12 @@
 
 
 def square_columns(as_float):
-    squares = jnp.sum(as_float * as_float, axis=1, keepdims=True)
+    return two_terms(jnp.sum(as_float * as_float, axis=1, keepdims=True))
+
+
+def two_terms(squares):
     high = squares.astype(bf16).astype(f32)
-    lane = lax.broadcasted_iota(jnp.int32, (squares.shape[0], GATES), 1)
-    return jnp.where(lane == 0, high, jnp.where(lane == 1, squares - high, 0.0))
+    return high * np.eye(1, GATES, 0, np.float32) + (squares - high) * np.eye(1, GATES, 1, np.float32)
 
 
 def row_scale(first_two):
@@ -64,15 +67,15 @@
     for step in range(1, size // 2):
         forward = blocks[size - step] = lax.ppermute(forward, axis, ahead)
         backward = blocks[step] = lax.ppermute(backward, axis, behind)
-    half = block.shape[1] // 256 * 128
+    half = (block.shape[1] + 128) // 256 * 128
     forward = lax.ppermute(forward[:, :half], axis, ahead)
     backward = lax.ppermute(backward[:, half:], axis, behind)
     blocks[size // 2] = jnp.concatenate([forward, backward], axis=1)
     return blocks
 
 
-def hidden_units(residual, partial_value):
-    both = jnp.concatenate([partial_value, square_columns(residual.astype(f32))], axis=1).astype(bf16)
+def hidden_units(partial_value, squares):
+    both = jnp.concatenate([partial_value, squares], axis=1).astype(bf16)
     summed = ring_sum(both, "y")
     width = partial_value.shape[1]
     scale = row_scale(summed[:, width:])
@@ -202,9 +205,10 @@
         lax.dynamic_slice_in_dim(decay_weight, head_start, heads_dev, 1),
         jnp.zeros((beta_weight.shape[0], GATES - 2 * heads_dev), bf16),
     ]
-    first_in = scaled_rows(norm_gain_first, [gate_first, up_first])
-    width = first_in.shape[1]
-    first_blocks = around(jnp.concatenate([first_in, down_first.T], axis=1), "z")
+    columns = from_everyone(residual_in.T, TP)
+    own_cols, batch = columns.shape[1:]
+    rows, block_size = batch // planes, own_cols * tp_count
+    down_blocks = around(down_first.T, "z")
     mixer_in = scaled_rows(
         norm_gain_mixer, [query_weight, key_weight, value_weight, output_gate_weight, *gate_cols]
     )
@@ -212,43 +216,33 @@
     mixer_width = mixer_in.shape[1]
     middle = jnp.concatenate([mixer_in, out_weight.T], axis=1)
     last = jnp.concatenate([second_in, down_second.T], axis=1)
-    first_blocks[2], first_blocks[-2], middle, last = lax.optimization_barrier(
-        (first_blocks[2], first_blocks[-2], middle, last)
-    )
+    residual = columns.reshape(block_size, batch).T
+    as_float = residual.astype(f32)
+    scaled = (as_float * norm_gain_first).astype(bf16)
+    first_in = jnp.concatenate([gate_first, up_first], axis=1)
+    width = first_in.shape[1]
+    partial_value = jnp.dot(scaled, first_in, preferred_element_type=f32).astype(bf16)
+    spare = square_columns(as_float)[:, : GATES - block_size].astype(bf16)
+    pieces = jnp.concatenate([partial_value, spare, residual], axis=1)
+    arrived = exchange(pieces.reshape(planes, rows, -1), "z")
     middle = gathered([middle])
+    down_blocks[3], down_blocks[-3], last, plane = lax.optimization_barrier(
+        (down_blocks[3], down_blocks[-3], last, lax.axis_index("z"))
+    )
     last = gathered([last])
     mixer_in, out_rows = middle[:, :mixer_width], middle[:, mixer_width:]
     second_in, down_second = last[:, :width], last[:, width:]
 
-    columns = residual_in.T
-    own_cols, rows = columns.shape[0], columns.shape[1] // planes
-    pieces = jnp.moveaxis(columns.reshape(own_cols, planes, rows), 1, 0)
-    pieces = jnp.broadcast_to(pieces[:, None], (planes, tp_count, own_cols, rows))
-    arrived = exchange(pieces.reshape(-1, own_cols, rows), ACROSS)
-    arrived = arrived.reshape(planes, -1, rows)
-    arrived, first_blocks[3], first_blocks[-3] = lax.optimization_barrier(
-        (arrived, first_blocks[3], first_blocks[-3])
-    )
-    residual = arrived.reshape(-1, rows).T
-    across = planes * own_cols * tp_count
-    block_size = own_cols * tp_count
+    across = planes * block_size
     to = lax.broadcasted_iota(jnp.int32, (across, across), 1)
     at = lax.broadcasted_iota(jnp.int32, (across, across), 0)
-    turned = lax.rem(to + (planes - lax.axis_index("z")) * block_size, across)
-    order = (at == turned).astype(bf16)
-    twice = jnp.concatenate([arrived, arrived], axis=0)
-    ahead = lax.dynamic_slice_in_dim(twice, lax.axis_index("z"), planes, 0)
-    products = [
-        lax.dot_general(ahead[o], first_blocks[o][:, :width], (((0,), (0,)), ((), ())), preferred_element_type=f32)
-        for step in range(planes // 2 + 1)
-        for o in sorted({step, (planes - step) % planes})
-    ]
-    partial_value = products[0]
-    for product in products[1:]:
-        partial_value = partial_value + product
-
-    hidden = hidden_units(residual, partial_value)
-    down_first = jnp.concatenate([block[:, width:] for block in first_blocks], axis=0)
+    order = (at == lax.rem(to + (planes - plane) * block_size, across)).astype(bf16)
+
+    residual = jnp.moveaxis(arrived[:, :, width + GATES - block_size :], 0, 1).reshape(rows, across)
+    summed = arrived[:, :, : width + GATES - block_size].astype(f32).sum(axis=0)
+    squares = two_terms(summed[:, width : width + 1] + summed[:, width + 1 : width + 2])
+    hidden = hidden_units(summed[:, :width], squares)
+    down_first = jnp.concatenate(down_blocks, axis=0)
     projected = times_transposed(hidden, down_first).astype(bf16)
     projected = jnp.dot(projected, order, preferred_element_type=f32).astype(bf16)
     after_first = (residual.astype(f32) + 0.5 * everyone_sum(projected, TP)).astype(bf16)
@@ -260,7 +254,8 @@
     projected = times_transposed(normed, out_rows).astype(bf16)
     after_mixer = (after_first.astype(f32) + everyone_sum(projected, TP)).astype(bf16)
 
-    hidden = hidden_units(after_mixer, jnp.dot(after_mixer, second_in, preferred_element_type=f32))
+    partial_value = jnp.dot(after_mixer, second_in, preferred_element_type=f32)
+    hidden = hidden_units(partial_value, square_columns(after_mixer.astype(f32)))
     projected = times_transposed(down_second, hidden).astype(bf16)
     pieces = jnp.concatenate([projected, after_mixer.T], axis=1)
     arrived = exchange(pieces.reshape(-1, own_cols, 2 * rows), ACROSS)

time: 169 us -> 174 us (1.030)
  blocking collectives: 57.7 us -> 45.2 us
  starting transfers between devices: 29.7 us -> 38.1 us
  waiting for transfers between devices: 44.8 us -> 52.8 us
  local copies, waits for them, and re-layouts: 4.4 us -> 6.91 us
    ppermute x3, waiting for transfers between devices: 16.7 us -> 31 us  [around(): backward = blocks[step] = lax.ppermute(backward, axis, behind)]
    all_to_all x5 -> x4, blocking collectives: 57.7 us -> 45.2 us  [exchange(): return lax.all_to_all(blocks, axis, split_axis=0, concat_axis=0, tiled=True)]
    all_to_all x1 -> x3, starting transfers between devices: 8.75 us -> 18.1 us  [exchange(): return lax.all_to_all(blocks, axis, split_axis=0, concat_axis=0, tiled=True)]
    ppermute x3, waiting for transfers between devices: 4.94 us -> 1.47 us  [around(): forward = blocks[size - step] = lax.ppermute(forward, axis, ahead)]
    ppermute x1, waiting for transfers between devices: 5.75 us -> 2.6 us  [around(): forward = lax.ppermute(forward[:, :half], axis, ahead)]
    broadcast_in_dim x2 -> x3, local copies, waits for them, and re-layouts: 0.06 us -> 2.08 us  [from_everyone(): jnp.broadcast_to(value, (lax.axis_size(axis), *value.shape))]
    ppermute x6, waiting for transfers between devices: 8.15 us -> 6.39 us  [ring_sum(): lax.ppermute(value, axis, [(i, (i + places) % size) for i in range(size)])]
    all_to_all x1 -> x3, waiting for transfers between devices: 9.29 us -> 9.91 us  [exchange(): return lax.all_to_all(blocks, axis, split_axis=0, concat_axis=0, tiled=True)]
  transfers between devices with their start and end apart: 17 -> 19, of which waited for: 10 -> 11; matrix products, arithmetic and copies ran while one was open for 8% -> 7% of each run, Pallas kernels for 1% -> 1%
where the time goes in v2:
time: 174 us; the launch traced here: 173 us
  waiting for transfers between devices  52.8 us (30%)
  blocking collectives  45.2 us (26%)
  starting transfers between devices  38.1 us (22%)
  between operations  14.4 us (8%)
  matrix products  7.25 us (4%)
  local copies, waits for them, and re-layouts  6.91 us (4%)
  other arithmetic  6.28 us (4%)
  Pallas kernels  2.23 us (1%)
    all_to_all x4, blocking collectives, exchange(): return lax.all_to_all(blocks, axis, split_axis=0, concat_axis=0, tiled=True)  45.2 us
    ppermute x3, waiting for transfers between devices, around(): backward = blocks[step] = lax.ppermute(backward, axis, behind)  31 us
    all_to_all x3, starting transfers between devices, exchange(): return lax.all_to_all(blocks, axis, split_axis=0, concat_axis=0, tiled=True)  18.1 us
    all_to_all x3, waiting for transfers between devices, exchange(): return lax.all_to_all(blocks, axis, split_axis=0, concat_axis=0, tiled=True)  9.91 us
    ppermute x3, starting transfers between devices, around(): backward = blocks[step] = lax.ppermute(backward, axis, behind)  9.74 us
    ppermute x6, starting transfers between devices, ring_sum(): lax.ppermute(value, axis, [(i, (i + places) % size) for i in range(size)])  7.83 us
    ppermute x6, waiting for transfers between devices, ring_sum(): lax.ppermute(value, axis, [(i, (i + places) % size) for i in range(size)])  6.39 us
  transfers between devices with their start and end apart: 19, of which 11 were waited for; matrix products, arithmetic and copies ran while one was open for 7% of the time, Pallas kernels for 1%

profile of v2, /device:TPU:1, one launch (start us, length us, event | category | flops | bytes accessed | tf_op | source)
XLA Modules:
  0.0 173.2 jit_solution(5955357773288521888)
XLA Ops:
  7.3 0.7 constant_dynamic-slice_fusion
  8.0 0.1 copy.48
  8.1 0.1 copy.49
  8.2 1.0 concatenate.55
  9.3 0.8 multiply_convert_fusion
  10.0 1.6 pad_maximum_fusion.1
  11.6 6.5 %collective-permute-start = (bf16[64,704]{1,0:T(8,128)(2,1)}, bf16[64,704]{1,0:T(8,128)(2,1)S(1)}, u32[]{:S(2)}, u32[]{:S(2)}) collective-permute-start(bf16[64,704]{1,0:T(8,128)(2,1)} %bitcast.61), channel_id=1, source_target_pairs={{0,224},{32,0},{64,32},{96,64},{128,96},{160,128},{192,160},{224,1... | collective-permute-start | bytes 270344 | tf_op jit(solution)/shard_map/ppermute | solution.py:69
  18.1 1.3 broadcast_in_dim.27
  19.4 5.3 %all-to-all-start = ((bf16[8,8,256]{2,1,0:T(8,128)(2,1)}), bf16[8,8,256]{2,1,0:T(8,128)(2,1)S(1)}, u32[]{:S(2)}, u32[]{:S(2)}) async-start(bf16[8,8,256]{2,1,0:T(8,128)(2,1)} %broadcast_in_dim.27), calls=%async_computation | async-start | bytes 65536 | tf_op jit(solution)/shard_map/all_to_all | solution.py:25
  24.7 1.0 multiply_convert_fusion.1
  25.7 3.7 %all-to-all-done = bf16[8,8,256]{2,1,0:T(8,128)(2,1)S(1)} async-done(((bf16[8,8,256]{2,1,0:T(8,128)(2,1)}), bf16[8,8,256]{2,1,0:T(8,128)(2,1)S(1)}, u32[]{:S(2)}, u32[]{:S(2)}) %all-to-all-start) | async-done | bytes 32800 | tf_op jit(solution)/shard_map/all_to_all | solution.py:25
  29.4 0.1 copy.46
  29.5 0.1 fusion.15
  29.6 0.1 add_convert_fusion
  29.8 0.3 convolution_convert_fusion
  30.2 1.1 concatenate.51
  31.2 4.4 %all-to-all-start.1 = ((bf16[8,32,1536]{2,1,0:T(8,128)(2,1)}), bf16[8,32,1536]{2,1,0:T(8,128)(2,1)S(1)}, u32[]{:S(2)}, u32[]{:S(2)}) async-start(bf16[8,32,1536]{2,1,0:T(8,128)(2,1)} %bitcast.5), calls=%async_computation.1 | async-start | bytes 1572864 | tf_op jit(solution)/shard_map/all_to_all | solution.py:25
  35.6 0.7 pad_maximum_fusion
  36.4 2.7 %collective-permute-start.1 = (bf16[64,704]{1,0:T(8,128)(2,1)S(1)}, bf16[64,704]{1,0:T(8,128)(2,1)S(1)}, u32[]{:S(2)}, u32[]{:S(2)}) collective-permute-start(bf16[64,704]{1,0:T(8,128)(2,1)S(1)} %collective-permute-done), channel_id=1, source_target_pairs={{0,224},{32,0},{64,32},{96,64},{128,96},{160,128},{192,160},{224,1... | collective-permute-start | bytes 270344 | tf_op jit(solution)/shard_map/ppermute | solution.py:69
  39.1 27.6 %collective-permute-done.1 = bf16[64,704]{1,0:T(8,128)(2,1)S(1)} collective-permute-done((bf16[64,704]{1,0:T(8,128)(2,1)S(1)}, bf16[64,704]{1,0:T(8,128)(2,1)S(1)}, u32[]{:S(2)}, u32[]{:S(2)}) %collective-permute-start.1) | collective-permute-done | bytes 90144 | tf_op jit(solution)/shard_map/ppermute | solution.py:69
  66.8 0.6 collective-permute-start.2
  67.3 0.9 collective-permute-start.5
  68.2 3.3 %collective-permute-done.2 = bf16[64,704]{1,0:T(8,128)(2,1)S(1)} collective-permute-done((bf16[64,704]{1,0:T(8,128)(2,1)S(1)}, bf16[64,704]{1,0:T(8,128)(2,1)S(1)}, u32[]{:S(2)}, u32[]{:S(2)}) %collective-permute-start.2) | collective-permute-done | bytes 90144 | tf_op jit(solution)/shard_map/ppermute | solution.py:69
  71.6 1.5 collective-permute-done.5
  73.0 1.4 collective-permute-start.10
  74.4 0.1 collective-permute-start.9
  74.6 1.4 collective-permute-done.10
  76.0 2.6 %collective-permute-done.9 = bf16[64,384]{1,0:T(8,128)(2,1)S(1)} collective-permute-done((bf16[64,384]{1,0:T(8,128)(2,1)S(1)}, bf16[64,384]{1,0:T(8,128)(2,1)S(1)}, u32[]{:S(2)}, u32[]{:S(2)}) %collective-permute-start.9) | collective-permute-done | bytes 49184 | tf_op jit(solution)/shard_map/ppermute | solution.py:71
  78.6 0.1 convert_reduce_fusion
  78.8 0.2 convert_reduce_fusion.3
  79.0 1.3 collective-permute-start.6
  80.3 2.4 %collective-permute-start.7 = (bf16[32,1536]{1,0:T(8,128)(2,1)S(1)}, bf16[32,1536]{1,0:T(8,128)(2,1)S(1)}, u32[]{:S(2)}, u32[]{:S(2)}) collective-permute-start(bf16[32,1536]{1,0:T(8,128)(2,1)S(1)} %pad_maximum_fusion.3), channel_id=1, source_target_pairs={{0,16},{8,24},{16,0},{24,8},{1,17},{9,25},{17,1},{25,9},{2,18},{10... | collective-permute-start | bytes 294920 | tf_op jit(solution)/shard_map/ppermute | solution.py:40
  82.7 1.2 collective-permute-start.8
  83.9 1.8 %collective-permute-done.7 = bf16[32,1536]{1,0:T(8,128)(2,1)S(1)} collective-permute-done((bf16[32,1536]{1,0:T(8,128)(2,1)S(1)}, bf16[32,1536]{1,0:T(8,128)(2,1)S(1)}, u32[]{:S(2)}, u32[]{:S(2)}) %collective-permute-start.7) | collective-permute-done | bytes 98336 | tf_op jit(solution)/shard_map/ppermute | solution.py:40
  85.8 0.4 collective-permute-done.8
  86.3 0.2 fusion.48
  86.4 0.5 convolution_convert_fusion.3
  87.0 0.7 broadcast_in_dim.28
  87.7 8.5 %all-to-all-start.2 = ((bf16[8,32,512]{2,1,0:T(8,128)(2,1)}), bf16[8,32,512]{2,1,0:T(8,128)(2,1)S(1)}, u32[]{:S(2)}, u32[]{:S(2)}) async-start(bf16[8,32,512]{2,1,0:T(8,128)(2,1)} %broadcast_in_dim.28), calls=%async_computation.2 | async-start | bytes 524288 | tf_op jit(solution)/shard_map/all_to_all | solution.py:25
  96.2 0.1 convert_bitcast_fusion
  96.4 0.1 reshape.71
  96.5 6.3 %all-to-all-done.2 = bf16[8,32,512]{2,1,0:T(8,128)(2,1)S(1)} async-done(((bf16[8,32,512]{2,1,0:T(8,128)(2,1)}), bf16[8,32,512]{2,1,0:T(8,128)(2,1)S(1)}, u32[]{:S(2)}, u32[]{:S(2)}) %all-to-all-start.2) | async-done | bytes 262176 | tf_op jit(solution)/shard_map/all_to_all | solution.py:25
  102.9 0.2 fusion.16
  103.3 1.9 %fusion = f32[32,1664]{1,0:T(8,128)S(1)} fusion(bf16[32,512]{1,0:T(8,128)(2,1)S(1)} %get-tuple-element.16, bf16[512,2176]{1,0:T(8,128)(2,1)} %all-gather.5.cloned.1.call-done), kind=kOutput, calls=%fused_computation.2 | convolution fusion | flops 54525952 | bytes 1949696 | tf_op jit(solution)/shard_map/dot_general | solution.py:145
  105.3 8.0 %all_to_all.35.arrived_ref = bf16[4,8,1664]{2,1,0:T(8,128)(2,1)S(1)} all-to-all(bf16[4,8,1664]{2,1,0:T(8,128)(2,1)S(1)} %pad_maximum_fusion.2), channel_id=1, replica_groups=mesh['z'=8,'y'=4,'x'=4,'c'=2] {'y'}, dimensions={0} | all-to-all | bytes 212992 | tf_op jit(solution)/shard_map/all_to_all | solution.py:25
  113.3 2.2 %shard_map.284 = (bf16[4,8,512]{2,1,0:T(8,128)(2,1)S(1)}, f32[8,4,128,128]{3,2,1,0:T(8,128)}) custom-call(bf16[4,8,1664]{2,1,0:T(8,128)(2,1)S(1)} %all_to_all.35.arrived_ref, f32[1,4]{1,0:T(1,128)S(1)} %bitcast.54, f32[1,4]{1,0:T(1,128)S(1)} %bitcast.55, f32[1,128]{1,0:T(1,128)S(1)} %bitcast.56, f32[8,4,128,128]{3,2,1,0:T(8,128)S(1)} %copy-done), custom_call_target="tpu_custom_call" | custom-call | flops 20000000 | bytes 4200000 | tf_op jit(solution)/shard_map/pallas_call | solution.py:152
  115.6 6.7 %all_to_all.36 = bf16[4,8,512]{2,1,0:T(8,128)(2,1)S(1)} all-to-all(bf16[4,8,512]{2,1,0:T(8,128)(2,1)S(1)} %get-tuple-element.12), channel_id=1, replica_groups=mesh['z'=8,'y'=4,'x'=4,'c'=2] {'y'}, dimensions={0} | all-to-all | bytes 65536 | tf_op jit(solution)/shard_map/all_to_all | solution.py:25
  122.2 1.3 convolution_convert_fusion.5
  123.5 12.4 %all_to_all.37 = bf16[8,32,512]{2,1,0:T(8,128)(2,1)S(1)} all-to-all(bf16[8,32,512]{2,1,0:T(8,128)(2,1)S(1)} %broadcast_in_dim.33), channel_id=1, replica_groups=mesh['z'=8,'y'=4,'x'=4,'c'=2] {'x','c'}, dimensions={0} | all-to-all | bytes 524288 | tf_op jit(solution)/shard_map/all_to_all | solution.py:25
  136.0 0.1 reduce_sum.70
  136.1 0.2 multiply_reduce_fusion
  136.4 1.7 convolution_convert_fusion.1
  138.1 0.4 collective-permute-start.11
  138.5 1.8 %collective-permute-start.12 = (bf16[32,1536]{1,0:T(8,128)(2,1)S(1)}, bf16[32,1536]{1,0:T(8,128)(2,1)S(1)}, u32[]{:S(2)}, u32[]{:S(2)}) collective-permute-start(bf16[32,1536]{1,0:T(8,128)(2,1)S(1)} %pad_maximum_fusion.4), channel_id=1, source_target_pairs={{0,16},{8,24},{16,0},{24,8},{1,17},{9,25},{17,1},{25,9},{2,18},{10... | collective-permute-start | bytes 294920 | tf_op jit(solution)/shard_map/ppermute | solution.py:40
  140.3 0.8 collective-permute-start.13
  141.1 3.2 %collective-permute-done.11 = bf16[32,1536]{1,0:T(8,128)(2,1)S(1)} collective-permute-done((bf16[32,1536]{1,0:T(8,128)(2,1)S(1)}, bf16[32,1536]{1,0:T(8,128)(2,1)S(1)}, u32[]{:S(2)}, u32[]{:S(2)}) %collective-permute-start.11) | collective-permute-done | bytes 98336 | tf_op jit(solution)/shard_map/ppermute | solution.py:40
  144.3 0.9 collective-permute-done.13
  145.3 0.2 fusion.43
  145.5 1.5 convolution_convert_fusion.2
  147.0 0.1 copy.52
  147.1 0.2 reshape.77
  147.3 18.1 %all_to_all.38 = bf16[64,2,256]{2,1,0:T(2,128)(2,1)S(1)} all-to-all(bf16[64,2,256]{2,1,0:T(2,128)(2,1)S(1)} %reshape.77), channel_id=1, replica_groups=mesh['z'=8,'y'=4,'x'=4,'c'=2] {'z','x','c'}, dimensions={0} | all-to-all | bytes 131072 | tf_op jit(solution)/shard_map/all_to_all | solution.py:25
  165.4 0.1 reshape.78
  165.7 0.7 convert_element_type.251
  (76 shorter events, 1.3 us)
Async XLA Ops:
  7.2 22.5 %copy-start.8 = (f32[128]{0:T(128)S(1)}, f32[128]{0:T(128)}, u32[]{:S(2)}) copy-start(f32[128]{0:T(128)} %constant.58) | copy-start | bytes 1540
  7.2 22.5 %copy-start.9 = (f32[128]{0:T(128)S(1)}, f32[128]{0:T(128)}, u32[]{:S(2)}) copy-start(f32[128]{0:T(128)} %constant.57) | copy-start | bytes 1540
  7.2 22.6 %copy-start.10 = (f32[64]{0:T(128)S(1)}, f32[64]{0:T(128)}, u32[]{:S(2)}) copy-start(f32[64]{0:T(128)} %param.31) | copy-start | bytes 772
  7.2 22.6 %copy-start.5 = (bf16[64,704]{1,0:T(8,128)(2,1)S(1)}, bf16[64,704]{1,0:T(8,128)(2,1)}, u32[]{:S(2)}) copy-start(bf16[64,704]{1,0:T(8,128)(2,1)} %param.32) | copy-start | bytes 270340
  7.2 22.6 %copy-start.4 = (bf16[64,704]{1,0:T(8,128)(2,1)S(1)}, bf16[64,704]{1,0:T(8,128)(2,1)}, u32[]{:S(2)}) copy-start(bf16[64,704]{1,0:T(8,128)(2,1)} %param.33) | copy-start | bytes 270340
  7.2 96.0 %all-gather.5.cloned.1.call-start = ((), (), s32[]{:S(2)}) async-start(), calls=%async_computation.8 | async-start | bytes 2506752 | tf_op jit(solution)/shard_map/all_gather | solution.py:200
  11.6 24.8 %collective-permute-start = (bf16[64,704]{1,0:T(8,128)(2,1)}, bf16[64,704]{1,0:T(8,128)(2,1)S(1)}, u32[]{:S(2)}, u32[]{:S(2)}) collective-permute-start(bf16[64,704]{1,0:T(8,128)(2,1)} %bitcast.61), channel_id=1, source_target_pairs={{0,224},{32,0},{64,32},{96,64},{128,96},{160,128},{192,160},{224,1... | collective-permute-start | bytes 270344 | tf_op jit(solution)/shard_map/ppermute | solution.py:69
  18.1 21.0 %collective-permute-start.3 = (bf16[64,704]{1,0:T(8,128)(2,1)}, bf16[64,704]{1,0:T(8,128)(2,1)S(1)}, u32[]{:S(2)}, u32[]{:S(2)}) collective-permute-start(bf16[64,704]{1,0:T(8,128)(2,1)} %bitcast.62), channel_id=1, source_target_pairs={{0,32},{32,64},{64,96},{96,128},{128,160},{160,192},{192,224},{224... | collective-permute-start | bytes 270344 | tf_op jit(solution)/shard_map/ppermute | solution.py:68
  19.4 10.0 %all-to-all-start = ((bf16[8,8,256]{2,1,0:T(8,128)(2,1)}), bf16[8,8,256]{2,1,0:T(8,128)(2,1)S(1)}, u32[]{:S(2)}, u32[]{:S(2)}) async-start(bf16[8,8,256]{2,1,0:T(8,128)(2,1)} %broadcast_in_dim.27), calls=%async_computation | async-start | bytes 65536 | tf_op jit(solution)/shard_map/all_to_all | solution.py:25
  25.7 9.9 %copy-start.7 = (bf16[704,64]{0,1:T(8,128)(2,1)S(1)}, bf16[704,64]{0,1:T(8,128)(2,1)}, u32[]{:S(2)}) copy-start(bf16[704,64]{0,1:T(8,128)(2,1)} %param.49) | copy-start | bytes 270340
  29.8 6.6 %copy-start.6 = (bf16[704,64]{0,1:T(8,128)(2,1)S(1)}, bf16[704,64]{0,1:T(8,128)(2,1)}, u32[]{:S(2)}) copy-start(bf16[704,64]{0,1:T(8,128)(2,1)} %param.34) | copy-start | bytes 270340
  31.2 47.4 %all-to-all-start.1 = ((bf16[8,32,1536]{2,1,0:T(8,128)(2,1)}), bf16[8,32,1536]{2,1,0:T(8,128)(2,1)S(1)}, u32[]{:S(2)}, u32[]{:S(2)}) async-start(bf16[8,32,1536]{2,1,0:T(8,128)(2,1)} %bitcast.5), calls=%async_computation.1 | async-start | bytes 1572864 | tf_op jit(solution)/shard_map/all_to_all | solution.py:25
  35.6 100.8 %all-gather.3.cloned.1.call-start = ((), (), s32[]{:S(2)}) async-start(), calls=%async_computation.7 | async-start | bytes 2506752 | tf_op jit(solution)/shard_map/all_gather | solution.py:200
  36.4 30.4 %collective-permute-start.1 = (bf16[64,704]{1,0:T(8,128)(2,1)S(1)}, bf16[64,704]{1,0:T(8,128)(2,1)S(1)}, u32[]{:S(2)}, u32[]{:S(2)}) collective-permute-start(bf16[64,704]{1,0:T(8,128)(2,1)S(1)} %collective-permute-done), channel_id=1, source_target_pairs={{0,224},{32,0},{64,32},{96,64},{128,96},{160,128},{192,160},{224,1... | collective-permute-start | bytes 270344 | tf_op jit(solution)/shard_map/ppermute | solution.py:69
  39.1 28.2 %collective-permute-start.4 = (bf16[64,704]{1,0:T(8,128)(2,1)S(1)}, bf16[64,704]{1,0:T(8,128)(2,1)S(1)}, u32[]{:S(2)}, u32[]{:S(2)}) collective-permute-start(bf16[64,704]{1,0:T(8,128)(2,1)S(1)} %collective-permute-done.3), channel_id=1, source_target_pairs={{0,32},{32,64},{64,96},{96,128},{128,160},{160,192},{192,224},{224... | collective-permute-start | bytes 270344 | tf_op jit(solution)/shard_map/ppermute | solution.py:68
  66.8 4.8 %collective-permute-start.2 = (bf16[64,704]{1,0:T(8,128)(2,1)S(1)}, bf16[64,704]{1,0:T(8,128)(2,1)S(1)}, u32[]{:S(2)}, u32[]{:S(2)}) collective-permute-start(bf16[64,704]{1,0:T(8,128)(2,1)S(1)} %collective-permute-done.1), channel_id=1, source_target_pairs={{0,224},{32,0},{64,32},{96,64},{128,96},{160,128},{192,160},{224,1... | collective-permute-start | bytes 270344 | tf_op jit(solution)/shard_map/ppermute | solution.py:69
  67.3 5.7 %collective-permute-start.5 = (bf16[64,704]{1,0:T(8,128)(2,1)S(1)}, bf16[64,704]{1,0:T(8,128)(2,1)S(1)}, u32[]{:S(2)}, u32[]{:S(2)}) collective-permute-start(bf16[64,704]{1,0:T(8,128)(2,1)S(1)} %collective-permute-done.4), channel_id=1, source_target_pairs={{0,32},{32,64},{64,96},{96,128},{128,160},{160,192},{192,224},{224... | collective-permute-start | bytes 270344 | tf_op jit(solution)/shard_map/ppermute | solution.py:68
  73.0 2.9 %collective-permute-start.10 = (bf16[64,320]{1,0:T(8,128)(2,1)S(1)}, bf16[64,320]{1,0:T(8,128)(2,1)S(1)}, u32[]{:S(2)}, u32[]{:S(2)}) collective-permute-start(bf16[64,320]{1,0:T(8,128)(2,1)S(1)} %slice.128), channel_id=1, source_target_pairs={{0,224},{32,0},{64,32},{96,64},{128,96},{160,128},{192,160},{224,1... | collective-permute-start | bytes 122888 | tf_op jit(solution)/shard_map/ppermute | solution.py:72
  74.4 4.2 %collective-permute-start.9 = (bf16[64,384]{1,0:T(8,128)(2,1)S(1)}, bf16[64,384]{1,0:T(8,128)(2,1)S(1)}, u32[]{:S(2)}, u32[]{:S(2)}) collective-permute-start(bf16[64,384]{1,0:T(8,128)(2,1)S(1)} %slice.127), channel_id=1, source_target_pairs={{0,32},{32,64},{64,96},{96,128},{128,160},{160,192},{192,224},{224... | collective-permute-start | bytes 147464 | tf_op jit(solution)/shard_map/ppermute | solution.py:71
  79.0 4.9 %collective-permute-start.6 = (bf16[32,1536]{1,0:T(8,128)(2,1)S(1)}, bf16[32,1536]{1,0:T(8,128)(2,1)S(1)}, u32[]{:S(2)}, u32[]{:S(2)}) collective-permute-start(bf16[32,1536]{1,0:T(8,128)(2,1)S(1)} %pad_maximum_fusion.3), channel_id=1, source_target_pairs={{0,8},{8,16},{16,24},{24,0},{1,9},{9,17},{17,25},{25,1},{2,10},{10... | collective-permute-start | bytes 294920 | tf_op jit(solution)/shard_map/ppermute | solution.py:40
  80.3 5.4 %collective-permute-start.7 = (bf16[32,1536]{1,0:T(8,128)(2,1)S(1)}, bf16[32,1536]{1,0:T(8,128)(2,1)S(1)}, u32[]{:S(2)}, u32[]{:S(2)}) collective-permute-start(bf16[32,1536]{1,0:T(8,128)(2,1)S(1)} %pad_maximum_fusion.3), channel_id=1, source_target_pairs={{0,16},{8,24},{16,0},{24,8},{1,17},{9,25},{17,1},{25,9},{2,18},{10... | collective-permute-start | bytes 294920 | tf_op jit(solution)/shard_map/ppermute | solution.py:40
  82.7 3.5 %collective-permute-start.8 = (bf16[32,1536]{1,0:T(8,128)(2,1)S(1)}, bf16[32,1536]{1,0:T(8,128)(2,1)S(1)}, u32[]{:S(2)}, u32[]{:S(2)}) collective-permute-start(bf16[32,1536]{1,0:T(8,128)(2,1)S(1)} %pad_maximum_fusion.3), channel_id=1, source_target_pairs={{0,24},{8,0},{16,8},{24,16},{1,25},{9,1},{17,9},{25,17},{2,26},{10... | collective-permute-start | bytes 294920 | tf_op jit(solution)/shard_map/ppermute | solution.py:40
  87.7 15.1 %all-to-all-start.2 = ((bf16[8,32,512]{2,1,0:T(8,128)(2,1)}), bf16[8,32,512]{2,1,0:T(8,128)(2,1)S(1)}, u32[]{:S(2)}, u32[]{:S(2)}) async-start(bf16[8,32,512]{2,1,0:T(8,128)(2,1)} %broadcast_in_dim.28), calls=%async_computation.2 | async-start | bytes 524288 | tf_op jit(solution)/shard_map/all_to_all | solution.py:25
  96.2 17.1 %copy-start = (f32[8,4,128,128]{3,2,1,0:T(8,128)S(1)}, f32[8,4,128,128]{3,2,1,0:T(8,128)}, u32[]{:S(2)}) copy-start(f32[8,4,128,128]{3,2,1,0:T(8,128)} %state_ref.1) | copy-start | bytes 6291460
  96.2 17.1 %copy-start.1 = (f32[4]{0:T(128)S(1)}, f32[4]{0:T(128)}, u32[]{:S(2)}) copy-start(f32[4]{0:T(128)} %param.42) | copy-start | bytes 52
  96.2 17.1 %copy-start.2 = (f32[4]{0:T(128)S(1)}, f32[4]{0:T(128)}, u32[]{:S(2)}) copy-start(f32[4]{0:T(128)} %param.43) | copy-start | bytes 52
  96.2 17.1 %copy-start.3 = (f32[128]{0:T(128)S(1)}, f32[128]{0:T(128)}, u32[]{:S(2)}) copy-start(f32[128]{0:T(128)} %param.44) | copy-start | bytes 1540
  138.1 6.2 %collective-permute-start.11 = (bf16[32,1536]{1,0:T(8,128)(2,1)S(1)}, bf16[32,1536]{1,0:T(8,128)(2,1)S(1)}, u32[]{:S(2)}, u32[]{:S(2)}) collective-permute-start(bf16[32,1536]{1,0:T(8,128)(2,1)S(1)} %pad_maximum_fusion.4), channel_id=1, source_target_pairs={{0,8},{8,16},{16,24},{24,0},{1,9},{9,17},{17,25},{25,1},{2,10},{10... | collective-permute-start | bytes 294920 | tf_op jit(solution)/shard_map/ppermute | solution.py:40
  138.5 5.8 %collective-permute-start.12 = (bf16[32,1536]{1,0:T(8,128)(2,1)S(1)}, bf16[32,1536]{1,0:T(8,128)(2,1)S(1)}, u32[]{:S(2)}, u32[]{:S(2)}) collective-permute-start(bf16[32,1536]{1,0:T(8,128)(2,1)S(1)} %pad_maximum_fusion.4), channel_id=1, source_target_pairs={{0,16},{8,24},{16,0},{24,8},{1,17},{9,25},{17,1},{25,9},{2,18},{10... | collective-permute-start | bytes 294920 | tf_op jit(solution)/shard_map/ppermute | solution.py:40
  140.3 5.0 %collective-permute-start.13 = (bf16[32,1536]{1,0:T(8,128)(2,1)S(1)}, bf16[32,1536]{1,0:T(8,128)(2,1)S(1)}, u32[]{:S(2)}, u32[]{:S(2)}) collective-permute-start(bf16[32,1536]{1,0:T(8,128)(2,1)S(1)} %pad_maximum_fusion.4), channel_id=1, source_target_pairs={{0,24},{8,0},{16,8},{24,16},{1,25},{9,1},{17,9},{25,17},{2,26},{10... | collective-permute-start | bytes 294920 | tf_op jit(solution)/shard_map/ppermute | solution.py:40
Sparse Core Ops, SparseCore 0:
  11.7 59.5 all-gather.4
  74.7 37.4 all-gather.2

commit v3 on v1

--- a/solution.py
+++ b/solution.py
@@ -1,5 +1,6 @@
 import jax
 import jax.numpy as jnp
+import numpy as np
 from jax import lax
 from jax.experimental import pallas as pl
 from jax.experimental.pallas import tpu as pltpu
@@ -47,8 +48,7 @@
 def square_columns(as_float):
     squares = jnp.sum(as_float * as_float, axis=1, keepdims=True)
     high = squares.astype(bf16).astype(f32)
-    lane = lax.broadcasted_iota(jnp.int32, (squares.shape[0], GATES), 1)
-    return jnp.where(lane == 0, high, jnp.where(lane == 1, squares - high, 0.0))
+    return high * np.eye(1, GATES, 0, np.float32) + (squares - high) * np.eye(1, GATES, 1, np.float32)
 
 
 def row_scale(first_two):
@@ -205,26 +205,28 @@
     first_in = scaled_rows(norm_gain_first, [gate_first, up_first])
     width = first_in.shape[1]
     first_blocks = around(jnp.concatenate([first_in, down_first.T], axis=1), "z")
-    mixer_in = scaled_rows(
-        norm_gain_mixer, [query_weight, key_weight, value_weight, output_gate_weight, *gate_cols]
-    )
+    first_blocks[1], first_blocks[-1], query_weight, out_weight = lax.optimization_barrier(
+        (first_blocks[1], first_blocks[-1], query_weight, out_weight)
+    )
+    mixer_in = scaled_rows(norm_gain_mixer, [query_weight, key_weight, value_weight, output_gate_weight, *gate_cols])
     second_in = scaled_rows(norm_gain_second, [gate_second, up_second])
     mixer_width = mixer_in.shape[1]
     middle = jnp.concatenate([mixer_in, out_weight.T], axis=1)
     last = jnp.concatenate([second_in, down_second.T], axis=1)
-    first_blocks[2], first_blocks[-2], middle, last = lax.optimization_barrier(
-        (first_blocks[2], first_blocks[-2], middle, last)
+    columns = residual_in.T
+    own_cols, rows = columns.shape[0], columns.shape[1] // planes
+    pieces = jnp.moveaxis(columns.reshape(own_cols, planes, rows), 1, 0)
+    pieces = jnp.broadcast_to(pieces[:, None], (planes, tp_count, own_cols, rows))
+    pieces = pieces.reshape(-1, own_cols, rows)
+    first_blocks[3], first_blocks[-3], last, plane = lax.optimization_barrier(
+        (first_blocks[3], first_blocks[-3], last, lax.axis_index("z"))
     )
     middle = gathered([middle])
     last = gathered([last])
     mixer_in, out_rows = middle[:, :mixer_width], middle[:, mixer_width:]
     second_in, down_second = last[:, :width], last[:, width:]
 
-    columns = residual_in.T
-    own_cols, rows = columns.shape[0], columns.shape[1] // planes
-    pieces = jnp.moveaxis(columns.reshape(own_cols, planes, rows), 1, 0)
-    pieces = jnp.broadcast_to(pieces[:, None], (planes, tp_count, own_cols, rows))
-    arrived = exchange(pieces.reshape(-1, own_cols, rows), ACROSS)
+    arrived = exchange(pieces, ACROSS)
     arrived = arrived.reshape(planes, -1, rows)
     arrived, first_blocks[3], first_blocks[-3] = lax.optimization_barrier(
         (arrived, first_blocks[3], first_blocks[-3])
@@ -234,7 +236,7 @@
     block_size = own_cols * tp_count
     to = lax.broadcasted_iota(jnp.int32, (across, across), 1)
     at = lax.broadcasted_iota(jnp.int32, (across, across), 0)
-    turned = lax.rem(to + (planes - lax.axis_index("z")) * block_size, across)
+    turned = lax.rem(to + (planes - plane) * block_size, across)
     order = (at == turned).astype(bf16)
     twice = jnp.concatenate([arrived, arrived], axis=0)
     ahead = lax.dynamic_slice_in_dim(twice, lax.axis_index("z"), planes, 0)

time: 169 us -> 161 us (0.953)
  waiting for transfers between devices: 44.8 us -> 32.5 us
    all_to_all x1, waiting for transfers between devices: 9.29 us -> 1.9 us  [exchange(): return lax.all_to_all(blocks, axis, split_axis=0, concat_axis=0, tiled=True)]
    ppermute x3, waiting for transfers between devices: 16.7 us -> 13.4 us  [around(): backward = blocks[step] = lax.ppermute(backward, axis, behind)]
    ppermute x3, starting transfers between devices: 10.2 us -> 12.8 us  [around(): backward = blocks[step] = lax.ppermute(backward, axis, behind)]
  transfers between devices with their start and end apart: 17 -> 17, of which waited for: 10 -> 9; matrix products, arithmetic and copies ran while one was open for 8% -> 8% of each run, Pallas kernels for 1% -> 1%
where the time goes in v3:
time: 161 us; the launch traced here: 160 us
  blocking collectives  59.3 us (37%)
  waiting for transfers between devices  32.5 us (20%)
  starting transfers between devices  31.1 us (19%)
  between operations  14.6 us (9%)
  matrix products  8.45 us (5%)
  other arithmetic  5.95 us (4%)
  local copies, waits for them, and re-layouts  5.78 us (4%)
  Pallas kernels  2.23 us (1%)
    all_to_all x5, blocking collectives, exchange(): return lax.all_to_all(blocks, axis, split_axis=0, concat_axis=0, tiled=True)  59.3 us
    ppermute x3, waiting for transfers between devices, around(): backward = blocks[step] = lax.ppermute(backward, axis, behind)  13.4 us
    ppermute x3, starting transfers between devices, around(): backward = blocks[step] = lax.ppermute(backward, axis, behind)  12.8 us
    ppermute x6, waiting for transfers between devices, ring_sum(): lax.ppermute(value, axis, [(i, (i + places) % size) for i in range(size)])  8.85 us
    all_to_all x1, starting transfers between devices, exchange(): return lax.all_to_all(blocks, axis, split_axis=0, concat_axis=0, tiled=True)  8.6 us
    ppermute x6, starting transfers between devices, ring_sum(): lax.ppermute(value, axis, [(i, (i + places) % size) for i in range(size)])  8.03 us
    ppermute x1, waiting for transfers between devices, around(): forward = lax.ppermute(forward[:, :half], axis, ahead)  4.6 us
    ppermute x3, waiting for transfers between devices, around(): forward = blocks[size - step] = lax.ppermute(forward, axis, ahead)  3.7 us
  transfers between devices with their start and end apart: 17, of which 9 were waited for; matrix products, arithmetic and copies ran while one was open for 8% of the time, Pallas kernels for 1%

profile of v3, /device:TPU:1, one launch (start us, length us, event | category | flops | bytes accessed | tf_op | source)
XLA Modules:
  0.0 159.9 jit_solution(14886935697957784036)
XLA Ops:
  7.2 1.1 multiply_convert_fusion.2
  8.4 0.9 pad_maximum_fusion
  9.3 6.5 %collective-permute-start = (bf16[64,2112]{1,0:T(8,128)(2,1)S(1)}, bf16[64,2112]{1,0:T(8,128)(2,1)S(1)}, u32[]{:S(2)}, u32[]{:S(2)}) collective-permute-start(bf16[64,2112]{1,0:T(8,128)(2,1)S(1)} %pad_maximum_fusion), channel_id=1, source_target_pairs={{0,224},{32,0},{64,32},{96,64},{128,96},{160,128},{192,160},{224,1... | collective-permute-start | bytes 811016 | tf_op jit(solution)/shard_map/ppermute | solution.py:66
  15.8 0.8 reshape.68
  16.6 0.7 reshape.78
  17.3 8.6 %all-to-all-start = ((bf16[64,2,128]{2,1,0:T(2,128)(2,1)}), bf16[64,2,128]{2,1,0:T(2,128)(2,1)S(1)}, u32[]{:S(2)}, u32[]{:S(2)}) async-start(bf16[64,2,128]{2,1,0:T(2,128)(2,1)} %reshape.78), calls=%async_computation | async-start | bytes 65536 | tf_op jit(solution)/shard_map/all_to_all | solution.py:25
  26.0 0.7 constant_dynamic-slice_fusion
  26.7 0.1 copy.57
  26.8 0.1 copy.58
  27.0 1.0 concatenate.59
  28.0 0.8 multiply_convert_fusion
  28.7 0.7 pad_maximum_fusion.2
  29.6 0.1 multiply_convert_fusion.1
  29.7 2.9 %collective-permute-start.1 = (bf16[64,2112]{1,0:T(8,128)(2,1)S(1)}, bf16[64,2112]{1,0:T(8,128)(2,1)S(1)}, u32[]{:S(2)}, u32[]{:S(2)}) collective-permute-start(bf16[64,2112]{1,0:T(8,128)(2,1)S(1)} %collective-permute-done), channel_id=1, source_target_pairs={{0,224},{32,0},{64,32},{96,64},{128,96},{160,128},{192,160},{224,1... | collective-permute-start | bytes 811016 | tf_op jit(solution)/shard_map/ppermute | solution.py:66
  32.6 0.7 pad_maximum_fusion.1
  33.4 1.9 %all-to-all-done = bf16[64,2,128]{2,1,0:T(2,128)(2,1)S(1)} async-done(((bf16[64,2,128]{2,1,0:T(2,128)(2,1)}), bf16[64,2,128]{2,1,0:T(2,128)(2,1)S(1)}, u32[]{:S(2)}, u32[]{:S(2)}) %all-to-all-start) | async-done | bytes 32800 | tf_op jit(solution)/shard_map/all_to_all | solution.py:25
  35.3 0.1 reshape.79
  35.4 2.9 %collective-permute-done.1 = bf16[64,2112]{1,0:T(8,128)(2,1)S(1)} collective-permute-done((bf16[64,2112]{1,0:T(8,128)(2,1)S(1)}, bf16[64,2112]{1,0:T(8,128)(2,1)S(1)}, u32[]{:S(2)}, u32[]{:S(2)}) %collective-permute-start.1) | collective-permute-done | bytes 270368 | tf_op jit(solution)/shard_map/ppermute | solution.py:66
  38.2 3.4 %collective-permute-start.2 = (bf16[64,2112]{1,0:T(8,128)(2,1)S(1)}, bf16[64,2112]{1,0:T(8,128)(2,1)S(1)}, u32[]{:S(2)}, u32[]{:S(2)}) collective-permute-start(bf16[64,2112]{1,0:T(8,128)(2,1)S(1)} %collective-permute-done.1), channel_id=1, source_target_pairs={{0,224},{32,0},{64,32},{96,64},{128,96},{160,128},{192,160},{224,1... | collective-permute-start | bytes 811016 | tf_op jit(solution)/shard_map/ppermute | solution.py:66
  41.7 10.5 %collective-permute-done.2 = bf16[64,2112]{1,0:T(8,128)(2,1)S(1)} collective-permute-done((bf16[64,2112]{1,0:T(8,128)(2,1)S(1)}, bf16[64,2112]{1,0:T(8,128)(2,1)S(1)}, u32[]{:S(2)}, u32[]{:S(2)}) %collective-permute-start.2) | collective-permute-done | bytes 270368 | tf_op jit(solution)/shard_map/ppermute | solution.py:66
  52.2 3.7 %collective-permute-done.5 = bf16[64,2112]{1,0:T(8,128)(2,1)S(1)} collective-permute-done((bf16[64,2112]{1,0:T(8,128)(2,1)S(1)}, bf16[64,2112]{1,0:T(8,128)(2,1)S(1)}, u32[]{:S(2)}, u32[]{:S(2)}) %collective-permute-start.5) | collective-permute-done | bytes 270368 | tf_op jit(solution)/shard_map/ppermute | solution.py:65
  55.9 0.1 collective-permute-start.7
  56.0 1.5 collective-permute-start.6
  57.6 0.1 fusion.23
  57.7 0.1 copy.61
  57.8 0.1 fusion.33
  57.9 0.7 slice_dynamic-update-slice_fusion.5
  58.6 0.2 fusion.57
  58.8 0.2 fusion.19
  59.0 0.2 fusion.15
  59.2 0.2 convolution_add_fusion.4
  59.4 0.2 convolution_add_fusion.3
  59.6 0.2 fusion.1
  59.8 0.2 convolution_add_fusion.1
  60.2 4.6 %collective-permute-done.6 = bf16[64,1024]{1,0:T(8,128)(2,1)S(1)} collective-permute-done((bf16[64,1024]{1,0:T(8,128)(2,1)S(1)}, bf16[64,1024]{1,0:T(8,128)(2,1)S(1)}, u32[]{:S(2)}, u32[]{:S(2)}) %collective-permute-start.6) | collective-permute-done | bytes 131104 | tf_op jit(solution)/shard_map/ppermute | solution.py:68
  64.8 0.2 fusion.2
  65.0 3.7 %collective-permute-start.10 = (bf16[32,1536]{1,0:T(8,128)(2,1)S(1)}, bf16[32,1536]{1,0:T(8,128)(2,1)S(1)}, u32[]{:S(2)}, u32[]{:S(2)}) collective-permute-start(bf16[32,1536]{1,0:T(8,128)(2,1)S(1)} %pad_maximum_fusion.6), channel_id=1, source_target_pairs={{0,24},{8,0},{16,8},{24,16},{1,25},{9,1},{17,9},{25,17},{2,26},{10... | collective-permute-start | bytes 294920 | tf_op jit(solution)/shard_map/ppermute | solution.py:40
  68.7 1.3 collective-permute-start.9
  70.1 0.2 collective-permute-done.10
  70.4 4.5 %collective-permute-done.8 = bf16[32,1536]{1,0:T(8,128)(2,1)S(1)} collective-permute-done((bf16[32,1536]{1,0:T(8,128)(2,1)S(1)}, bf16[32,1536]{1,0:T(8,128)(2,1)S(1)}, u32[]{:S(2)}, u32[]{:S(2)}) %collective-permute-start.8) | collective-permute-done | bytes 98336 | tf_op jit(solution)/shard_map/ppermute | solution.py:40
  74.9 0.2 fusion.56
  75.1 0.5 convolution_convert_fusion.2
  75.7 14.6 %all_to_all.30 = bf16[8,32,512]{2,1,0:T(8,128)(2,1)S(1)} all-to-all(bf16[8,32,512]{2,1,0:T(8,128)(2,1)S(1)} %broadcast_in_dim.15), channel_id=1, replica_groups=mesh['z'=8,'y'=4,'x'=4,'c'=2] {'x','c'}, dimensions={0} | all-to-all | bytes 524288 | tf_op jit(solution)/shard_map/all_to_all | solution.py:25
  90.3 0.1 fusion.29
  90.6 1.9 %fusion.3 = f32[32,1664]{1,0:T(8,128)S(1)} fusion(bf16[32,512]{1,0:T(8,128)(2,1)S(1)} %get-tuple-element.29, bf16[512,2176]{1,0:T(8,128)(2,1)} %all-gather.5.cloned.1.call-done), kind=kOutput, calls=%fused_computation.9 | convolution fusion | flops 54525952 | bytes 1949696 | tf_op jit(solution)/shard_map/dot_general | solution.py:142
  92.6 8.0 %all_to_all.31.arrived_ref = bf16[4,8,1664]{2,1,0:T(8,128)(2,1)S(1)} all-to-all(bf16[4,8,1664]{2,1,0:T(8,128)(2,1)S(1)} %pad_maximum_fusion.5), channel_id=1, replica_groups=mesh['z'=8,'y'=4,'x'=4,'c'=2] {'y'}, dimensions={0} | all-to-all | bytes 212992 | tf_op jit(solution)/shard_map/all_to_all | solution.py:25
  100.6 2.2 %shard_map.266 = (bf16[4,8,512]{2,1,0:T(8,128)(2,1)S(1)}, f32[8,4,128,128]{3,2,1,0:T(8,128)}) custom-call(bf16[4,8,1664]{2,1,0:T(8,128)(2,1)S(1)} %all_to_all.31.arrived_ref, f32[1,4]{1,0:T(1,128)S(1)} %bitcast.91, f32[1,4]{1,0:T(1,128)S(1)} %bitcast.92, f32[1,128]{1,0:T(1,128)S(1)} %bitcast.93, f32[8,4,128,128]{3,2,1,0:T(8,128)S(1)} %copy-done), custom_call_target="tpu_custom_call" | custom-call | flops 20000000 | bytes 4200000 | tf_op jit(solution)/shard_map/pallas_call | solution.py:149
  102.8 6.7 %all_to_all.32 = bf16[4,8,512]{2,1,0:T(8,128)(2,1)S(1)} all-to-all(bf16[4,8,512]{2,1,0:T(8,128)(2,1)S(1)} %get-tuple-element.26), channel_id=1, replica_groups=mesh['z'=8,'y'=4,'x'=4,'c'=2] {'y'}, dimensions={0} | all-to-all | bytes 65536 | tf_op jit(solution)/shard_map/all_to_all | solution.py:25
  109.5 1.3 convolution_convert_fusion.4
  110.9 12.4 %all_to_all.33 = bf16[8,32,512]{2,1,0:T(8,128)(2,1)S(1)} all-to-all(bf16[8,32,512]{2,1,0:T(8,128)(2,1)S(1)} %broadcast_in_dim.36), channel_id=1, replica_groups=mesh['z'=8,'y'=4,'x'=4,'c'=2] {'x','c'}, dimensions={0} | all-to-all | bytes 524288 | tf_op jit(solution)/shard_map/all_to_all | solution.py:25
  123.3 0.1 multiply_reduce_fusion
  123.6 1.7 %convolution_convert_fusion = bf16[32,1408]{1,0:T(8,128)(2,1)S(1)} fusion(bf16[512,2112]{1,0:T(8,128)(2,1)} %all-gather.3.cloned.1.call-done, f32[32,512]{1,0:T(8,128)S(1)} %convert_reduce_fusion, bf16[32,512]{1,0:T(8,128)(2,1)S(1)} %get-tuple-element.29), kind=kOutput, calls=%fused_computation.8 | convolution fusion | flops 46231552 | bytes 1630208 | tf_op jit(solution)/shard_map/dot_general | solution.py:265
  125.3 0.4 collective-permute-start.11
  125.7 1.8 %collective-permute-start.12 = (bf16[32,1536]{1,0:T(8,128)(2,1)S(1)}, bf16[32,1536]{1,0:T(8,128)(2,1)S(1)}, u32[]{:S(2)}, u32[]{:S(2)}) collective-permute-start(bf16[32,1536]{1,0:T(8,128)(2,1)S(1)} %pad_maximum_fusion.7), channel_id=1, source_target_pairs={{0,16},{8,24},{16,0},{24,8},{1,17},{9,25},{17,1},{25,9},{2,18},{10... | collective-permute-start | bytes 294920 | tf_op jit(solution)/shard_map/ppermute | solution.py:40
  127.5 0.8 collective-permute-start.13
  128.3 3.2 %collective-permute-done.11 = bf16[32,1536]{1,0:T(8,128)(2,1)S(1)} collective-permute-done((bf16[32,1536]{1,0:T(8,128)(2,1)S(1)}, bf16[32,1536]{1,0:T(8,128)(2,1)S(1)}, u32[]{:S(2)}, u32[]{:S(2)}) %collective-permute-start.11) | collective-permute-done | bytes 98336 | tf_op jit(solution)/shard_map/ppermute | solution.py:40
  131.5 0.9 collective-permute-done.13
  132.5 0.2 fusion.51
  132.6 1.5 convolution_convert_fusion.1
  134.2 0.1 copy.59
  134.3 0.2 reshape.80
  134.4 17.6 %all_to_all.34 = bf16[64,2,256]{2,1,0:T(2,128)(2,1)S(1)} all-to-all(bf16[64,2,256]{2,1,0:T(2,128)(2,1)S(1)} %reshape.80), channel_id=1, replica_groups=mesh['z'=8,'y'=4,'x'=4,'c'=2] {'z','x','c'}, dimensions={0} | all-to-all | bytes 131072 | tf_op jit(solution)/shard_map/all_to_all | solution.py:25
  152.0 0.1 reshape.81
  152.3 0.7 convert_element_type.231
  (82 shorter events, 1.2 us)
Async XLA Ops:
  7.2 26.2 %copy-start.4 = (bf16[704,64]{0,1:T(8,128)(2,1)S(1)}, bf16[704,64]{0,1:T(8,128)(2,1)}, u32[]{:S(2)}) copy-start(bf16[704,64]{0,1:T(8,128)(2,1)} %param.32) | copy-start | bytes 270340
  7.2 21.6 %copy-start.8 = (bf16[512,64]{0,1:T(8,128)(2,1)S(1)}, bf16[512,64]{0,1:T(8,128)(2,1)}, u32[]{:S(2)}) copy-start(bf16[512,64]{0,1:T(8,128)(2,1)} %param.43) | copy-start | bytes 196612
  7.2 22.4 %copy-start.13 = (f32[64]{0:T(128)S(1)}, f32[64]{0:T(128)}, u32[]{:S(2)}) copy-start(f32[64]{0:T(128)} %param.44) | copy-start | bytes 772
  7.2 22.4 %copy-start.6 = (bf16[64,704]{1,0:T(8,128)(2,1)S(1)}, bf16[64,704]{1,0:T(8,128)(2,1)}, u32[]{:S(2)}) copy-start(bf16[64,704]{1,0:T(8,128)(2,1)} %param.45) | copy-start | bytes 270340
  7.2 22.4 %copy-start.5 = (bf16[64,704]{1,0:T(8,128)(2,1)S(1)}, bf16[64,704]{1,0:T(8,128)(2,1)}, u32[]{:S(2)}) copy-start(bf16[64,704]{1,0:T(8,128)(2,1)} %param.46) | copy-start | bytes 270340
  7.2 25.4 %copy-start.7 = (bf16[704,64]{0,1:T(8,128)(2,1)S(1)}, bf16[704,64]{0,1:T(8,128)(2,1)}, u32[]{:S(2)}) copy-start(bf16[704,64]{0,1:T(8,128)(2,1)} %param.47) | copy-start | bytes 270340
  9.3 17.6 %collective-permute-start = (bf16[64,2112]{1,0:T(8,128)(2,1)S(1)}, bf16[64,2112]{1,0:T(8,128)(2,1)S(1)}, u32[]{:S(2)}, u32[]{:S(2)}) collective-permute-start(bf16[64,2112]{1,0:T(8,128)(2,1)S(1)} %pad_maximum_fusion), channel_id=1, source_target_pairs={{0,224},{32,0},{64,32},{96,64},{128,96},{160,128},{192,160},{224,1... | collective-permute-start | bytes 811016 | tf_op jit(solution)/shard_map/ppermute | solution.py:66
  15.8 11.2 %collective-permute-start.3 = (bf16[64,2112]{1,0:T(8,128)(2,1)S(1)}, bf16[64,2112]{1,0:T(8,128)(2,1)S(1)}, u32[]{:S(2)}, u32[]{:S(2)}) collective-permute-start(bf16[64,2112]{1,0:T(8,128)(2,1)S(1)} %pad_maximum_fusion), channel_id=1, source_target_pairs={{0,32},{32,64},{64,96},{96,128},{128,160},{160,192},{192,224},{224... | collective-permute-start | bytes 811016 | tf_op jit(solution)/shard_map/ppermute | solution.py:65
  17.3 17.9 %all-to-all-start = ((bf16[64,2,128]{2,1,0:T(2,128)(2,1)}), bf16[64,2,128]{2,1,0:T(2,128)(2,1)S(1)}, u32[]{:S(2)}, u32[]{:S(2)}) async-start(bf16[64,2,128]{2,1,0:T(2,128)(2,1)} %reshape.78), calls=%async_computation | async-start | bytes 65536 | tf_op jit(solution)/shard_map/all_to_all | solution.py:25
  25.9 64.7 %all-gather.5.cloned.1.call-start = ((), (), s32[]{:S(2)}) async-start(), calls=%async_computation.7 | async-start | bytes 2506752 | tf_op jit(solution)/shard_map/all_gather | solution.py:197
  29.5 94.0 %all-gather.3.cloned.1.call-start = ((), (), s32[]{:S(2)}) async-start(), calls=%async_computation.6 | async-start | bytes 2506752 | tf_op jit(solution)/shard_map/all_gather | solution.py:197
  29.7 8.5 %collective-permute-start.1 = (bf16[64,2112]{1,0:T(8,128)(2,1)S(1)}, bf16[64,2112]{1,0:T(8,128)(2,1)S(1)}, u32[]{:S(2)}, u32[]{:S(2)}) collective-permute-start(bf16[64,2112]{1,0:T(8,128)(2,1)S(1)} %collective-permute-done), channel_id=1, source_target_pairs={{0,224},{32,0},{64,32},{96,64},{128,96},{160,128},{192,160},{224,1... | collective-permute-start | bytes 811016 | tf_op jit(solution)/shard_map/ppermute | solution.py:66
  32.6 9.0 %collective-permute-start.4 = (bf16[64,2112]{1,0:T(8,128)(2,1)S(1)}, bf16[64,2112]{1,0:T(8,128)(2,1)S(1)}, u32[]{:S(2)}, u32[]{:S(2)}) collective-permute-start(bf16[64,2112]{1,0:T(8,128)(2,1)S(1)} %collective-permute-done.3), channel_id=1, source_target_pairs={{0,32},{32,64},{64,96},{96,128},{128,160},{160,192},{192,224},{224... | collective-permute-start | bytes 811016 | tf_op jit(solution)/shard_map/ppermute | solution.py:65
  38.2 14.0 %collective-permute-start.2 = (bf16[64,2112]{1,0:T(8,128)(2,1)S(1)}, bf16[64,2112]{1,0:T(8,128)(2,1)S(1)}, u32[]{:S(2)}, u32[]{:S(2)}) collective-permute-start(bf16[64,2112]{1,0:T(8,128)(2,1)S(1)} %collective-permute-done.1), channel_id=1, source_target_pairs={{0,224},{32,0},{64,32},{96,64},{128,96},{160,128},{192,160},{224,1... | collective-permute-start | bytes 811016 | tf_op jit(solution)/shard_map/ppermute | solution.py:66
  41.7 14.3 %collective-permute-start.5 = (bf16[64,2112]{1,0:T(8,128)(2,1)S(1)}, bf16[64,2112]{1,0:T(8,128)(2,1)S(1)}, u32[]{:S(2)}, u32[]{:S(2)}) collective-permute-start(bf16[64,2112]{1,0:T(8,128)(2,1)S(1)} %collective-permute-done.4), channel_id=1, source_target_pairs={{0,32},{32,64},{64,96},{96,128},{128,160},{160,192},{192,224},{224... | collective-permute-start | bytes 811016 | tf_op jit(solution)/shard_map/ppermute | solution.py:65
  41.7 14.4 %copy-start.9 = (bf16[512,704]{1,0:T(8,128)(2,1)}, bf16[512,704]{1,0:T(8,128)(2,1)S(1)}, u32[]{:S(2)}) copy-start(bf16[512,704]{1,0:T(8,128)(2,1)S(1)} %slice_dynamic-update-slice_fusion.2) | copy-start | bytes 2162692
  55.9 8.8 %collective-permute-start.7 = (bf16[64,1088]{1,0:T(8,128)(2,1)S(1)}, bf16[64,1088]{1,0:T(8,128)(2,1)S(1)}, u32[]{:S(2)}, u32[]{:S(2)}) collective-permute-start(bf16[64,1088]{1,0:T(8,128)(2,1)S(1)} %slice.189), channel_id=1, source_target_pairs={{0,224},{32,0},{64,32},{96,64},{128,96},{160,128},{192,160},{224,1... | collective-permute-start | bytes 417800 | tf_op jit(solution)/shard_map/ppermute | solution.py:69
  56.0 8.7 %collective-permute-start.6 = (bf16[64,1024]{1,0:T(8,128)(2,1)S(1)}, bf16[64,1024]{1,0:T(8,128)(2,1)S(1)}, u32[]{:S(2)}, u32[]{:S(2)}) collective-permute-start(bf16[64,1024]{1,0:T(8,128)(2,1)S(1)} %slice.188), channel_id=1, source_target_pairs={{0,32},{32,64},{64,96},{96,128},{128,160},{160,192},{192,224},{224... | collective-permute-start | bytes 393224 | tf_op jit(solution)/shard_map/ppermute | solution.py:68
  57.7 2.4 %copy-start.11 = (f32[128]{0:T(128)S(1)}, f32[128]{0:T(128)}, u32[]{:S(2)}) copy-start(f32[128]{0:T(128)} %constant.59) | copy-start | bytes 1540
  57.7 2.4 %copy-start.12 = (f32[128]{0:T(128)S(1)}, f32[128]{0:T(128)}, u32[]{:S(2)}) copy-start(f32[128]{0:T(128)} %constant.60) | copy-start | bytes 1540
  58.8 11.3 %copy-start.10 = (bf16[512,704]{1,0:T(8,128)(2,1)S(1)}, bf16[512,704]{1,0:T(8,128)(2,1)}, u32[]{:S(2)}) copy-start(bf16[512,704]{1,0:T(8,128)(2,1)} %slice_dynamic-update-slice_fusion.5) | copy-start | bytes 2162692
  65.0 5.4 %collective-permute-start.10 = (bf16[32,1536]{1,0:T(8,128)(2,1)S(1)}, bf16[32,1536]{1,0:T(8,128)(2,1)S(1)}, u32[]{:S(2)}, u32[]{:S(2)}) collective-permute-start(bf16[32,1536]{1,0:T(8,128)(2,1)S(1)} %pad_maximum_fusion.6), channel_id=1, source_target_pairs={{0,24},{8,0},{16,8},{24,16},{1,25},{9,1},{17,9},{25,17},{2,26},{10... | collective-permute-start | bytes 294920 | tf_op jit(solution)/shard_map/ppermute | solution.py:40
  68.7 6.1 %collective-permute-start.8 = (bf16[32,1536]{1,0:T(8,128)(2,1)S(1)}, bf16[32,1536]{1,0:T(8,128)(2,1)S(1)}, u32[]{:S(2)}, u32[]{:S(2)}) collective-permute-start(bf16[32,1536]{1,0:T(8,128)(2,1)S(1)} %pad_maximum_fusion.6), channel_id=1, source_target_pairs={{0,8},{8,16},{16,24},{24,0},{1,9},{9,17},{17,25},{25,1},{2,10},{10... | collective-permute-start | bytes 294920 | tf_op jit(solution)/shard_map/ppermute | solution.py:40
  68.7 6.1 %collective-permute-start.9 = (bf16[32,1536]{1,0:T(8,128)(2,1)S(1)}, bf16[32,1536]{1,0:T(8,128)(2,1)S(1)}, u32[]{:S(2)}, u32[]{:S(2)}) collective-permute-start(bf16[32,1536]{1,0:T(8,128)(2,1)S(1)} %pad_maximum_fusion.6), channel_id=1, source_target_pairs={{0,16},{8,24},{16,0},{24,8},{1,17},{9,25},{17,1},{25,9},{2,18},{10... | collective-permute-start | bytes 294920 | tf_op jit(solution)/shard_map/ppermute | solution.py:40
  75.6 24.9 %copy-start = (f32[8,4,128,128]{3,2,1,0:T(8,128)S(1)}, f32[8,4,128,128]{3,2,1,0:T(8,128)}, u32[]{:S(2)}) copy-start(f32[8,4,128,128]{3,2,1,0:T(8,128)} %state_ref.1) | copy-start | bytes 6291460
  75.6 24.9 %copy-start.1 = (f32[4]{0:T(128)S(1)}, f32[4]{0:T(128)}, u32[]{:S(2)}) copy-start(f32[4]{0:T(128)} %param.40) | copy-start | bytes 52
  75.7 24.9 %copy-start.2 = (f32[4]{0:T(128)S(1)}, f32[4]{0:T(128)}, u32[]{:S(2)}) copy-start(f32[4]{0:T(128)} %param.41) | copy-start | bytes 52
  75.7 24.9 %copy-start.3 = (f32[128]{0:T(128)S(1)}, f32[128]{0:T(128)}, u32[]{:S(2)}) copy-start(f32[128]{0:T(128)} %param.42) | copy-start | bytes 1540
  125.3 6.2 %collective-permute-start.11 = (bf16[32,1536]{1,0:T(8,128)(2,1)S(1)}, bf16[32,1536]{1,0:T(8,128)(2,1)S(1)}, u32[]{:S(2)}, u32[]{:S(2)}) collective-permute-start(bf16[32,1536]{1,0:T(8,128)(2,1)S(1)} %pad_maximum_fusion.7), channel_id=1, source_target_pairs={{0,8},{8,16},{16,24},{24,0},{1,9},{9,17},{17,25},{25,1},{2,10},{10... | collective-permute-start | bytes 294920 | tf_op jit(solution)/shard_map/ppermute | solution.py:40
  125.7 5.8 %collective-permute-start.12 = (bf16[32,1536]{1,0:T(8,128)(2,1)S(1)}, bf16[32,1536]{1,0:T(8,128)(2,1)S(1)}, u32[]{:S(2)}, u32[]{:S(2)}) collective-permute-start(bf16[32,1536]{1,0:T(8,128)(2,1)S(1)} %pad_maximum_fusion.7), channel_id=1, source_target_pairs={{0,16},{8,24},{16,0},{24,8},{1,17},{9,25},{17,1},{25,9},{2,18},{10... | collective-permute-start | bytes 294920 | tf_op jit(solution)/shard_map/ppermute | solution.py:40
  127.5 4.9 %collective-permute-start.13 = (bf16[32,1536]{1,0:T(8,128)(2,1)S(1)}, bf16[32,1536]{1,0:T(8,128)(2,1)S(1)}, u32[]{:S(2)}, u32[]{:S(2)}) collective-permute-start(bf16[32,1536]{1,0:T(8,128)(2,1)S(1)} %pad_maximum_fusion.7), channel_id=1, source_target_pairs={{0,24},{8,0},{16,8},{24,16},{1,25},{9,1},{17,9},{25,17},{2,26},{10... | collective-permute-start | bytes 294920 | tf_op jit(solution)/shard_map/ppermute | solution.py:40
Sparse Core Ops, SparseCore 0:
  29.6 45.9 all-gather.4
  77.4 37.6 all-gather.2

commit v4 on v3

--- a/solution.py
+++ b/solution.py
@@ -11,6 +11,7 @@
 D = 2048
 HEAD = 128
 GATES = 128
+HEADS_DEV = 4
 
 epsilon = 1e-06
 
@@ -87,14 +88,14 @@
 
 
 def mixer_kernel(
-    arrived_ref, rate_ref, bias_ref, gain_ref, state_ref, out_ref, new_ref, made, read_ref, went
+    own_ref, near_ref, far_ref, last_ref, rate_ref, bias_ref, gain_ref, state_ref, out_ref, new_ref, made, read_ref, went
 ):
     count, heads = state_ref.shape[:2]
     pairs = heads // 2
     store = [pltpu.make_async_copy(made.at[s], new_ref.at[s], went.at[s]) for s in range(count)]
-    summed = arrived_ref[0].astype(f32)
-    for i in range(1, arrived_ref.shape[0]):
-        summed = summed + arrived_ref[i].astype(f32)
+    summed = own_ref[...].astype(f32)
+    for ref in (near_ref, far_ref, last_ref):
+        summed = summed + ref[...].astype(f32)
     width = summed.shape[1] - GATES
     tail = summed[:, width:]
     scale = row_scale(tail[:, 2 * heads : 2 * heads + 2])
@@ -144,15 +145,21 @@
     squares = square_columns(residual.astype(f32))
     tail = projected[:, width:] + jnp.roll(squares, 2 * heads_dev, axis=1)
     both = jnp.concatenate([projected[:, :width], tail], axis=1).astype(bf16)
-    arrived = exchange(both.reshape(-1, row_count, both.shape[1]), "y")
+    size = lax.axis_size("y")
+    blocks = both.reshape(size, row_count, both.shape[1])
+    blocks = jnp.concatenate([blocks, blocks], axis=0)
+    blocks = lax.dynamic_slice_in_dim(blocks, lax.axis_index("y"), size, 0)
+    parts = [blocks[0]]
+    for places in range(1, size):
+        parts.append(lax.ppermute(blocks[places], "y", [(i, (i + places) % size) for i in range(size)]))
     whole = pl.BlockSpec(memory_space=pltpu.VMEM)
     return pl.pallas_call(
         mixer_kernel,
         out_shape=(
-            jax.ShapeDtypeStruct((arrived.shape[0], row_count, heads_dev * head_size), bf16),
+            jax.ShapeDtypeStruct((size, row_count, heads_dev * head_size), bf16),
             jax.ShapeDtypeStruct(old_state.shape, f32),
         ),
-        in_specs=[whole] * 5,
+        in_specs=[whole] * 8,
         out_specs=(whole, pl.BlockSpec(memory_space=pl.ANY)),
         scratch_shapes=[
             pltpu.VMEM(old_state.shape, f32),
@@ -161,7 +168,38 @@
         ],
         compiler_params=pltpu.CompilerParams(vmem_limit_bytes=16 * 1024 * 1024),
         cost_estimate=pl.CostEstimate(flops=20_000_000, bytes_accessed=4_200_000, transcendentals=20_000),
-    )(arrived, decay_rate[None, :], decay_bias[None, :], head_gain[None, :], old_state)
+    )(*parts, decay_rate[None, :], decay_bias[None, :], head_gain[None, :], old_state)
+
+
+def pack_kernel(
+    start_ref, gains_ref, gate_ref, up_ref, down_ref, query_ref, key_ref, value_ref, out_gate_ref,
+    beta_ref, decay_ref, out_ref, first_ref, middle_ref,
+):
+    count = gate_ref.shape[0]
+    at = lambda shape, dim: lax.broadcasted_iota(jnp.int32, shape, dim)
+    diagonal = at((count, count), 0) == at((count, count), 1)
+    gain = lambda i: jnp.sum(jnp.where(diagonal, gains_ref[i : i + 1, :], 0.0), axis=1, keepdims=True)
+    first_gain, mixer_gain = gain(0), gain(1)
+    scaled = lambda ref, column: (ref[...].astype(f32) * column).astype(bf16)
+    width = gate_ref.shape[1]
+    first_ref[:, :width] = scaled(gate_ref, first_gain)
+    first_ref[:, width : 2 * width] = scaled(up_ref, first_gain)
+    first_ref[:, 2 * width :] = down_ref[...]
+    place = 0
+    for ref in (query_ref, key_ref, value_ref, out_gate_ref):
+        middle_ref[:, place : place + ref.shape[1]] = scaled(ref, mixer_gain)
+        place += ref.shape[1]
+    shape = (beta_ref.shape[0], GATES)
+    head, lane = at(shape, 0), at(shape, 1)
+    heads = HEADS_DEV
+    picked = jnp.zeros((count, GATES), f32)
+    for i, ref in enumerate((beta_ref, decay_ref)):
+        own = (lane >= i * heads) & (lane < (i + 1) * heads) & (head == start_ref[0] + lane - i * heads)
+        picked = picked + lax.dot_general(
+            ref[...], own.astype(bf16), (((0,), (0,)), ((), ())), preferred_element_type=f32
+        )
+    middle_ref[:, place : place + GATES] = (picked * mixer_gain).astype(bf16)
+    middle_ref[:, place + GATES :] = out_ref[...]
 
 
 def body(
@@ -196,22 +234,35 @@
     def gathered(weights):
         return lax.all_gather(jnp.concatenate(weights, axis=1), "z", axis=0, tiled=True)
 
-    head_start = lax.axis_index(TP) * heads_dev
-    gate_cols = [
-        lax.dynamic_slice_in_dim(beta_weight, head_start, heads_dev, 1),
-        lax.dynamic_slice_in_dim(decay_weight, head_start, heads_dev, 1),
-        jnp.zeros((beta_weight.shape[0], GATES - 2 * heads_dev), bf16),
-    ]
-    first_in = scaled_rows(norm_gain_first, [gate_first, up_first])
-    width = first_in.shape[1]
-    first_blocks = around(jnp.concatenate([first_in, down_first.T], axis=1), "z")
-    first_blocks[1], first_blocks[-1], query_weight, out_weight = lax.optimization_barrier(
-        (first_blocks[1], first_blocks[-1], query_weight, out_weight)
-    )
-    mixer_in = scaled_rows(norm_gain_mixer, [query_weight, key_weight, value_weight, output_gate_weight, *gate_cols])
+    width = 2 * gate_first.shape[1]
+    mixer_width = 2 * query_weight.shape[1] + 2 * value_weight.shape[1] + GATES
+    whole = pl.BlockSpec(memory_space=pltpu.VMEM)
+    first, middle = pl.pallas_call(
+        pack_kernel,
+        out_shape=(
+            jax.ShapeDtypeStruct((gate_first.shape[0], width + down_first.shape[0]), bf16),
+            jax.ShapeDtypeStruct((gate_first.shape[0], mixer_width + out_weight.shape[0]), bf16),
+        ),
+        in_specs=[pl.BlockSpec(memory_space=pltpu.SMEM)] + [whole] * 11,
+        out_specs=(whole, whole),
+        compiler_params=pltpu.CompilerParams(vmem_limit_bytes=60 * 1024 * 1024),
+        cost_estimate=pl.CostEstimate(flops=20_000_000, bytes_accessed=1_100_000, transcendentals=0),
+    )(
+        (lax.axis_index(TP) * heads_dev).reshape(1),
+        jnp.stack([norm_gain_first, norm_gain_mixer]),
+        gate_first,
+        up_first,
+        down_first.T,
+        query_weight,
+        key_weight,
+        value_weight,
+        output_gate_weight,
+        beta_weight.T,
+        decay_weight.T,
+        out_weight.T,
+    )
+    first_blocks = around(first, "z")
     second_in = scaled_rows(norm_gain_second, [gate_second, up_second])
-    mixer_width = mixer_in.shape[1]
-    middle = jnp.concatenate([mixer_in, out_weight.T], axis=1)
     last = jnp.concatenate([second_in, down_second.T], axis=1)
     columns = residual_in.T
     own_cols, rows = columns.shape[0], columns.shape[1] // planes

time: 161 us -> 165 us (1.025)
  blocking collectives: 59.3 us -> 42.5 us
  starting transfers between devices: 31.1 us -> 45.1 us
  waiting for transfers between devices: 32.5 us -> 35.2 us
  local copies, waits for them, and re-layouts: 5.78 us -> 7.97 us
  Pallas kernels: 2.23 us -> 4.32 us
    all_to_all x5 -> x3, blocking collectives: 59.3 us -> 42.5 us  [exchange(): return lax.all_to_all(blocks, axis, split_axis=0, concat_axis=0, tiled=True)]
    all_to_all x1 -> x2, starting transfers between devices: 8.6 us -> 18.2 us  [exchange(): return lax.all_to_all(blocks, axis, split_axis=0, concat_axis=0, tiled=True)]
    all_to_all x1 -> x2, waiting for transfers between devices: 1.9 us -> 7.79 us  [exchange(): return lax.all_to_all(blocks, axis, split_axis=0, concat_axis=0, tiled=True)]
    ppermute x6, waiting for transfers between devices: 8.85 us -> 4.22 us  [ring_sum(): lax.ppermute(value, axis, [(i, (i + places) % size) for i in range(size)])]
    ppermute x0 -> x3, starting transfers between devices: none -> 3.63 us  [mixer_values(): lax.ppermute(blocks[places], 'y', [(i, (i + places) % size) for i in rang...]
    ppermute x3, waiting for transfers between devices: 13.4 us -> 10.1 us  [around(): backward = blocks[step] = lax.ppermute(backward, axis, behind)]
    ppermute x0 -> x3, waiting for transfers between devices: none -> 3.19 us  [mixer_values(): lax.ppermute(blocks[places], 'y', [(i, (i + places) % size) for i in rang...]
    unnamed x39 -> x27, local copies, waits for them, and re-layouts: 1.93 us -> 4.71 us
  transfers between devices with their start and end apart: 17 -> 21, of which waited for: 9 -> 12; matrix products, arithmetic and copies ran while one was open for 8% -> 10% of each run, Pallas kernels for 1% -> 1%
where the time goes in v4:
time: 165 us
  starting transfers between devices  45.1 us (27%)
  blocking collectives  42.5 us (26%)
  waiting for transfers between devices  35.2 us (21%)
  between operations  14.4 us (9%)
  matrix products  9.59 us (6%)
  local copies, waits for them, and re-layouts  7.97 us (5%)
  other arithmetic  5.56 us (3%)
  Pallas kernels  4.32 us (3%)
    all_to_all x3, blocking collectives, exchange(): return lax.all_to_all(blocks, axis, split_axis=0, concat_axis=0, tiled=True)  42.5 us
    all_to_all x2, starting transfers between devices, exchange(): return lax.all_to_all(blocks, axis, split_axis=0, concat_axis=0, tiled=True)  18.2 us
    ppermute x3, starting transfers between devices, around(): backward = blocks[step] = lax.ppermute(backward, axis, behind)  12.7 us
    ppermute x3, waiting for transfers between devices, around(): backward = blocks[step] = lax.ppermute(backward, axis, behind)  10.1 us
    ppermute x6, starting transfers between devices, ring_sum(): lax.ppermute(value, axis, [(i, (i + places) % size) for i in range(size)])  8.96 us
    all_to_all x2, waiting for transfers between devices, exchange(): return lax.all_to_all(blocks, axis, split_axis=0, concat_axis=0, tiled=True)  7.79 us
    ppermute x1, waiting for transfers between devices, around(): forward = lax.ppermute(forward[:, :half], axis, ahead)  5.62 us
    unnamed x27, local copies, waits for them, and re-layouts  4.71 us
  transfers between devices with their start and end apart: 21, of which 12 were waited for; matrix products, arithmetic and copies ran while one was open for 10% of the time, Pallas kernels for 1%

profile of v4, /device:TPU:1, one launch (start us, length us, event | category | flops | bytes accessed | tf_op | source)
XLA Modules:
  0.0 164.7 jit_solution(5820742804681391891)
XLA Ops:
  7.2 1.2 pad_maximum_fusion.6.gains_ref
  8.4 2.1 %shard_map.266 = (bf16[64,2112]{1,0:T(8,128)(2,1)}, bf16[64,2176]{1,0:T(8,128)(2,1)}) custom-call(s32[1]{0:T(128)} %bitcast.start_ref, f32[2,64]{1,0:T(2,128)} %pad_maximum_fusion.6.gains_ref, bf16[64,704]{1,0:T(8,128)(2,1)} %gate_ref.1, bf16[64,704]{1,0:T(8,128)(2,1)} %up_ref.1, bf16[64,704]{1,0:T(8,128)(2,1)} %bitcast.109, bf16[64,256]{1,0:T(8,128)(2,1)} %query_ref.1, ...), custom_call_target="tpu_custom_call" | custom-call | flops 20000000 | bytes 1100000 | tf_op jit(solution)/shard_map/pallas_call | solution.py:240
  10.5 6.4 %collective-permute-start = (bf16[64,2112]{1,0:T(8,128)(2,1)}, bf16[64,2112]{1,0:T(8,128)(2,1)S(1)}, u32[]{:S(2)}, u32[]{:S(2)}) collective-permute-start(bf16[64,2112]{1,0:T(8,128)(2,1)} %get-tuple-element.13), channel_id=1, source_target_pairs={{0,224},{32,0},{64,32},{96,64},{128,96},{160,128},{192,160},{224,1... | collective-permute-start | bytes 811016 | tf_op jit(solution)/shard_map/ppermute | solution.py:67
  16.9 0.8 reshape.70
  17.7 0.7 reshape.80
  18.5 8.6 %all-to-all-start = ((bf16[64,2,128]{2,1,0:T(2,128)(2,1)}), bf16[64,2,128]{2,1,0:T(2,128)(2,1)S(1)}, u32[]{:S(2)}, u32[]{:S(2)}) async-start(bf16[64,2,128]{2,1,0:T(2,128)(2,1)} %reshape.80), calls=%async_computation | async-start | bytes 65536 | tf_op jit(solution)/shard_map/all_to_all | solution.py:26
  27.1 0.7 all-gather.5.cloned.1.call-update
  27.8 1.0 multiply_convert_fusion
  28.9 2.9 %collective-permute-start.1 = (bf16[64,2112]{1,0:T(8,128)(2,1)S(1)}, bf16[64,2112]{1,0:T(8,128)(2,1)S(1)}, u32[]{:S(2)}, u32[]{:S(2)}) collective-permute-start(bf16[64,2112]{1,0:T(8,128)(2,1)S(1)} %collective-permute-done), channel_id=1, source_target_pairs={{0,224},{32,0},{64,32},{96,64},{128,96},{160,128},{192,160},{224,1... | collective-permute-start | bytes 811016 | tf_op jit(solution)/shard_map/ppermute | solution.py:67
  31.8 1.6 pad_maximum_fusion
  33.4 0.9 slice_dynamic-update-slice_fusion.7
  34.3 2.1 %all-to-all-done = bf16[64,2,128]{2,1,0:T(2,128)(2,1)S(1)} async-done(((bf16[64,2,128]{2,1,0:T(2,128)(2,1)}), bf16[64,2,128]{2,1,0:T(2,128)(2,1)S(1)}, u32[]{:S(2)}, u32[]{:S(2)}) %all-to-all-start) | async-done | bytes 32800 | tf_op jit(solution)/shard_map/all_to_all | solution.py:26
  36.5 0.9 collective-permute-done.1
  37.4 3.4 %collective-permute-start.2 = (bf16[64,2112]{1,0:T(8,128)(2,1)S(1)}, bf16[64,2112]{1,0:T(8,128)(2,1)S(1)}, u32[]{:S(2)}, u32[]{:S(2)}) collective-permute-start(bf16[64,2112]{1,0:T(8,128)(2,1)S(1)} %collective-permute-done.1), channel_id=1, source_target_pairs={{0,224},{32,0},{64,32},{96,64},{128,96},{160,128},{192,160},{224,1... | collective-permute-start | bytes 811016 | tf_op jit(solution)/shard_map/ppermute | solution.py:67
  40.9 9.2 %collective-permute-done.2 = bf16[64,2112]{1,0:T(8,128)(2,1)S(1)} collective-permute-done((bf16[64,2112]{1,0:T(8,128)(2,1)S(1)}, bf16[64,2112]{1,0:T(8,128)(2,1)S(1)}, u32[]{:S(2)}, u32[]{:S(2)}) %collective-permute-start.2) | collective-permute-done | bytes 270368 | tf_op jit(solution)/shard_map/ppermute | solution.py:67
  50.1 2.8 %collective-permute-done.5 = bf16[64,2112]{1,0:T(8,128)(2,1)S(1)} collective-permute-done((bf16[64,2112]{1,0:T(8,128)(2,1)S(1)}, bf16[64,2112]{1,0:T(8,128)(2,1)S(1)}, u32[]{:S(2)}, u32[]{:S(2)}) %collective-permute-start.5) | collective-permute-done | bytes 270368 | tf_op jit(solution)/shard_map/ppermute | solution.py:66
  53.0 0.2 fusion.23
  53.2 0.2 fusion.21
  53.4 0.8 collective-permute-start.7
  54.2 0.8 collective-permute-start.6
  55.3 0.7 slice_dynamic-update-slice_fusion.6
  56.0 0.2 fusion.15
  56.2 0.2 convolution_add_fusion.4
  56.4 0.2 convolution_add_fusion.3
  56.7 0.2 fusion.1
  56.9 0.2 convolution_add_fusion.1
  57.1 5.6 %collective-permute-done.6 = bf16[64,1024]{1,0:T(8,128)(2,1)S(1)} collective-permute-done((bf16[64,1024]{1,0:T(8,128)(2,1)S(1)}, bf16[64,1024]{1,0:T(8,128)(2,1)S(1)}, u32[]{:S(2)}, u32[]{:S(2)}) %collective-permute-start.6) | collective-permute-done | bytes 131104 | tf_op jit(solution)/shard_map/ppermute | solution.py:69
  62.7 0.2 fusion.2
  63.0 3.7 %collective-permute-start.10 = (bf16[32,1536]{1,0:T(8,128)(2,1)S(1)}, bf16[32,1536]{1,0:T(8,128)(2,1)S(1)}, u32[]{:S(2)}, u32[]{:S(2)}) collective-permute-start(bf16[32,1536]{1,0:T(8,128)(2,1)S(1)} %pad_maximum_fusion.3), channel_id=1, source_target_pairs={{0,24},{8,0},{16,8},{24,16},{1,25},{9,1},{17,9},{25,17},{2,26},{10... | collective-permute-start | bytes 294920 | tf_op jit(solution)/shard_map/ppermute | solution.py:41
  66.6 1.3 collective-permute-start.9
  67.9 0.6 slice_dynamic-update-slice_fusion.2
  68.5 0.6 slice_dynamic-update-slice_fusion.5
  69.2 0.6 slice_dynamic-update-slice_fusion.1
  69.8 0.6 slice_dynamic-update-slice_fusion
  70.5 1.9 %collective-permute-done.8 = bf16[32,1536]{1,0:T(8,128)(2,1)S(1)} collective-permute-done((bf16[32,1536]{1,0:T(8,128)(2,1)S(1)}, bf16[32,1536]{1,0:T(8,128)(2,1)S(1)}, u32[]{:S(2)}, u32[]{:S(2)}) %collective-permute-start.8) | collective-permute-done | bytes 98336 | tf_op jit(solution)/shard_map/ppermute | solution.py:41
  72.4 0.2 fusion.61
  72.6 1.7 %convolution_convert_fusion.2 = bf16[32,512]{1,0:T(8,128)(2,1)S(1)} fusion(bf16[512,704]{1,0:T(8,128)(2,1)} %slice_dynamic-update-slice_fusion, s32[512]{0:T(512)S(1)} %get-tuple-element.38, s32[512]{0:T(512)S(1)} %get-tuple-element.39, pred[512]{0:T(512)(128)(4,1)S(1)} %fusion.64, f32[32,1536]{1,0:T(8,128)S(1)} %convert_add_fusion.1, f32[32]{0:T(128)S(1)} %fusion.61), kind=kOutput, calls=%fused_computation.14 | convolution fusion | flops 41369600 | bytes 955008 | tf_op jit(solution)/shard_map/dot_general | solution.py:306
  74.3 0.7 broadcast_in_dim.26
  75.0 9.6 %all-to-all-start.1 = ((bf16[8,32,512]{2,1,0:T(8,128)(2,1)}), bf16[8,32,512]{2,1,0:T(8,128)(2,1)S(1)}, u32[]{:S(2)}, u32[]{:S(2)}) async-start(bf16[8,32,512]{2,1,0:T(8,128)(2,1)} %broadcast_in_dim.26), calls=%async_computation.1 | async-start | bytes 524288 | tf_op jit(solution)/shard_map/all_to_all | solution.py:26
  84.6 0.7 all-gather.3.cloned.1.call-update
  85.3 5.7 %all-to-all-done.1 = bf16[8,32,512]{2,1,0:T(8,128)(2,1)S(1)} async-done(((bf16[8,32,512]{2,1,0:T(8,128)(2,1)}), bf16[8,32,512]{2,1,0:T(8,128)(2,1)S(1)}, u32[]{:S(2)}, u32[]{:S(2)}) %all-to-all-start.1) | async-done | bytes 262176 | tf_op jit(solution)/shard_map/all_to_all | solution.py:26
  91.1 0.1 fusion.34
  91.4 1.9 %fusion.3 = f32[32,1664]{1,0:T(8,128)S(1)} fusion(bf16[32,512]{1,0:T(8,128)(2,1)S(1)} %get-tuple-element.25, bf16[512,2176]{1,0:T(8,128)(2,1)} %all-gather.5.cloned.1.call-done), kind=kOutput, calls=%fused_computation.9 | convolution fusion | flops 54525952 | bytes 1949696 | tf_op jit(solution)/shard_map/dot_general | solution.py:143
  93.5 0.3 collective-permute-start.11
  93.8 3.4 %collective-permute-start.12 = (bf16[8,1664]{1,0:T(8,128)(2,1)S(1)}, bf16[8,1664]{1,0:T(8,128)(2,1)S(1)}, u32[]{:S(2)}, u32[]{:S(2)}) collective-permute-start(bf16[8,1664]{1,0:T(8,128)(2,1)S(1)} %get-tuple-element.29), channel_id=1, source_target_pairs={{0,16},{8,24},{16,0},{24,8},{1,17},{9,25},{17,1},{25,9},{2,18},{10... | collective-permute-start | bytes 79880 | tf_op jit(solution)/shard_map/ppermute | solution.py:154
  97.1 0.5 collective-permute-done.11.near_ref
  97.7 1.0 collective-permute-done.12.far_ref
  98.6 1.7 %collective-permute-done.13.last_ref = bf16[8,1664]{1,0:T(8,128)(2,1)S(1)} collective-permute-done((bf16[8,1664]{1,0:T(8,128)(2,1)S(1)}, bf16[8,1664]{1,0:T(8,128)(2,1)S(1)}, u32[]{:S(2)}, u32[]{:S(2)}) %collective-permute-start.13) | collective-permute-done | bytes 26656 | tf_op jit(solution)/shard_map/ppermute | solution.py:154
  100.3 2.2 %shard_map.267 = (bf16[4,8,512]{2,1,0:T(8,128)(2,1)S(1)}, f32[8,4,128,128]{3,2,1,0:T(8,128)}) custom-call(bf16[8,1664]{1,0:T(8,128)(2,1)S(1)} %get-tuple-element.31.own_ref, bf16[8,1664]{1,0:T(8,128)(2,1)S(1)} %collective-permute-done.11.near_ref, bf16[8,1664]{1,0:T(8,128)(2,1)S(1)} %collective-permute-done.12.far_ref, ...), custom_call_target="tpu_custom_call" | custom-call | flops 20000000 | bytes 4200000 | tf_op jit(solution)/shard_map/pallas_call | solution.py:156
  102.6 6.7 %all_to_all.25 = bf16[4,8,512]{2,1,0:T(8,128)(2,1)S(1)} all-to-all(bf16[4,8,512]{2,1,0:T(8,128)(2,1)S(1)} %get-tuple-element.22), channel_id=1, replica_groups=mesh['z'=8,'y'=4,'x'=4,'c'=2] {'y'}, dimensions={0} | all-to-all | bytes 65536 | tf_op jit(solution)/shard_map/all_to_all | solution.py:26
  109.3 1.3 convolution_convert_fusion.4
  110.6 12.5 %all_to_all.26 = bf16[8,32,512]{2,1,0:T(8,128)(2,1)S(1)} all-to-all(bf16[8,32,512]{2,1,0:T(8,128)(2,1)S(1)} %broadcast_in_dim.30), channel_id=1, replica_groups=mesh['z'=8,'y'=4,'x'=4,'c'=2] {'x','c'}, dimensions={0} | all-to-all | bytes 524288 | tf_op jit(solution)/shard_map/all_to_all | solution.py:26
  123.4 1.7 %convolution_convert_fusion = bf16[32,1408]{1,0:T(8,128)(2,1)S(1)} fusion(bf16[512,2112]{1,0:T(8,128)(2,1)} %all-gather.3.cloned.1.call-done, f32[32,512]{1,0:T(8,128)S(1)} %convert_reduce_fusion, bf16[32,512]{1,0:T(8,128)(2,1)S(1)} %get-tuple-element.25), kind=kOutput, calls=%fused_computation.8 | convolution fusion | flops 46231552 | bytes 1630208 | tf_op jit(solution)/shard_map/dot_general | solution.py:316
  125.1 0.4 collective-permute-start.14
  125.5 2.3 %collective-permute-start.15 = (bf16[32,1536]{1,0:T(8,128)(2,1)S(1)}, bf16[32,1536]{1,0:T(8,128)(2,1)S(1)}, u32[]{:S(2)}, u32[]{:S(2)}) collective-permute-start(bf16[32,1536]{1,0:T(8,128)(2,1)S(1)} %pad_maximum_fusion.4), channel_id=1, source_target_pairs={{0,16},{8,24},{16,0},{24,8},{1,17},{9,25},{17,1},{25,9},{2,18},{10... | collective-permute-start | bytes 294920 | tf_op jit(solution)/shard_map/ppermute | solution.py:41
  127.8 1.4 collective-permute-start.16
  129.2 1.8 %collective-permute-done.14 = bf16[32,1536]{1,0:T(8,128)(2,1)S(1)} collective-permute-done((bf16[32,1536]{1,0:T(8,128)(2,1)S(1)}, bf16[32,1536]{1,0:T(8,128)(2,1)S(1)}, u32[]{:S(2)}, u32[]{:S(2)}) %collective-permute-start.14) | collective-permute-done | bytes 98336 | tf_op jit(solution)/shard_map/ppermute | solution.py:41
  130.9 0.6 collective-permute-done.16
  131.6 0.2 fusion.56
  131.8 1.5 convolution_convert_fusion.1
  133.4 0.2 reshape.82
  133.6 23.3 %all_to_all.27 = bf16[64,2,256]{2,1,0:T(2,128)(2,1)S(1)} all-to-all(bf16[64,2,256]{2,1,0:T(2,128)(2,1)S(1)} %reshape.82), channel_id=1, replica_groups=mesh['z'=8,'y'=4,'x'=4,'c'=2] {'z','x','c'}, dimensions={0} | all-to-all | bytes 131072 | tf_op jit(solution)/shard_map/all_to_all | solution.py:26
  156.9 0.1 reshape.83
  157.1 0.7 convert_element_type.215
  (70 shorter events, 1.8 us)
Async XLA Ops:
  10.5 42.5 %copy-start.4 = (bf16[64,2112]{1,0:T(8,128)(2,1)S(1)}, bf16[64,2112]{1,0:T(8,128)(2,1)}, u32[]{:S(2)}) copy-start(bf16[64,2112]{1,0:T(8,128)(2,1)} %get-tuple-element.13) | copy-start | bytes 811012
  10.5 18.4 %collective-permute-start = (bf16[64,2112]{1,0:T(8,128)(2,1)}, bf16[64,2112]{1,0:T(8,128)(2,1)S(1)}, u32[]{:S(2)}, u32[]{:S(2)}) collective-permute-start(bf16[64,2112]{1,0:T(8,128)(2,1)} %get-tuple-element.13), channel_id=1, source_target_pairs={{0,224},{32,0},{64,32},{96,64},{128,96},{160,128},{192,160},{224,1... | collective-permute-start | bytes 811016 | tf_op jit(solution)/shard_map/ppermute | solution.py:67
  16.9 14.9 %collective-permute-start.3 = (bf16[64,2112]{1,0:T(8,128)(2,1)}, bf16[64,2112]{1,0:T(8,128)(2,1)S(1)}, u32[]{:S(2)}, u32[]{:S(2)}) collective-permute-start(bf16[64,2112]{1,0:T(8,128)(2,1)} %get-tuple-element.13), channel_id=1, source_target_pairs={{0,32},{32,64},{64,96},{96,128},{128,160},{160,192},{192,224},{224... | collective-permute-start | bytes 811016 | tf_op jit(solution)/shard_map/ppermute | solution.py:66
  18.5 17.9 %all-to-all-start = ((bf16[64,2,128]{2,1,0:T(2,128)(2,1)}), bf16[64,2,128]{2,1,0:T(2,128)(2,1)S(1)}, u32[]{:S(2)}, u32[]{:S(2)}) async-start(bf16[64,2,128]{2,1,0:T(2,128)(2,1)} %reshape.80), calls=%async_computation | async-start | bytes 65536 | tf_op jit(solution)/shard_map/all_to_all | solution.py:26
  27.1 28.9 %copy-start.6 = (f32[128]{0:T(128)S(1)}, f32[128]{0:T(128)}, u32[]{:S(2)}) copy-start(f32[128]{0:T(128)} %constant.57) | copy-start | bytes 1540
  27.1 28.9 %copy-start.7 = (f32[128]{0:T(128)S(1)}, f32[128]{0:T(128)}, u32[]{:S(2)}) copy-start(f32[128]{0:T(128)} %constant.58) | copy-start | bytes 1540
  27.1 64.3 %all-gather.5.cloned.1.call-start = ((), (), s32[]{:S(2)}) async-start(), calls=%async_computation.6 | async-start | bytes 2506752 | tf_op jit(solution)/shard_map/all_gather | solution.py:235
  28.9 8.5 %collective-permute-start.1 = (bf16[64,2112]{1,0:T(8,128)(2,1)S(1)}, bf16[64,2112]{1,0:T(8,128)(2,1)S(1)}, u32[]{:S(2)}, u32[]{:S(2)}) collective-permute-start(bf16[64,2112]{1,0:T(8,128)(2,1)S(1)} %collective-permute-done), channel_id=1, source_target_pairs={{0,224},{32,0},{64,32},{96,64},{128,96},{160,128},{192,160},{224,1... | collective-permute-start | bytes 811016 | tf_op jit(solution)/shard_map/ppermute | solution.py:67
  31.8 9.0 %collective-permute-start.4 = (bf16[64,2112]{1,0:T(8,128)(2,1)S(1)}, bf16[64,2112]{1,0:T(8,128)(2,1)S(1)}, u32[]{:S(2)}, u32[]{:S(2)}) collective-permute-start(bf16[64,2112]{1,0:T(8,128)(2,1)S(1)} %collective-permute-done.3), channel_id=1, source_target_pairs={{0,32},{32,64},{64,96},{96,128},{128,160},{160,192},{192,224},{224... | collective-permute-start | bytes 811016 | tf_op jit(solution)/shard_map/ppermute | solution.py:66
  37.4 12.7 %collective-permute-start.2 = (bf16[64,2112]{1,0:T(8,128)(2,1)S(1)}, bf16[64,2112]{1,0:T(8,128)(2,1)S(1)}, u32[]{:S(2)}, u32[]{:S(2)}) collective-permute-start(bf16[64,2112]{1,0:T(8,128)(2,1)S(1)} %collective-permute-done.1), channel_id=1, source_target_pairs={{0,224},{32,0},{64,32},{96,64},{128,96},{160,128},{192,160},{224,1... | collective-permute-start | bytes 811016 | tf_op jit(solution)/shard_map/ppermute | solution.py:67
  40.8 12.1 %collective-permute-start.5 = (bf16[64,2112]{1,0:T(8,128)(2,1)S(1)}, bf16[64,2112]{1,0:T(8,128)(2,1)S(1)}, u32[]{:S(2)}, u32[]{:S(2)}) collective-permute-start(bf16[64,2112]{1,0:T(8,128)(2,1)S(1)} %collective-permute-done.4), channel_id=1, source_target_pairs={{0,32},{32,64},{64,96},{96,128},{128,160},{160,192},{192,224},{224... | collective-permute-start | bytes 811016 | tf_op jit(solution)/shard_map/ppermute | solution.py:66
  40.9 12.0 %copy-start.5 = (bf16[512,704]{1,0:T(8,128)(2,1)}, bf16[512,704]{1,0:T(8,128)(2,1)S(1)}, u32[]{:S(2)}) copy-start(bf16[512,704]{1,0:T(8,128)(2,1)S(1)} %slice_dynamic-update-slice_fusion.3) | copy-start | bytes 2162692
  53.4 9.3 %collective-permute-start.7 = (bf16[64,1088]{1,0:T(8,128)(2,1)S(1)}, bf16[64,1088]{1,0:T(8,128)(2,1)S(1)}, u32[]{:S(2)}, u32[]{:S(2)}) collective-permute-start(bf16[64,1088]{1,0:T(8,128)(2,1)S(1)} %slice.215), channel_id=1, source_target_pairs={{0,224},{32,0},{64,32},{96,64},{128,96},{160,128},{192,160},{224,1... | collective-permute-start | bytes 417800 | tf_op jit(solution)/shard_map/ppermute | solution.py:70
  54.2 8.5 %collective-permute-start.6 = (bf16[64,1024]{1,0:T(8,128)(2,1)S(1)}, bf16[64,1024]{1,0:T(8,128)(2,1)S(1)}, u32[]{:S(2)}, u32[]{:S(2)}) collective-permute-start(bf16[64,1024]{1,0:T(8,128)(2,1)S(1)} %slice.214), channel_id=1, source_target_pairs={{0,32},{32,64},{64,96},{96,128},{128,160},{160,192},{192,224},{224... | collective-permute-start | bytes 393224 | tf_op jit(solution)/shard_map/ppermute | solution.py:69
  63.0 7.5 %collective-permute-start.10 = (bf16[32,1536]{1,0:T(8,128)(2,1)S(1)}, bf16[32,1536]{1,0:T(8,128)(2,1)S(1)}, u32[]{:S(2)}, u32[]{:S(2)}) collective-permute-start(bf16[32,1536]{1,0:T(8,128)(2,1)S(1)} %pad_maximum_fusion.3), channel_id=1, source_target_pairs={{0,24},{8,0},{16,8},{24,16},{1,25},{9,1},{17,9},{25,17},{2,26},{10... | collective-permute-start | bytes 294920 | tf_op jit(solution)/shard_map/ppermute | solution.py:41
  66.6 5.7 %collective-permute-start.8 = (bf16[32,1536]{1,0:T(8,128)(2,1)S(1)}, bf16[32,1536]{1,0:T(8,128)(2,1)S(1)}, u32[]{:S(2)}, u32[]{:S(2)}) collective-permute-start(bf16[32,1536]{1,0:T(8,128)(2,1)S(1)} %pad_maximum_fusion.3), channel_id=1, source_target_pairs={{0,8},{8,16},{16,24},{24,0},{1,9},{9,17},{17,25},{25,1},{2,10},{10... | collective-permute-start | bytes 294920 | tf_op jit(solution)/shard_map/ppermute | solution.py:41
  66.6 5.7 %collective-permute-start.9 = (bf16[32,1536]{1,0:T(8,128)(2,1)S(1)}, bf16[32,1536]{1,0:T(8,128)(2,1)S(1)}, u32[]{:S(2)}, u32[]{:S(2)}) collective-permute-start(bf16[32,1536]{1,0:T(8,128)(2,1)S(1)} %pad_maximum_fusion.3), channel_id=1, source_target_pairs={{0,16},{8,24},{16,0},{24,8},{1,17},{9,25},{17,1},{25,9},{2,18},{10... | collective-permute-start | bytes 294920 | tf_op jit(solution)/shard_map/ppermute | solution.py:41
  74.3 26.1 %copy-start = (f32[8,4,128,128]{3,2,1,0:T(8,128)S(1)}, f32[8,4,128,128]{3,2,1,0:T(8,128)}, u32[]{:S(2)}) copy-start(f32[8,4,128,128]{3,2,1,0:T(8,128)} %state_ref.1) | copy-start | bytes 6291460
  74.3 26.1 %copy-start.1 = (f32[4]{0:T(128)S(1)}, f32[4]{0:T(128)}, u32[]{:S(2)}) copy-start(f32[4]{0:T(128)} %param.40) | copy-start | bytes 52
  74.3 26.1 %copy-start.2 = (f32[4]{0:T(128)S(1)}, f32[4]{0:T(128)}, u32[]{:S(2)}) copy-start(f32[4]{0:T(128)} %param.41) | copy-start | bytes 52
  74.3 26.0 %copy-start.3 = (f32[128]{0:T(128)S(1)}, f32[128]{0:T(128)}, u32[]{:S(2)}) copy-start(f32[128]{0:T(128)} %param.42) | copy-start | bytes 1540
  75.0 16.0 %all-to-all-start.1 = ((bf16[8,32,512]{2,1,0:T(8,128)(2,1)}), bf16[8,32,512]{2,1,0:T(8,128)(2,1)S(1)}, u32[]{:S(2)}, u32[]{:S(2)}) async-start(bf16[8,32,512]{2,1,0:T(8,128)(2,1)} %broadcast_in_dim.26), calls=%async_computation.1 | async-start | bytes 524288 | tf_op jit(solution)/shard_map/all_to_all | solution.py:26
  84.6 38.8 %all-gather.3.cloned.1.call-start = ((), (), s32[]{:S(2)}) async-start(), calls=%async_computation.5 | async-start | bytes 2506752 | tf_op jit(solution)/shard_map/all_gather | solution.py:235
  93.5 4.2 %collective-permute-start.11 = (bf16[8,1664]{1,0:T(8,128)(2,1)S(1)}, bf16[8,1664]{1,0:T(8,128)(2,1)S(1)}, u32[]{:S(2)}, u32[]{:S(2)}) collective-permute-start(bf16[8,1664]{1,0:T(8,128)(2,1)S(1)} %get-tuple-element.30), channel_id=1, source_target_pairs={{0,8},{8,16},{16,24},{24,0},{1,9},{9,17},{17,25},{25,1},{2,10},{10... | collective-permute-start | bytes 79880 | tf_op jit(solution)/shard_map/ppermute | solution.py:154
  93.8 4.9 %collective-permute-start.12 = (bf16[8,1664]{1,0:T(8,128)(2,1)S(1)}, bf16[8,1664]{1,0:T(8,128)(2,1)S(1)}, u32[]{:S(2)}, u32[]{:S(2)}) collective-permute-start(bf16[8,1664]{1,0:T(8,128)(2,1)S(1)} %get-tuple-element.29), channel_id=1, source_target_pairs={{0,16},{8,24},{16,0},{24,8},{1,17},{9,25},{17,1},{25,9},{2,18},{10... | collective-permute-start | bytes 79880 | tf_op jit(solution)/shard_map/ppermute | solution.py:154
  97.1 3.2 %collective-permute-start.13 = (bf16[8,1664]{1,0:T(8,128)(2,1)S(1)}, bf16[8,1664]{1,0:T(8,128)(2,1)S(1)}, u32[]{:S(2)}, u32[]{:S(2)}) collective-permute-start(bf16[8,1664]{1,0:T(8,128)(2,1)S(1)} %get-tuple-element.28), channel_id=1, source_target_pairs={{0,24},{8,0},{16,8},{24,16},{1,25},{9,1},{17,9},{25,17},{2,26},{10... | collective-permute-start | bytes 79880 | tf_op jit(solution)/shard_map/ppermute | solution.py:154
  125.1 5.8 %collective-permute-start.14 = (bf16[32,1536]{1,0:T(8,128)(2,1)S(1)}, bf16[32,1536]{1,0:T(8,128)(2,1)S(1)}, u32[]{:S(2)}, u32[]{:S(2)}) collective-permute-start(bf16[32,1536]{1,0:T(8,128)(2,1)S(1)} %pad_maximum_fusion.4), channel_id=1, source_target_pairs={{0,8},{8,16},{16,24},{24,0},{1,9},{9,17},{17,25},{25,1},{2,10},{10... | collective-permute-start | bytes 294920 | tf_op jit(solution)/shard_map/ppermute | solution.py:41
  125.5 5.4 %collective-permute-start.15 = (bf16[32,1536]{1,0:T(8,128)(2,1)S(1)}, bf16[32,1536]{1,0:T(8,128)(2,1)S(1)}, u32[]{:S(2)}, u32[]{:S(2)}) collective-permute-start(bf16[32,1536]{1,0:T(8,128)(2,1)S(1)} %pad_maximum_fusion.4), channel_id=1, source_target_pairs={{0,16},{8,24},{16,0},{24,8},{1,17},{9,25},{17,1},{25,9},{2,18},{10... | collective-permute-start | bytes 294920 | tf_op jit(solution)/shard_map/ppermute | solution.py:41
  127.8 3.7 %collective-permute-start.16 = (bf16[32,1536]{1,0:T(8,128)(2,1)S(1)}, bf16[32,1536]{1,0:T(8,128)(2,1)S(1)}, u32[]{:S(2)}, u32[]{:S(2)}) collective-permute-start(bf16[32,1536]{1,0:T(8,128)(2,1)S(1)} %pad_maximum_fusion.4), channel_id=1, source_target_pairs={{0,24},{8,0},{16,8},{24,16},{1,25},{9,1},{17,9},{25,17},{2,26},{10... | collective-permute-start | bytes 294920 | tf_op jit(solution)/shard_map/ppermute | solution.py:41
Sparse Core Ops, SparseCore 0:
  29.7 44.4 all-gather.4
  87.2 35.3 all-gather.2

commit v5 on v3

--- a/solution.py
+++ b/solution.py
@@ -205,9 +205,6 @@
     first_in = scaled_rows(norm_gain_first, [gate_first, up_first])
     width = first_in.shape[1]
     first_blocks = around(jnp.concatenate([first_in, down_first.T], axis=1), "z")
-    first_blocks[1], first_blocks[-1], query_weight, out_weight = lax.optimization_barrier(
-        (first_blocks[1], first_blocks[-1], query_weight, out_weight)
-    )
     mixer_in = scaled_rows(norm_gain_mixer, [query_weight, key_weight, value_weight, output_gate_weight, *gate_cols])
     second_in = scaled_rows(norm_gain_second, [gate_second, up_second])
     mixer_width = mixer_in.shape[1]
@@ -217,7 +214,10 @@
     own_cols, rows = columns.shape[0], columns.shape[1] // planes
     pieces = jnp.moveaxis(columns.reshape(own_cols, planes, rows), 1, 0)
     pieces = jnp.broadcast_to(pieces[:, None], (planes, tp_count, own_cols, rows))
-    pieces = pieces.reshape(-1, own_cols, rows)
+    pieces, middle = lax.optimization_barrier((pieces.reshape(-1, own_cols, rows), middle))
+    first_blocks[1], first_blocks[-1], middle = lax.optimization_barrier(
+        (first_blocks[1], first_blocks[-1], middle)
+    )
     first_blocks[3], first_blocks[-3], last, plane = lax.optimization_barrier(
         (first_blocks[3], first_blocks[-3], last, lax.axis_index("z"))
     )

time: 161 us -> 161 us (level)
  blocking collectives: 59.3 us -> 62.3 us
  waiting for transfers between devices: 32.5 us -> 29.5 us
    ppermute x3, waiting for transfers between devices: 13.4 us -> 7.6 us  [around(): backward = blocks[step] = lax.ppermute(backward, axis, behind)]
    all_to_all x5, blocking collectives: 59.3 us -> 62.3 us  [exchange(): return lax.all_to_all(blocks, axis, split_axis=0, concat_axis=0, tiled=True)]
    all_to_all x1, waiting for transfers between devices: 1.9 us -> 4.72 us  [exchange(): return lax.all_to_all(blocks, axis, split_axis=0, concat_axis=0, tiled=True)]
  transfers between devices with their start and end apart: 17 -> 17, of which waited for: 9 -> 8; matrix products, arithmetic and copies ran while one was open for 8% -> 9% of each run, Pallas kernels for 1% -> 1%
where the time goes in v5:
time: 161 us; the launch traced here: 160 us
  blocking collectives  62.3 us (39%)
  starting transfers between devices  30.6 us (19%)
  waiting for transfers between devices  29.5 us (18%)
  between operations  14.5 us (9%)
  matrix products  8.45 us (5%)
  other arithmetic  6.79 us (4%)
  local copies, waits for them, and re-layouts  5.77 us (4%)
  Pallas kernels  2.23 us (1%)
    all_to_all x5, blocking collectives, exchange(): return lax.all_to_all(blocks, axis, split_axis=0, concat_axis=0, tiled=True)  62.3 us
    ppermute x3, starting transfers between devices, around(): backward = blocks[step] = lax.ppermute(backward, axis, behind)  12.8 us
    ppermute x6, waiting for transfers between devices, ring_sum(): lax.ppermute(value, axis, [(i, (i + places) % size) for i in range(size)])  8.68 us
    all_to_all x1, starting transfers between devices, exchange(): return lax.all_to_all(blocks, axis, split_axis=0, concat_axis=0, tiled=True)  8.6 us
    ppermute x3, waiting for transfers between devices, around(): backward = blocks[step] = lax.ppermute(backward, axis, behind)  7.6 us
    ppermute x6, starting transfers between devices, ring_sum(): lax.ppermute(value, axis, [(i, (i + places) % size) for i in range(size)])  7.53 us
    ppermute x1, waiting for transfers between devices, around(): forward = lax.ppermute(forward[:, :half], axis, ahead)  5.61 us
    all_to_all x1, waiting for transfers between devices, exchange(): return lax.all_to_all(blocks, axis, split_axis=0, concat_axis=0, tiled=True)  4.72 us
  transfers between devices with their start and end apart: 17, of which 8 were waited for; matrix products, arithmetic and copies ran while one was open for 9% of the time, Pallas kernels for 1%

profile of v5, /device:TPU:1, one launch (start us, length us, event | category | flops | bytes accessed | tf_op | source)
XLA Modules:
  0.0 160.2 jit_solution(7078279666171215726)
XLA Ops:
  7.2 1.1 multiply_convert_fusion.2
  8.4 0.9 pad_maximum_fusion
  9.3 6.5 %collective-permute-start = (bf16[64,2112]{1,0:T(8,128)(2,1)S(1)}, bf16[64,2112]{1,0:T(8,128)(2,1)S(1)}, u32[]{:S(2)}, u32[]{:S(2)}) collective-permute-start(bf16[64,2112]{1,0:T(8,128)(2,1)S(1)} %pad_maximum_fusion), channel_id=1, source_target_pairs={{0,224},{32,0},{64,32},{96,64},{128,96},{160,128},{192,160},{224,1... | collective-permute-start | bytes 811016 | tf_op jit(solution)/shard_map/ppermute | solution.py:66
  15.7 0.7 constant_dynamic-slice_fusion
  16.5 0.1 copy.48
  16.6 0.1 copy.49
  16.7 0.8 reshape.68
  17.5 1.0 concatenate.55
  18.5 0.8 multiply_convert_fusion
  19.3 1.6 pad_maximum_fusion.2
  20.9 0.7 reshape.78
  21.6 8.6 %all-to-all-start = ((bf16[64,2,128]{2,1,0:T(2,128)(2,1)}), bf16[64,2,128]{2,1,0:T(2,128)(2,1)S(1)}, u32[]{:S(2)}, u32[]{:S(2)}) async-start(bf16[64,2,128]{2,1,0:T(2,128)(2,1)} %reshape.78), calls=%async_computation | async-start | bytes 65536 | tf_op jit(solution)/shard_map/all_to_all | solution.py:25
  30.3 0.7 all-gather.5.cloned.1.call-update
  31.0 0.1 multiply_convert_fusion.1
  31.1 2.9 %collective-permute-start.1 = (bf16[64,2112]{1,0:T(8,128)(2,1)S(1)}, bf16[64,2112]{1,0:T(8,128)(2,1)S(1)}, u32[]{:S(2)}, u32[]{:S(2)}) collective-permute-start(bf16[64,2112]{1,0:T(8,128)(2,1)S(1)} %collective-permute-done), channel_id=1, source_target_pairs={{0,224},{32,0},{64,32},{96,64},{128,96},{160,128},{192,160},{224,1... | collective-permute-start | bytes 811016 | tf_op jit(solution)/shard_map/ppermute | solution.py:66
  34.1 0.8 pad_maximum_fusion.1
  34.8 4.7 %all-to-all-done = bf16[64,2,128]{2,1,0:T(2,128)(2,1)S(1)} async-done(((bf16[64,2,128]{2,1,0:T(2,128)(2,1)}), bf16[64,2,128]{2,1,0:T(2,128)(2,1)S(1)}, u32[]{:S(2)}, u32[]{:S(2)}) %all-to-all-start) | async-done | bytes 32800 | tf_op jit(solution)/shard_map/all_to_all | solution.py:25
  39.5 0.1 reshape.79
  39.7 3.4 %collective-permute-start.2 = (bf16[64,2112]{1,0:T(8,128)(2,1)S(1)}, bf16[64,2112]{1,0:T(8,128)(2,1)S(1)}, u32[]{:S(2)}, u32[]{:S(2)}) collective-permute-start(bf16[64,2112]{1,0:T(8,128)(2,1)S(1)} %collective-permute-done.1), channel_id=1, source_target_pairs={{0,224},{32,0},{64,32},{96,64},{128,96},{160,128},{192,160},{224,1... | collective-permute-start | bytes 811016 | tf_op jit(solution)/shard_map/ppermute | solution.py:66
  43.1 7.6 %collective-permute-done.2 = bf16[64,2112]{1,0:T(8,128)(2,1)S(1)} collective-permute-done((bf16[64,2112]{1,0:T(8,128)(2,1)S(1)}, bf16[64,2112]{1,0:T(8,128)(2,1)S(1)}, u32[]{:S(2)}, u32[]{:S(2)}) %collective-permute-start.2) | collective-permute-done | bytes 270368 | tf_op jit(solution)/shard_map/ppermute | solution.py:66
  50.7 2.2 %collective-permute-done.5 = bf16[64,2112]{1,0:T(8,128)(2,1)S(1)} collective-permute-done((bf16[64,2112]{1,0:T(8,128)(2,1)S(1)}, bf16[64,2112]{1,0:T(8,128)(2,1)S(1)}, u32[]{:S(2)}, u32[]{:S(2)}) %collective-permute-start.5) | collective-permute-done | bytes 270368 | tf_op jit(solution)/shard_map/ppermute | solution.py:65
  53.0 1.4 collective-permute-start.7
  54.4 0.3 collective-permute-start.6
  54.6 0.1 fusion.23
  54.7 0.1 copy.61
  54.9 0.1 fusion.33
  55.0 0.7 slice_dynamic-update-slice_fusion.5
  55.6 0.2 fusion.57
  55.8 0.2 fusion.19
  56.0 0.2 fusion.15
  56.2 0.2 convolution_add_fusion.4
  56.5 0.2 convolution_add_fusion.3
  56.7 0.2 fusion.1
  56.9 0.2 convolution_add_fusion.1
  57.2 5.6 %collective-permute-done.6 = bf16[64,1024]{1,0:T(8,128)(2,1)S(1)} collective-permute-done((bf16[64,1024]{1,0:T(8,128)(2,1)S(1)}, bf16[64,1024]{1,0:T(8,128)(2,1)S(1)}, u32[]{:S(2)}, u32[]{:S(2)}) %collective-permute-start.6) | collective-permute-done | bytes 131104 | tf_op jit(solution)/shard_map/ppermute | solution.py:68
  62.8 0.2 fusion.2
  63.1 3.1 %collective-permute-start.10 = (bf16[32,1536]{1,0:T(8,128)(2,1)S(1)}, bf16[32,1536]{1,0:T(8,128)(2,1)S(1)}, u32[]{:S(2)}, u32[]{:S(2)}) collective-permute-start(bf16[32,1536]{1,0:T(8,128)(2,1)S(1)} %pad_maximum_fusion.6), channel_id=1, source_target_pairs={{0,24},{8,0},{16,8},{24,16},{1,25},{9,1},{17,9},{25,17},{2,26},{10... | collective-permute-start | bytes 294920 | tf_op jit(solution)/shard_map/ppermute | solution.py:40
  66.1 1.5 collective-permute-start.9
  67.8 4.5 %collective-permute-done.8 = bf16[32,1536]{1,0:T(8,128)(2,1)S(1)} collective-permute-done((bf16[32,1536]{1,0:T(8,128)(2,1)S(1)}, bf16[32,1536]{1,0:T(8,128)(2,1)S(1)}, u32[]{:S(2)}, u32[]{:S(2)}) %collective-permute-start.8) | collective-permute-done | bytes 98336 | tf_op jit(solution)/shard_map/ppermute | solution.py:40
  72.3 0.2 fusion.56
  72.5 0.5 convolution_convert_fusion.2
  73.1 17.3 %all_to_all.30 = bf16[8,32,512]{2,1,0:T(8,128)(2,1)S(1)} all-to-all(bf16[8,32,512]{2,1,0:T(8,128)(2,1)S(1)} %broadcast_in_dim.32), channel_id=1, replica_groups=mesh['z'=8,'y'=4,'x'=4,'c'=2] {'x','c'}, dimensions={0} | all-to-all | bytes 524288 | tf_op jit(solution)/shard_map/all_to_all | solution.py:25
  90.4 0.1 fusion.29
  90.7 1.9 %fusion.3 = f32[32,1664]{1,0:T(8,128)S(1)} fusion(bf16[32,512]{1,0:T(8,128)(2,1)S(1)} %get-tuple-element.31, bf16[512,2176]{1,0:T(8,128)(2,1)} %all-gather.5.cloned.1.call-done), kind=kOutput, calls=%fused_computation.9 | convolution fusion | flops 54525952 | bytes 1949696 | tf_op jit(solution)/shard_map/dot_general | solution.py:142
  92.6 0.1 fusion.58
  92.7 8.1 %all_to_all.31.arrived_ref = bf16[4,8,1664]{2,1,0:T(8,128)(2,1)S(1)} all-to-all(bf16[4,8,1664]{2,1,0:T(8,128)(2,1)S(1)} %pad_maximum_fusion.5), channel_id=1, replica_groups=mesh['z'=8,'y'=4,'x'=4,'c'=2] {'y'}, dimensions={0} | all-to-all | bytes 212992 | tf_op jit(solution)/shard_map/all_to_all | solution.py:25
  100.8 2.2 %shard_map.266 = (bf16[4,8,512]{2,1,0:T(8,128)(2,1)S(1)}, f32[8,4,128,128]{3,2,1,0:T(8,128)}) custom-call(bf16[4,8,1664]{2,1,0:T(8,128)(2,1)S(1)} %all_to_all.31.arrived_ref, f32[1,4]{1,0:T(1,128)S(1)} %bitcast.91, f32[1,4]{1,0:T(1,128)S(1)} %bitcast.92, f32[1,128]{1,0:T(1,128)S(1)} %bitcast.93, f32[8,4,128,128]{3,2,1,0:T(8,128)S(1)} %copy-done), custom_call_target="tpu_custom_call" | custom-call | flops 20000000 | bytes 4200000 | tf_op jit(solution)/shard_map/pallas_call | solution.py:149
  103.0 6.7 %all_to_all.32 = bf16[4,8,512]{2,1,0:T(8,128)(2,1)S(1)} all-to-all(bf16[4,8,512]{2,1,0:T(8,128)(2,1)S(1)} %get-tuple-element.28), channel_id=1, replica_groups=mesh['z'=8,'y'=4,'x'=4,'c'=2] {'y'}, dimensions={0} | all-to-all | bytes 65536 | tf_op jit(solution)/shard_map/all_to_all | solution.py:25
  109.7 1.3 convolution_convert_fusion.4
  111.0 12.4 %all_to_all.33 = bf16[8,32,512]{2,1,0:T(8,128)(2,1)S(1)} all-to-all(bf16[8,32,512]{2,1,0:T(8,128)(2,1)S(1)} %broadcast_in_dim.36), channel_id=1, replica_groups=mesh['z'=8,'y'=4,'x'=4,'c'=2] {'x','c'}, dimensions={0} | all-to-all | bytes 524288 | tf_op jit(solution)/shard_map/all_to_all | solution.py:25
  123.4 0.1 multiply_reduce_fusion
  123.6 1.7 %convolution_convert_fusion = bf16[32,1408]{1,0:T(8,128)(2,1)S(1)} fusion(bf16[512,2112]{1,0:T(8,128)(2,1)} %all-gather.3.cloned.1.call-done, f32[32,512]{1,0:T(8,128)S(1)} %convert_reduce_fusion, bf16[32,512]{1,0:T(8,128)(2,1)S(1)} %get-tuple-element.31), kind=kOutput, calls=%fused_computation.8 | convolution fusion | flops 46231552 | bytes 1630208 | tf_op jit(solution)/shard_map/dot_general | solution.py:265
  125.4 0.4 collective-permute-start.11
  125.7 1.8 %collective-permute-start.12 = (bf16[32,1536]{1,0:T(8,128)(2,1)S(1)}, bf16[32,1536]{1,0:T(8,128)(2,1)S(1)}, u32[]{:S(2)}, u32[]{:S(2)}) collective-permute-start(bf16[32,1536]{1,0:T(8,128)(2,1)S(1)} %pad_maximum_fusion.7), channel_id=1, source_target_pairs={{0,16},{8,24},{16,0},{24,8},{1,17},{9,25},{17,1},{25,9},{2,18},{10... | collective-permute-start | bytes 294920 | tf_op jit(solution)/shard_map/ppermute | solution.py:40
  127.5 0.8 collective-permute-start.13
  128.4 3.2 %collective-permute-done.11 = bf16[32,1536]{1,0:T(8,128)(2,1)S(1)} collective-permute-done((bf16[32,1536]{1,0:T(8,128)(2,1)S(1)}, bf16[32,1536]{1,0:T(8,128)(2,1)S(1)}, u32[]{:S(2)}, u32[]{:S(2)}) %collective-permute-start.11) | collective-permute-done | bytes 98336 | tf_op jit(solution)/shard_map/ppermute | solution.py:40
  131.6 0.9 collective-permute-done.13
  132.5 0.2 fusion.51
  132.7 1.5 convolution_convert_fusion.1
  134.2 0.1 copy.59
  134.4 0.2 reshape.80
  134.5 17.8 %all_to_all.34 = bf16[64,2,256]{2,1,0:T(2,128)(2,1)S(1)} all-to-all(bf16[64,2,256]{2,1,0:T(2,128)(2,1)S(1)} %reshape.80), channel_id=1, replica_groups=mesh['z'=8,'y'=4,'x'=4,'c'=2] {'z','x','c'}, dimensions={0} | all-to-all | bytes 131072 | tf_op jit(solution)/shard_map/all_to_all | solution.py:25
  152.4 0.1 reshape.81
  152.7 0.7 convert_element_type.231
  (80 shorter events, 1.2 us)
Async XLA Ops:
  7.2 27.6 %copy-start.4 = (bf16[704,64]{0,1:T(8,128)(2,1)S(1)}, bf16[704,64]{0,1:T(8,128)(2,1)}, u32[]{:S(2)}) copy-start(bf16[704,64]{0,1:T(8,128)(2,1)} %param.32) | copy-start | bytes 270340
  7.2 23.8 %copy-start.12 = (f32[64]{0:T(128)S(1)}, f32[64]{0:T(128)}, u32[]{:S(2)}) copy-start(f32[64]{0:T(128)} %param.44) | copy-start | bytes 772
  7.2 23.8 %copy-start.6 = (bf16[64,704]{1,0:T(8,128)(2,1)S(1)}, bf16[64,704]{1,0:T(8,128)(2,1)}, u32[]{:S(2)}) copy-start(bf16[64,704]{1,0:T(8,128)(2,1)} %param.45) | copy-start | bytes 270340
  7.2 23.8 %copy-start.5 = (bf16[64,704]{1,0:T(8,128)(2,1)S(1)}, bf16[64,704]{1,0:T(8,128)(2,1)}, u32[]{:S(2)}) copy-start(bf16[64,704]{1,0:T(8,128)(2,1)} %param.46) | copy-start | bytes 270340
  7.2 26.8 %copy-start.7 = (bf16[704,64]{0,1:T(8,128)(2,1)S(1)}, bf16[704,64]{0,1:T(8,128)(2,1)}, u32[]{:S(2)}) copy-start(bf16[704,64]{0,1:T(8,128)(2,1)} %param.47) | copy-start | bytes 270340
  9.3 21.0 %collective-permute-start = (bf16[64,2112]{1,0:T(8,128)(2,1)S(1)}, bf16[64,2112]{1,0:T(8,128)(2,1)S(1)}, u32[]{:S(2)}, u32[]{:S(2)}) collective-permute-start(bf16[64,2112]{1,0:T(8,128)(2,1)S(1)} %pad_maximum_fusion), channel_id=1, source_target_pairs={{0,224},{32,0},{64,32},{96,64},{128,96},{160,128},{192,160},{224,1... | collective-permute-start | bytes 811016 | tf_op jit(solution)/shard_map/ppermute | solution.py:66
  15.7 14.5 %collective-permute-start.3 = (bf16[64,2112]{1,0:T(8,128)(2,1)S(1)}, bf16[64,2112]{1,0:T(8,128)(2,1)S(1)}, u32[]{:S(2)}, u32[]{:S(2)}) collective-permute-start(bf16[64,2112]{1,0:T(8,128)(2,1)S(1)} %pad_maximum_fusion), channel_id=1, source_target_pairs={{0,32},{32,64},{64,96},{96,128},{128,160},{160,192},{192,224},{224... | collective-permute-start | bytes 811016 | tf_op jit(solution)/shard_map/ppermute | solution.py:65
  21.6 17.9 %all-to-all-start = ((bf16[64,2,128]{2,1,0:T(2,128)(2,1)}), bf16[64,2,128]{2,1,0:T(2,128)(2,1)S(1)}, u32[]{:S(2)}, u32[]{:S(2)}) async-start(bf16[64,2,128]{2,1,0:T(2,128)(2,1)} %reshape.78), calls=%async_computation | async-start | bytes 65536 | tf_op jit(solution)/shard_map/all_to_all | solution.py:25
  30.2 60.5 %all-gather.5.cloned.1.call-start = ((), (), s32[]{:S(2)}) async-start(), calls=%async_computation.7 | async-start | bytes 2506752 | tf_op jit(solution)/shard_map/all_gather | solution.py:197
  31.0 92.7 %all-gather.3.cloned.1.call-start = ((), (), s32[]{:S(2)}) async-start(), calls=%async_computation.6 | async-start | bytes 2506752 | tf_op jit(solution)/shard_map/all_gather | solution.py:197
  31.1 8.5 %collective-permute-start.1 = (bf16[64,2112]{1,0:T(8,128)(2,1)S(1)}, bf16[64,2112]{1,0:T(8,128)(2,1)S(1)}, u32[]{:S(2)}, u32[]{:S(2)}) collective-permute-start(bf16[64,2112]{1,0:T(8,128)(2,1)S(1)} %collective-permute-done), channel_id=1, source_target_pairs={{0,224},{32,0},{64,32},{96,64},{128,96},{160,128},{192,160},{224,1... | collective-permute-start | bytes 811016 | tf_op jit(solution)/shard_map/ppermute | solution.py:66
  34.0 9.0 %collective-permute-start.4 = (bf16[64,2112]{1,0:T(8,128)(2,1)S(1)}, bf16[64,2112]{1,0:T(8,128)(2,1)S(1)}, u32[]{:S(2)}, u32[]{:S(2)}) collective-permute-start(bf16[64,2112]{1,0:T(8,128)(2,1)S(1)} %collective-permute-done.3), channel_id=1, source_target_pairs={{0,32},{32,64},{64,96},{96,128},{128,160},{160,192},{192,224},{224... | collective-permute-start | bytes 811016 | tf_op jit(solution)/shard_map/ppermute | solution.py:65
  39.7 11.0 %collective-permute-start.2 = (bf16[64,2112]{1,0:T(8,128)(2,1)S(1)}, bf16[64,2112]{1,0:T(8,128)(2,1)S(1)}, u32[]{:S(2)}, u32[]{:S(2)}) collective-permute-start(bf16[64,2112]{1,0:T(8,128)(2,1)S(1)} %collective-permute-done.1), channel_id=1, source_target_pairs={{0,224},{32,0},{64,32},{96,64},{128,96},{160,128},{192,160},{224,1... | collective-permute-start | bytes 811016 | tf_op jit(solution)/shard_map/ppermute | solution.py:66
  43.1 9.9 %collective-permute-start.5 = (bf16[64,2112]{1,0:T(8,128)(2,1)S(1)}, bf16[64,2112]{1,0:T(8,128)(2,1)S(1)}, u32[]{:S(2)}, u32[]{:S(2)}) collective-permute-start(bf16[64,2112]{1,0:T(8,128)(2,1)S(1)} %collective-permute-done.4), channel_id=1, source_target_pairs={{0,32},{32,64},{64,96},{96,128},{128,160},{160,192},{192,224},{224... | collective-permute-start | bytes 811016 | tf_op jit(solution)/shard_map/ppermute | solution.py:65
  43.1 11.2 %copy-start.8 = (bf16[512,704]{1,0:T(8,128)(2,1)}, bf16[512,704]{1,0:T(8,128)(2,1)S(1)}, u32[]{:S(2)}) copy-start(bf16[512,704]{1,0:T(8,128)(2,1)S(1)} %slice_dynamic-update-slice_fusion.2) | copy-start | bytes 2162692
  53.0 9.8 %collective-permute-start.7 = (bf16[64,1088]{1,0:T(8,128)(2,1)S(1)}, bf16[64,1088]{1,0:T(8,128)(2,1)S(1)}, u32[]{:S(2)}, u32[]{:S(2)}) collective-permute-start(bf16[64,1088]{1,0:T(8,128)(2,1)S(1)} %slice.189), channel_id=1, source_target_pairs={{0,224},{32,0},{64,32},{96,64},{128,96},{160,128},{192,160},{224,1... | collective-permute-start | bytes 417800 | tf_op jit(solution)/shard_map/ppermute | solution.py:69
  54.4 8.5 %collective-permute-start.6 = (bf16[64,1024]{1,0:T(8,128)(2,1)S(1)}, bf16[64,1024]{1,0:T(8,128)(2,1)S(1)}, u32[]{:S(2)}, u32[]{:S(2)}) collective-permute-start(bf16[64,1024]{1,0:T(8,128)(2,1)S(1)} %slice.188), channel_id=1, source_target_pairs={{0,32},{32,64},{64,96},{96,128},{128,160},{160,192},{192,224},{224... | collective-permute-start | bytes 393224 | tf_op jit(solution)/shard_map/ppermute | solution.py:68
  54.7 2.4 %copy-start.10 = (f32[128]{0:T(128)S(1)}, f32[128]{0:T(128)}, u32[]{:S(2)}) copy-start(f32[128]{0:T(128)} %constant.59) | copy-start | bytes 1540
  54.7 2.4 %copy-start.11 = (f32[128]{0:T(128)S(1)}, f32[128]{0:T(128)}, u32[]{:S(2)}) copy-start(f32[128]{0:T(128)} %constant.60) | copy-start | bytes 1540
  55.8 11.8 %copy-start.9 = (bf16[512,704]{1,0:T(8,128)(2,1)S(1)}, bf16[512,704]{1,0:T(8,128)(2,1)}, u32[]{:S(2)}) copy-start(bf16[512,704]{1,0:T(8,128)(2,1)} %slice_dynamic-update-slice_fusion.5) | copy-start | bytes 2162692
  63.1 4.7 %collective-permute-start.10 = (bf16[32,1536]{1,0:T(8,128)(2,1)S(1)}, bf16[32,1536]{1,0:T(8,128)(2,1)S(1)}, u32[]{:S(2)}, u32[]{:S(2)}) collective-permute-start(bf16[32,1536]{1,0:T(8,128)(2,1)S(1)} %pad_maximum_fusion.6), channel_id=1, source_target_pairs={{0,24},{8,0},{16,8},{24,16},{1,25},{9,1},{17,9},{25,17},{2,26},{10... | collective-permute-start | bytes 294920 | tf_op jit(solution)/shard_map/ppermute | solution.py:40
  66.1 6.1 %collective-permute-start.8 = (bf16[32,1536]{1,0:T(8,128)(2,1)S(1)}, bf16[32,1536]{1,0:T(8,128)(2,1)S(1)}, u32[]{:S(2)}, u32[]{:S(2)}) collective-permute-start(bf16[32,1536]{1,0:T(8,128)(2,1)S(1)} %pad_maximum_fusion.6), channel_id=1, source_target_pairs={{0,8},{8,16},{16,24},{24,0},{1,9},{9,17},{17,25},{25,1},{2,10},{10... | collective-permute-start | bytes 294920 | tf_op jit(solution)/shard_map/ppermute | solution.py:40
  66.1 6.1 %collective-permute-start.9 = (bf16[32,1536]{1,0:T(8,128)(2,1)S(1)}, bf16[32,1536]{1,0:T(8,128)(2,1)S(1)}, u32[]{:S(2)}, u32[]{:S(2)}) collective-permute-start(bf16[32,1536]{1,0:T(8,128)(2,1)S(1)} %pad_maximum_fusion.6), channel_id=1, source_target_pairs={{0,16},{8,24},{16,0},{24,8},{1,17},{9,25},{17,1},{25,9},{2,18},{10... | collective-permute-start | bytes 294920 | tf_op jit(solution)/shard_map/ppermute | solution.py:40
  73.0 27.8 %copy-start = (f32[8,4,128,128]{3,2,1,0:T(8,128)S(1)}, f32[8,4,128,128]{3,2,1,0:T(8,128)}, u32[]{:S(2)}) copy-start(f32[8,4,128,128]{3,2,1,0:T(8,128)} %state_ref.1) | copy-start | bytes 6291460
  73.0 27.8 %copy-start.1 = (f32[4]{0:T(128)S(1)}, f32[4]{0:T(128)}, u32[]{:S(2)}) copy-start(f32[4]{0:T(128)} %param.40) | copy-start | bytes 52
  73.0 27.8 %copy-start.2 = (f32[4]{0:T(128)S(1)}, f32[4]{0:T(128)}, u32[]{:S(2)}) copy-start(f32[4]{0:T(128)} %param.41) | copy-start | bytes 52
  73.0 27.8 %copy-start.3 = (f32[128]{0:T(128)S(1)}, f32[128]{0:T(128)}, u32[]{:S(2)}) copy-start(f32[128]{0:T(128)} %param.42) | copy-start | bytes 1540
  125.4 6.2 %collective-permute-start.11 = (bf16[32,1536]{1,0:T(8,128)(2,1)S(1)}, bf16[32,1536]{1,0:T(8,128)(2,1)S(1)}, u32[]{:S(2)}, u32[]{:S(2)}) collective-permute-start(bf16[32,1536]{1,0:T(8,128)(2,1)S(1)} %pad_maximum_fusion.7), channel_id=1, source_target_pairs={{0,8},{8,16},{16,24},{24,0},{1,9},{9,17},{17,25},{25,1},{2,10},{10... | collective-permute-start | bytes 294920 | tf_op jit(solution)/shard_map/ppermute | solution.py:40
  125.7 5.8 %collective-permute-start.12 = (bf16[32,1536]{1,0:T(8,128)(2,1)S(1)}, bf16[32,1536]{1,0:T(8,128)(2,1)S(1)}, u32[]{:S(2)}, u32[]{:S(2)}) collective-permute-start(bf16[32,1536]{1,0:T(8,128)(2,1)S(1)} %pad_maximum_fusion.7), channel_id=1, source_target_pairs={{0,16},{8,24},{16,0},{24,8},{1,17},{9,25},{17,1},{25,9},{2,18},{10... | collective-permute-start | bytes 294920 | tf_op jit(solution)/shard_map/ppermute | solution.py:40
  127.5 4.9 %collective-permute-start.13 = (bf16[32,1536]{1,0:T(8,128)(2,1)S(1)}, bf16[32,1536]{1,0:T(8,128)(2,1)S(1)}, u32[]{:S(2)}, u32[]{:S(2)}) collective-permute-start(bf16[32,1536]{1,0:T(8,128)(2,1)S(1)} %pad_maximum_fusion.7), channel_id=1, source_target_pairs={{0,24},{8,0},{16,8},{24,16},{1,25},{9,1},{17,9},{25,17},{2,26},{10... | collective-permute-start | bytes 294920 | tf_op jit(solution)/shard_map/ppermute | solution.py:40
Sparse Core Ops, SparseCore 0:
  32.8 44.6 all-gather.4
  79.3 37.2 all-gather.2
